TPU v7x, 512 devices: a whole 4x8x8 slice. The times are simulated.
512 devices in a mesh: sp: 128 (over z, y, core), tp: 4 (over x).
Axes of the slice: x: 4, y: 8, z: 8, core: 2. Of those that a mesh axis runs over, the one named last changes fastest.
Arguments:
- stream: bfloat16 [32768, 2048], P('sp', 'tp'), may hold values from -6 to 6
- norm_gain: float32 [2, 2048], replicated, may hold values from 0.1 to 1.9
- w_value: bfloat16 [2, 2048, 1024], P(None, 'sp', 'tp'), may hold values from -0.125 to 0.125
- w_gate: bfloat16 [2, 2048, 1024], P(None, 'sp', 'tp'), may hold values from -0.125 to 0.125
- conv_taps: float32 [2, 128, 1024], P(None, None, 'tp'), as said below
- channel_gain: float32 [2, 1024], P(None, 'tp'), may hold values from 0.1 to 1.9
- w_out: bfloat16 [2, 1024, 2048], P(None, 'tp', 'sp'), may hold values from -0.1875 to 0.1875
Outputs:
- result: bfloat16 [32768, 2048], P('sp', 'tp')
Inputs may be any that keep to these rules, and one draw needn't show every extreme that they name: `conv_taps`: taps of each block of 128 consecutive channels share a scale factor of its own.
All inputs are finite; a program needn't handle non-finite values.
Results may differ from a plain program's by a relative error of at most 0.012.
Values may be sent and summed in bfloat16 or wider, within the bound.
No kernel may reach another device: no remote copies, remote signals or barrier semaphores. Data moves between devices by JAX's collectives and lax.ppermute only.
A program may use at most 64 MiB of HBM per device.

v0:
```python
import jax
import jax.numpy as jnp
from jax import lax
from jax.experimental import pallas as pl
from jax.experimental.pallas import tpu as pltpu
from jax.sharding import Mesh
from jax.sharding import PartitionSpec as P


C = 1024
LAYERS = 2
NZ, NY, NX = 8, 8, 4
TOK, CH, TAPS, FEAT = 256, 256, 128, 512
ROWS = 32
PACK = TOK + 16
BF = jnp.bfloat16
F32 = jnp.float32
INTERPRET = False


def at(z, y, c):
    return (z * NY + y) * 2 + c


ALONG_Y = [[at(z, y, 0) for y in range(NY)] for z in range(NZ)]
ALONG_Z = [[at(z, y, 1) for z in range(NZ)] for y in range(NY)]
ALONG_Y1 = [[at(z, y, 1) for y in range(NY)] for z in range(NZ)]
ALONG_Z0 = [[at(z, y, 0) for z in range(NZ)] for y in range(NY)]


def to_group(block, groups):
    n = len(groups[0])
    copies = jnp.broadcast_to(block, (n, *block.shape))
    return lax.all_to_all(
        copies, "sp", split_axis=0, concat_axis=0, tiled=True, axis_index_groups=groups
    )


def lines(block):
    return to_group(block, ALONG_Y + ALONG_Z)


def plane(once):
    return to_group(once, ALONG_Z0 + ALONG_Y1)


def after(v, earlier):
    return lax.optimization_barrier((v, earlier))[0]


def swap_cores(v):
    count = lax.axis_size("sp")
    return lax.ppermute(v, "sp", [(i, i ^ 1) for i in range(count)])


def by_core(first, mine, other):
    return jnp.where(first, mine, other), jnp.where(first, other, mine)


def to_column_owner(v, flip):
    nb = NZ // NX
    pairs = []
    for z in range(NZ):
        a, b = divmod(z, nb)
        for y in range(NY):
            for c in range(2):
                for x in range(NX):
                    half = c ^ flip
                    place = (x * nb + b, y) if half == 0 else (y, x * nb + b)
                    pairs.append((at(z, y, c) * NX + x, at(*place, half) * NX + a))
    return lax.ppermute(v, ("sp", "x"), pairs)


def from_all_x(v):
    return [v] + [
        lax.ppermute(v, "x", [(i, (i + step) % NX) for i in range(NX)]) for step in range(1, NX)
    ]


def exchange_x(copies):
    return [lax.all_to_all(copies, "x", split_axis=0, concat_axis=0, tiled=True)]


def part_of(refs, k):
    if len(refs) == 1:
        return refs[0].at[k], k
    return refs[k], (lax.axis_index("x") + NX - k) % NX


def core_here():
    return lax.axis_index("sp") % 2


def norm_kernel(layer, n, *refs):
    parts, (gain, xs) = refs[:n], refs[n:]

    def rows_at(i, _):
        rows = pl.ds(pl.multiple_of(i * 16, 16), 16)
        total = jnp.zeros((16, 128), F32)
        held = []
        for k in range(NX):
            ref, owner = part_of(parts, k)
            v = ref[rows, :].astype(F32)
            held.append((v, owner))
            sq = v * v
            for q in range(FEAT // 128):
                total += sq[:, q * 128 : (q + 1) * 128]
        scale = lax.rsqrt(jnp.sum(total, axis=1, keepdims=True) / (NX * FEAT) + 1e-06)
        for v, owner in held:
            g = gain[layer * NX + owner]
            xs[owner, rows, :] = (v * scale * g).astype(BF)
        return 0

    lax.fori_loop(0, TOK // 16, rows_at, 0)


def mix_kernel(xs, mine, other, glu, vs, gs):
    def fill(zy, yz):
        for z in range(NZ):
            rows = slice(z * NY * ROWS, (z + 1) * NY * ROWS)
            vs[rows, :] = zy[z, :, :ROWS, :].reshape(NY * ROWS, CH)
            gs[rows, :] = yz[:, z, :ROWS, :].reshape(NY * ROWS, CH)

    @pl.when(core_here() == 0)
    def _():
        fill(mine, other)

    @pl.when(core_here() == 1)
    def _():
        fill(other, mine)

    value = jnp.zeros((TOK, CH), F32)
    gate = jnp.zeros((TOK, CH), F32)
    for k in range(NX):
        rows = slice(k * FEAT, (k + 1) * FEAT)
        value += jnp.dot(xs[k], vs[rows, :], preferred_element_type=F32)
        gate += jnp.dot(xs[k], gs[rows, :], preferred_element_type=F32)
    glu[...] = (value * jax.nn.sigmoid(gate)).astype(BF)


def split_three(v):
    hi = v.astype(BF).astype(F32)
    mid = (v - hi).astype(BF).astype(F32)
    return [hi, mid, v - hi - mid]


def conv_kernel(layer, copies, before, glu, taps, gain, out, ext, shifted, conv):
    ext[:TAPS, :] = before[...].astype(F32)
    ext[TAPS:, :] = glu[...].astype(F32)
    span = TOK + TAPS - 8
    for b in range(8):
        shifted[b] = ext[1 + b : 1 + b + span, :]
    for lane in range(0, CH, 128):
        for base in range(0, TOK, 128):

            def step(a, acc):
                start = pl.multiple_of(a * 8, 8)
                tap = taps[layer, pl.ds(start, 8), lane : lane + 128]
                for b in range(8):
                    window = shifted[b, pl.ds(start + base, 128), lane : lane + 128]
                    acc += window * tap[b : b + 1]
                return acc

            acc = lax.fori_loop(0, TAPS // 8, step, jnp.zeros((128, 128), F32))
            conv[base : base + 128, lane : lane + 128] = acc

    def centre(i, _):
        rows = pl.ds(pl.multiple_of(i * 32, 32), 32)
        v = conv[rows, :]
        d = (v - jnp.mean(v, axis=1, keepdims=True)).astype(BF)
        for k in range(copies):
            out[k, rows, :] = d
        return 0

    lax.fori_loop(0, TOK // 32, centre, 0)
    ones = jnp.full((8, CH), 1.0 / CH, F32)
    means = lax.dot_general(
        ones, conv[...], (((1,), (1,)), ((), ())), precision=lax.Precision.HIGHEST,
        preferred_element_type=F32,
    )[:1]
    extra = split_three(means) + split_three(gain[layer : layer + 1, :])
    extra = jnp.concatenate(extra + [jnp.zeros((10, CH), F32)], axis=0).astype(BF)
    for k in range(copies):
        out[k, TOK:, :] = extra


def out_kernel(n, copies, *refs):
    parts, rest = refs[:n], refs[n:]
    x, mine, other, out, means, acts, wt = rest
    pick = (lax.broadcasted_iota(jnp.int32, (16, 128), 0) < 3).astype(BF)
    total = jnp.zeros((TOK, 128), F32)
    for k in range(NX):
        ref, _ = part_of(parts, k)
        m = lax.dot_general(
            ref[TOK:, :], pick, (((0,), (0,)), ((), ())), preferred_element_type=F32
        )
        means[k] = m
        total += m
    means[NX] = total / NX

    def rows_at(i, _):
        rows = pl.ds(pl.multiple_of(i * 16, 16), 16)
        held = []
        square = jnp.zeros((16, 128), F32)
        for k in range(NX):
            ref, owner = part_of(parts, k)
            shift = means[k, rows, :] - means[NX, rows, :]
            v = ref[rows, :].astype(F32)
            v = jnp.concatenate([v[:, :128] + shift, v[:, 128:] + shift], axis=1)
            sq = v * v
            square += sq[:, :128] + sq[:, 128:]
            tail = ref[TOK:, :].astype(F32)
            g = tail[3:4] + tail[4:5] + tail[5:6]
            held.append((v, g, owner))
        scale = lax.rsqrt(jnp.sum(square, axis=1, keepdims=True) / C + 1e-05)
        for v, g, owner in held:
            u = v * scale * g
            acts[owner, rows, :] = (u / (1.0 + jnp.exp(-u))).astype(BF)
        return 0

    lax.fori_loop(0, TOK // 16, rows_at, 0)

    def fill(halves):
        for k in range(NX):
            for h, ref in enumerate(halves):
                for q in range(2):
                    for i in range(2):
                        w = ref[k * 2 + i, :, ROWS:, q * 128 : (q + 1) * 128]
                        wt[k, i * NY : (i + 1) * NY, q, :, h * 128 : (h + 1) * 128] = w

    @pl.when(core_here() == 0)
    def _():
        fill((mine, other))

    @pl.when(core_here() == 1)
    def _():
        fill((other, mine))

    branch = jnp.zeros((TOK, FEAT), F32)
    for k in range(NX):
        branch += lax.dot_general(
            acts[k], wt[k].reshape(FEAT, CH), (((1,), (1,)), ((), ())),
            preferred_element_type=F32,
        )
    new = (x[...].astype(F32) + branch).astype(BF)
    for k in range(copies):
        out[k] = new


def call(body, out, ins, scratch, flops):
    return pl.pallas_call(
        body,
        out_shape=out,
        in_specs=[pl.BlockSpec(memory_space=pltpu.VMEM)] * len(ins),
        out_specs=pl.BlockSpec(memory_space=pltpu.VMEM),
        scratch_shapes=scratch,
        cost_estimate=pl.CostEstimate(flops=flops, transcendentals=0, bytes_accessed=1 << 20),
        compiler_params=pltpu.CompilerParams(vmem_limit_bytes=40 << 20),
        interpret=INTERPRET,
    )(*ins)


def normalise(layer, parts, gain):
    def body(*refs):
        norm_kernel(layer, len(parts), *refs)

    return call(
        body, jax.ShapeDtypeStruct((NX, TOK, FEAT), BF), [*parts, gain], [], 8 * NX * TOK * FEAT
    )


def mix(xs, mine, other):
    return call(
        mix_kernel,
        jax.ShapeDtypeStruct((TOK, CH), BF),
        [xs, mine, other],
        [pltpu.VMEM((NX * FEAT, CH), BF), pltpu.VMEM((NX * FEAT, CH), BF)],
        4 * NX * TOK * FEAT * CH,
    )


def convolve(layer, copies, before, glu, taps, gain):
    def body(*refs):
        conv_kernel(layer, copies, *refs)

    return call(
        body,
        jax.ShapeDtypeStruct((copies, PACK, CH), BF),
        [before, glu, taps, gain],
        [
            pltpu.VMEM((TAPS + TOK, CH), F32),
            pltpu.VMEM((8, TOK + TAPS - 8, CH), F32),
            pltpu.VMEM((TOK, CH), F32),
        ],
        2 * TOK * CH * TAPS,
    )


def project(copies, parts, x, mine, other):
    def body(*refs):
        out_kernel(len(parts), copies, *refs)

    return call(
        body,
        jax.ShapeDtypeStruct((copies, TOK, FEAT), BF),
        [*parts, x, mine, other],
        [
            pltpu.VMEM((NX + 1, TOK, 128), F32),
            pltpu.VMEM((NX, TOK, CH), BF),
            pltpu.VMEM((NX, 2 * NY, 2, 16, CH), BF),
        ],
        2 * NX * TOK * CH * FEAT,
    )


def shards(stream, norm_gain, w_value, w_gate, conv_taps, channel_gain, w_out):
    first = core_here() == 0
    gain = norm_gain.reshape(LAYERS * NX, 1, FEAT)

    keep, send = by_core(first, w_value, w_gate)
    top, bottom = by_core(first, keep, swap_cores(send))
    half_proj = jnp.concatenate([top, bottom], axis=1)
    out_t = jnp.swapaxes(w_out, 1, 2)
    keep, send = by_core(first, out_t[:, :, : CH // 2], out_t[:, :, CH // 2 :])
    left, right = by_core(first, to_column_owner(keep, 0), to_column_owner(send, 1))
    half_out = jnp.concatenate([left, right], axis=2)
    blocks = jnp.concatenate([half_proj, half_out], axis=1)

    x = stream
    count = lax.axis_size("sp")
    once = lines(blocks[0])
    parts = from_all_x(after(x, once))
    gathered = plane(once)
    for layer in range(LAYERS):
        last = layer + 1 == LAYERS
        mine = gathered
        other = swap_cores(mine)
        if not last:
            following = lines(after(blocks[layer + 1], gathered))
        normed = normalise(layer, parts, gain)
        glu = mix(normed, mine, other)
        if not last:
            gathered = plane(after(following, glu))
        before = lax.ppermute(glu[TOK - TAPS :], "sp", [(i, i + 1) for i in range(count - 1)])
        packed = convolve(layer, NX if last else 1, before, glu, conv_taps, channel_gain)
        parts = exchange_x(packed) if last else from_all_x(packed[0])
        new = project(1 if last else NX, parts, x, mine, other)
        x = new[0]
        if not last:
            parts = exchange_x(new)
    return x


def solution(mesh):
    flat = Mesh(mesh.devices, ("sp", "x"))
    in_specs = (
        P("sp", "x"),
        P(),
        P(None, "sp", "x"),
        P(None, "sp", "x"),
        P(None, None, "x"),
        P(None, "x"),
        P(None, "x", "sp"),
    )

    return jax.shard_map(shards, mesh=flat, in_specs=in_specs, out_specs=P("sp", "x"), check_vma=False)
```

profile of v0, /device:TPU:16, one launch (start us, length us, event | category | flops | bytes accessed | tf_op | source)
XLA Modules:
  0.0 210.0 jit_solution(6041914367362493474)
XLA Ops:
  1.4 6.6 %collective-permute-start.2 = (bf16[2,16,128]{2,1,0:T(8,128)(2,1)S(1)}, bf16[2,16,128]{2,1,0:T(8,128)(2,1)S(1)}, u32[]{:S(2)}, u32[]{:S(2)}) collective-permute-start(bf16[2,16,128]{2,1,0:T(8,128)(2,1)S(1)} %get-tuple-element.18), channel_id=1, source_target_pairs={{0,4},{1,20},{2,36},{3,52},{4,0},{5,128},{6,256},{7,384},{8,68},{9... | collective-permute-start | bytes 24584 | tf_op jit(solution)/shard_map/ppermute | solution.py:71
  12.5 18.7 %all_to_all.30 = bf16[8,48,256]{2,1,0:T(8,128)(2,1)S(1)} all-to-all(bf16[8,48,256]{2,1,0:T(8,128)(2,1)S(1)} %broadcast_in_dim.12), channel_id=1, replica_groups={{0,8,16,24,32,40,48,56},{64,72,80,88,96,104,112,120},{128,136,144,152,1..., dimensions={0} | all-to-all | bytes 393216 | tf_op jit(solution)/shard_map/all_to_all | solution.py:34
  31.4 34.9 %all_to_all.31.mine.refs_5_ = bf16[8,8,48,256]{3,2,1,0:T(8,128)(2,1)S(1)} all-to-all(bf16[8,8,48,256]{3,2,1,0:T(8,128)(2,1)S(1)} %broadcast_in_dim.13), channel_id=1, replica_groups={{0,64,128,192,256,320,384,448},{8,72,136,200,264,328,392,456},{16,80,14..., dimensions={0} | all-to-all | bytes 3145728 | tf_op jit(solution)/shard_map/all_to_all | solution.py:34
  68.9 6.8 %all-to-all-start.3 = ((bf16[8,48,256]{2,1,0:T(8,128)(2,1)}), bf16[8,48,256]{2,1,0:T(8,128)(2,1)}, u32[]{:S(2)}, u32[]{:S(2)}) async-start(bf16[8,48,256]{2,1,0:T(8,128)(2,1)} %broadcast_in_dim.14), calls=%async_computation.3 | async-start | bytes 393216 | tf_op jit(solution)/shard_map/all_to_all | solution.py:34
  75.7 6.3 %collective-permute-start.5 = (bf16[256,512]{1,0:T(8,128)(2,1)S(1)}, bf16[256,512]{1,0:T(8,128)(2,1)}, u32[]{:S(2)}, u32[]{:S(2)}) collective-permute-start(bf16[256,512]{1,0:T(8,128)(2,1)S(1)} %copy-done.7), channel_id=1, source_target_pairs={{0,3},{1,0},{2,1},{3,2},{4,7},{5,4},{6,5},{7,6},{8,11},{9,8},{10,9... | collective-permute-start | bytes 786440 | tf_op jit(solution)/shard_map/ppermute | solution.py:76
  83.9 2.8 %collective-permute-start.3 = (bf16[256,512]{1,0:T(8,128)(2,1)S(1)}, bf16[256,512]{1,0:T(8,128)(2,1)}, u32[]{:S(2)}, u32[]{:S(2)}) collective-permute-start(bf16[256,512]{1,0:T(8,128)(2,1)S(1)} %copy-done.7), channel_id=1, source_target_pairs={{0,1},{1,2},{2,3},{3,0},{4,5},{5,6},{6,7},{7,4},{8,9},{9,10},{10,1... | collective-permute-start | bytes 786440 | tf_op jit(solution)/shard_map/ppermute | solution.py:76
  86.7 4.3 %collective-permute-done.5.refs_3_ = bf16[256,512]{1,0:T(8,128)(2,1)} collective-permute-done((bf16[256,512]{1,0:T(8,128)(2,1)S(1)}, bf16[256,512]{1,0:T(8,128)(2,1)}, u32[]{:S(2)}, u32[]{:S(2)}) %collective-permute-start.5) | collective-permute-done | bytes 262176 | tf_op jit(solution)/shard_map/ppermute | solution.py:76
  91.0 2.9 %collective-permute-done.4.refs_2_ = bf16[256,512]{1,0:T(8,128)(2,1)} collective-permute-done((bf16[256,512]{1,0:T(8,128)(2,1)S(1)}, bf16[256,512]{1,0:T(8,128)(2,1)}, u32[]{:S(2)}, u32[]{:S(2)}) %collective-permute-start.4) | collective-permute-done | bytes 262176 | tf_op jit(solution)/shard_map/ppermute | solution.py:76
  93.9 2.8 %collective-permute-done.3.refs_1_ = bf16[256,512]{1,0:T(8,128)(2,1)} collective-permute-done((bf16[256,512]{1,0:T(8,128)(2,1)S(1)}, bf16[256,512]{1,0:T(8,128)(2,1)}, u32[]{:S(2)}, u32[]{:S(2)}) %collective-permute-start.3) | collective-permute-done | bytes 262176 | tf_op jit(solution)/shard_map/ppermute | solution.py:76
  96.7 2.9 %shard_map.73.xs = bf16[4,256,512]{2,1,0:T(8,128)(2,1)S(1)} custom-call(bf16[256,512]{1,0:T(8,128)(2,1)S(1)} %copy-done.7, bf16[256,512]{1,0:T(8,128)(2,1)} %collective-permute-done.3.refs_1_, bf16[256,512]{1,0:T(8,128)(2,1)} %collective-permute-done.4.refs_2_, bf16[256,512]{1,0:T(8,128)(2,1)} %collective-permute-done.5.refs_3_, ...), custom_call_target="tpu_custom_call" | custom-call | flops 4194304 | bytes 1048576 | tf_op jit(solution)/shard_map/pallas_call | solution.py:251
  102.0 29.7 %all_to_all.32.mine.refs_2_ = bf16[8,8,48,256]{3,2,1,0:T(8,128)(2,1)S(1)} all-to-all(bf16[8,8,48,256]{3,2,1,0:T(8,128)(2,1)S(1)} %broadcast_in_dim.15), channel_id=1, replica_groups={{0,64,128,192,256,320,384,448},{8,72,136,200,264,328,392,456},{16,80,14..., dimensions={0} | all-to-all | bytes 3145728 | tf_op jit(solution)/shard_map/all_to_all | solution.py:34
  133.6 2.4 %collective-permute-start.7 = (bf16[128,256]{1,0:T(8,128)(2,1)S(1)}, bf16[128,256]{1,0:T(8,128)(2,1)S(1)}, u32[]{:S(2)}, u32[]{:S(2)}) collective-permute-start(bf16[128,256]{1,0:T(8,128)(2,1)S(1)} %slice.31), channel_id=1, source_target_pairs={{0,4},{4,8},{8,12},{12,16},{16,20},{20,24},{24,28},{28,32},{32,36}... | collective-permute-start | bytes 196616 | tf_op jit(solution)/shard_map/ppermute | solution.py:344
  136.1 3.2 %collective-permute-done.7.refs_0_ = bf16[128,256]{1,0:T(8,128)(2,1)S(1)} collective-permute-done((bf16[128,256]{1,0:T(8,128)(2,1)S(1)}, bf16[128,256]{1,0:T(8,128)(2,1)S(1)}, u32[]{:S(2)}, u32[]{:S(2)}) %collective-permute-start.7) | collective-permute-done | bytes 65568 | tf_op jit(solution)/shard_map/ppermute | solution.py:344
  139.2 4.0 %shard_map.75 = bf16[1,272,256]{2,1,0:T(8,128)(2,1)S(1)} custom-call(bf16[128,256]{1,0:T(8,128)(2,1)S(1)} %collective-permute-done.7.refs_0_, bf16[256,256]{1,0:T(8,128)(2,1)S(1)} %shard_map.74.refs_1_, f32[2,128,256]{2,1,0:T(8,128)S(1)} %copy-done.6, f32[2,256]{1,0:T(2,128)S(1)} %copy-done.8), custom_call_target="tpu_custom_call" | custom-call | flops 16777216 | bytes 1048576 | tf_op jit(solution)/shard_map/pallas_call | solution.py:251
  147.4 3.6 %collective-permute-start.8 = (bf16[272,256]{1,0:T(8,128)(2,1)S(1)}, bf16[272,256]{1,0:T(8,128)(2,1)S(1)}, u32[]{:S(2)}, u32[]{:S(2)}) collective-permute-start(bf16[272,256]{1,0:T(8,128)(2,1)S(1)} %bitcast.11), channel_id=1, source_target_pairs={{0,1},{1,2},{2,3},{3,0},{4,5},{5,6},{6,7},{7,4},{8,9},{9,10},{10,1... | collective-permute-start | bytes 417800 | tf_op jit(solution)/shard_map/ppermute | solution.py:76
  151.5 2.5 %collective-permute-done.9.refs_2_ = bf16[272,256]{1,0:T(8,128)(2,1)S(1)} collective-permute-done((bf16[272,256]{1,0:T(8,128)(2,1)S(1)}, bf16[272,256]{1,0:T(8,128)(2,1)S(1)}, u32[]{:S(2)}, u32[]{:S(2)}) %collective-permute-start.9) | collective-permute-done | bytes 139296 | tf_op jit(solution)/shard_map/ppermute | solution.py:76
  154.0 2.9 %collective-permute-done.8.refs_1_ = bf16[272,256]{1,0:T(8,128)(2,1)S(1)} collective-permute-done((bf16[272,256]{1,0:T(8,128)(2,1)S(1)}, bf16[272,256]{1,0:T(8,128)(2,1)S(1)}, u32[]{:S(2)}, u32[]{:S(2)}) %collective-permute-start.8) | collective-permute-done | bytes 139296 | tf_op jit(solution)/shard_map/ppermute | solution.py:76
  156.9 3.0 %shard_map.76 = bf16[4,256,512]{2,1,0:T(8,128)(2,1)S(1)} custom-call(bf16[272,256]{1,0:T(8,128)(2,1)S(1)} %bitcast.12, bf16[272,256]{1,0:T(8,128)(2,1)S(1)} %collective-permute-done.8.refs_1_, bf16[272,256]{1,0:T(8,128)(2,1)S(1)} %collective-permute-done.9.refs_2_, bf16[272,256]{1,0:T(8,128)(2,1)S(1)} %collective-permute-done.10.refs_3_, ...), custom_call_target="tpu_custom_call" | custom-call | flops 268435456 | bytes 1048576 | tf_op jit(solution)/shard_map/pallas_call | solution.py:251
  160.8 16.7 %all_to_all.33.refs_0_ = bf16[4,256,512]{2,1,0:T(8,128)(2,1)S(1)} all-to-all(bf16[4,256,512]{2,1,0:T(8,128)(2,1)S(1)} %shard_map.76), channel_id=1, replica_groups=mesh['sp'=128,'tp'=4] {'tp'}, dimensions={0} | all-to-all | bytes 2097152 | tf_op jit(solution)/shard_map/all_to_all | solution.py:81
  182.7 3.7 %collective-permute-done.12.refs_0_ = bf16[128,256]{1,0:T(8,128)(2,1)S(1)} collective-permute-done((bf16[128,256]{1,0:T(8,128)(2,1)S(1)}, bf16[128,256]{1,0:T(8,128)(2,1)S(1)}, u32[]{:S(2)}, u32[]{:S(2)}) %collective-permute-start.12) | collective-permute-done | bytes 65568 | tf_op jit(solution)/shard_map/ppermute | solution.py:344
  186.3 4.0 %shard_map.79 = bf16[4,272,256]{2,1,0:T(8,128)(2,1)S(1)} custom-call(bf16[128,256]{1,0:T(8,128)(2,1)S(1)} %collective-permute-done.12.refs_0_, bf16[256,256]{1,0:T(8,128)(2,1)S(1)} %shard_map.78.refs_1_, f32[2,128,256]{2,1,0:T(8,128)S(1)} %copy-done.6, f32[2,256]{1,0:T(2,128)S(1)} %copy-done.8), custom_call_target="tpu_custom_call" | custom-call | flops 16777216 | bytes 1048576 | tf_op jit(solution)/shard_map/pallas_call | solution.py:251
  191.2 4.2 %all-to-all-start.5 = ((bf16[4,272,256]{2,1,0:T(8,128)(2,1)}), bf16[4,272,256]{2,1,0:T(8,128)(2,1)}, u32[]{:S(2)}, u32[]{:S(2)}) async-start(bf16[4,272,256]{2,1,0:T(8,128)(2,1)} %copy-done.5), calls=%async_computation.5 | async-start | bytes 1114112 | tf_op jit(solution)/shard_map/all_to_all | solution.py:81
  196.3 9.0 %all-to-all-done.5.refs_0_ = bf16[4,272,256]{2,1,0:T(8,128)(2,1)} async-done(((bf16[4,272,256]{2,1,0:T(8,128)(2,1)}), bf16[4,272,256]{2,1,0:T(8,128)(2,1)}, u32[]{:S(2)}, u32[]{:S(2)}) %all-to-all-start.5) | async-done | bytes 557088 | tf_op jit(solution)/shard_map/all_to_all | solution.py:81
  205.3 4.7 %shard_map.80 = bf16[1,256,512]{2,1,0:T(8,128)(2,1)} custom-call(bf16[4,272,256]{2,1,0:T(8,128)(2,1)} %all-to-all-done.5.refs_0_, bf16[256,512]{1,0:T(8,128)(2,1)S(1)} %slice_bitcast_fusion.refs_1_, bf16[8,8,48,256]{3,2,1,0:T(8,128)(2,1)S(1)} %all_to_all.32.mine.refs_2_, bf16[8,8,48,256]{3,2,1,0:T(8,128)(2,1)S(1)} %copy-done.3), custom_call_target="tpu_custom_call" | custom-call | flops 268435456 | bytes 1048576 | tf_op jit(solution)/shard_map/pallas_call | solution.py:251
  (52 shorter events, 27.1 us)
Async XLA Ops:
  0.7 10.0 %collective-permute-start.1 = (bf16[2,16,128]{2,1,0:T(8,128)(2,1)S(1)}, bf16[2,16,128]{2,1,0:T(8,128)(2,1)S(1)}, u32[]{:S(2)}, u32[]{:S(2)}) collective-permute-start(bf16[2,16,128]{2,1,0:T(8,128)(2,1)S(1)} %get-tuple-element.17), channel_id=1, source_target_pairs={{0,0},{1,128},{2,256},{3,384},{4,4},{5,20},{6,36},{7,52},{8,8},{9,... | collective-permute-start | bytes 24584 | tf_op jit(solution)/shard_map/ppermute | solution.py:71
  1.4 9.3 %collective-permute-start.2 = (bf16[2,16,128]{2,1,0:T(8,128)(2,1)S(1)}, bf16[2,16,128]{2,1,0:T(8,128)(2,1)S(1)}, u32[]{:S(2)}, u32[]{:S(2)}) collective-permute-start(bf16[2,16,128]{2,1,0:T(8,128)(2,1)S(1)} %get-tuple-element.18), channel_id=1, source_target_pairs={{0,4},{1,20},{2,36},{3,52},{4,0},{5,128},{6,256},{7,384},{8,68},{9... | collective-permute-start | bytes 24584 | tf_op jit(solution)/shard_map/ppermute | solution.py:71
  8.7 3.1 %collective-permute-start = (bf16[2,16,256]{2,1,0:T(8,128)(2,1)S(1)}, bf16[2,16,256]{2,1,0:T(8,128)(2,1)S(1)}, u32[]{:S(2)}, u32[]{:S(2)}) collective-permute-start(bf16[2,16,256]{2,1,0:T(8,128)(2,1)S(1)} %broadcast_select_fusion.2), channel_id=1, source_target_pairs={{0,4},{4,0},{8,12},{12,8},{16,20},{20,16},{24,28},{28,24},{32,36},... | collective-permute-start | bytes 49160 | tf_op jit(solution)/shard_map/ppermute | solution.py:53
  31.4 44.3 %copy-start.7 = (bf16[256,512]{1,0:T(8,128)(2,1)S(1)}, bf16[256,512]{1,0:T(8,128)(2,1)}, u32[]{:S(2)}) copy-start(bf16[256,512]{1,0:T(8,128)(2,1)} %refs_4_.1) | copy-start | bytes 786436
  31.4 55.2 %copy-start.9 = (f32[2,2048]{1,0:T(2,128)S(1)}, f32[2,2048]{1,0:T(2,128)}, u32[]{:S(2)}) copy-start(f32[2,2048]{1,0:T(2,128)} %param.8) | copy-start | bytes 49156
  66.3 33.4 %collective-permute-start.6 = (bf16[8,8,48,256]{3,2,1,0:T(8,128)(2,1)S(1)}, bf16[8,8,48,256]{3,2,1,0:T(8,128)(2,1)S(1)}, u32[]{:S(2)}, u32[]{:S(2)}) collective-permute-start(bf16[8,8,48,256]{3,2,1,0:T(8,128)(2,1)S(1)} %all_to_all.31.mine.refs_5_), channel_id=1, source_target_pairs={{0,4},{4,0},{8,12},{12,8},{16,20},{20,16},{24,28},{28,24},{32,36},... | collective-permute-start | bytes 4718600 | tf_op jit(solution)/shard_map/ppermute | solution.py:53
  68.9 32.0 %all-to-all-start.3 = ((bf16[8,48,256]{2,1,0:T(8,128)(2,1)}), bf16[8,48,256]{2,1,0:T(8,128)(2,1)}, u32[]{:S(2)}, u32[]{:S(2)}) async-start(bf16[8,48,256]{2,1,0:T(8,128)(2,1)} %broadcast_in_dim.14), calls=%async_computation.3 | async-start | bytes 393216 | tf_op jit(solution)/shard_map/all_to_all | solution.py:34
  75.7 15.3 %collective-permute-start.5 = (bf16[256,512]{1,0:T(8,128)(2,1)S(1)}, bf16[256,512]{1,0:T(8,128)(2,1)}, u32[]{:S(2)}, u32[]{:S(2)}) collective-permute-start(bf16[256,512]{1,0:T(8,128)(2,1)S(1)} %copy-done.7), channel_id=1, source_target_pairs={{0,3},{1,0},{2,1},{3,2},{4,7},{5,4},{6,5},{7,6},{8,11},{9,8},{10,9... | collective-permute-start | bytes 786440 | tf_op jit(solution)/shard_map/ppermute | solution.py:76
  81.9 12.0 %collective-permute-start.4 = (bf16[256,512]{1,0:T(8,128)(2,1)S(1)}, bf16[256,512]{1,0:T(8,128)(2,1)}, u32[]{:S(2)}, u32[]{:S(2)}) collective-permute-start(bf16[256,512]{1,0:T(8,128)(2,1)S(1)} %copy-done.7), channel_id=1, source_target_pairs={{0,2},{1,3},{2,0},{3,1},{4,6},{5,7},{6,4},{7,5},{8,10},{9,11},{10,... | collective-permute-start | bytes 786440 | tf_op jit(solution)/shard_map/ppermute | solution.py:76
  83.9 12.9 %collective-permute-start.3 = (bf16[256,512]{1,0:T(8,128)(2,1)S(1)}, bf16[256,512]{1,0:T(8,128)(2,1)}, u32[]{:S(2)}, u32[]{:S(2)}) collective-permute-start(bf16[256,512]{1,0:T(8,128)(2,1)S(1)} %copy-done.7), channel_id=1, source_target_pairs={{0,1},{1,2},{2,3},{3,0},{4,5},{5,6},{6,7},{7,4},{8,9},{9,10},{10,1... | collective-permute-start | bytes 786440 | tf_op jit(solution)/shard_map/ppermute | solution.py:76
  99.7 1.2 copy-start
  101.9 37.3 %copy-start.6 = (f32[2,128,256]{2,1,0:T(8,128)S(1)}, f32[2,128,256]{2,1,0:T(8,128)}, u32[]{:S(2)}) copy-start(f32[2,128,256]{2,1,0:T(8,128)} %refs_2_.3) | copy-start | bytes 786436
  101.9 37.3 %copy-start.8 = (f32[2,256]{1,0:T(2,128)S(1)}, f32[2,256]{1,0:T(2,128)}, u32[]{:S(2)}) copy-start(f32[2,256]{1,0:T(2,128)} %refs_3_.3) | copy-start | bytes 6148
  102.0 54.9 %copy-start.1 = (bf16[8,8,48,256]{3,2,1,0:T(8,128)(2,1)S(1)}, bf16[8,8,48,256]{3,2,1,0:T(8,128)(2,1)}, u32[]{:S(2)}) copy-start(bf16[8,8,48,256]{3,2,1,0:T(8,128)(2,1)} %copy-done) | copy-start | bytes 4718596
  131.7 47.7 %collective-permute-start.11 = (bf16[8,8,48,256]{3,2,1,0:T(8,128)(2,1)S(1)}, bf16[8,8,48,256]{3,2,1,0:T(8,128)(2,1)S(1)}, u32[]{:S(2)}, u32[]{:S(2)}) collective-permute-start(bf16[8,8,48,256]{3,2,1,0:T(8,128)(2,1)S(1)} %all_to_all.32.mine.refs_2_), channel_id=1, source_target_pairs={{0,4},{4,0},{8,12},{12,8},{16,20},{20,16},{24,28},{28,24},{32,36},... | collective-permute-start | bytes 4718600 | tf_op jit(solution)/shard_map/ppermute | solution.py:53
  133.6 5.6 %collective-permute-start.7 = (bf16[128,256]{1,0:T(8,128)(2,1)S(1)}, bf16[128,256]{1,0:T(8,128)(2,1)S(1)}, u32[]{:S(2)}, u32[]{:S(2)}) collective-permute-start(bf16[128,256]{1,0:T(8,128)(2,1)S(1)} %slice.31), channel_id=1, source_target_pairs={{0,4},{4,8},{8,12},{12,16},{16,20},{20,24},{24,28},{28,32},{32,36}... | collective-permute-start | bytes 196616 | tf_op jit(solution)/shard_map/ppermute | solution.py:344
  143.2 8.2 %collective-permute-start.10 = (bf16[272,256]{1,0:T(8,128)(2,1)S(1)}, bf16[272,256]{1,0:T(8,128)(2,1)S(1)}, u32[]{:S(2)}, u32[]{:S(2)}) collective-permute-start(bf16[272,256]{1,0:T(8,128)(2,1)S(1)} %bitcast.9), channel_id=1, source_target_pairs={{0,3},{1,0},{2,1},{3,2},{4,7},{5,4},{6,5},{7,6},{8,11},{9,8},{10,9... | collective-permute-start | bytes 417800 | tf_op jit(solution)/shard_map/ppermute | solution.py:76
  145.4 8.5 %collective-permute-start.9 = (bf16[272,256]{1,0:T(8,128)(2,1)S(1)}, bf16[272,256]{1,0:T(8,128)(2,1)S(1)}, u32[]{:S(2)}, u32[]{:S(2)}) collective-permute-start(bf16[272,256]{1,0:T(8,128)(2,1)S(1)} %bitcast.10), channel_id=1, source_target_pairs={{0,2},{1,3},{2,0},{3,1},{4,6},{5,7},{6,4},{7,5},{8,10},{9,11},{10,... | collective-permute-start | bytes 417800 | tf_op jit(solution)/shard_map/ppermute | solution.py:76
  147.4 9.5 %collective-permute-start.8 = (bf16[272,256]{1,0:T(8,128)(2,1)S(1)}, bf16[272,256]{1,0:T(8,128)(2,1)S(1)}, u32[]{:S(2)}, u32[]{:S(2)}) collective-permute-start(bf16[272,256]{1,0:T(8,128)(2,1)S(1)} %bitcast.11), channel_id=1, source_target_pairs={{0,1},{1,2},{2,3},{3,0},{4,5},{5,6},{6,7},{7,4},{8,9},{9,10},{10,1... | collective-permute-start | bytes 417800 | tf_op jit(solution)/shard_map/ppermute | solution.py:76
  159.9 1.0 copy-start.4
  179.4 1.2 copy-start.2
  180.6 24.7 %copy-start.3 = (bf16[8,8,48,256]{3,2,1,0:T(8,128)(2,1)S(1)}, bf16[8,8,48,256]{3,2,1,0:T(8,128)(2,1)}, u32[]{:S(2)}) copy-start(bf16[8,8,48,256]{3,2,1,0:T(8,128)(2,1)} %copy-done.2) | copy-start | bytes 4718596
  180.6 5.7 %collective-permute-start.12 = (bf16[128,256]{1,0:T(8,128)(2,1)S(1)}, bf16[128,256]{1,0:T(8,128)(2,1)S(1)}, u32[]{:S(2)}, u32[]{:S(2)}) collective-permute-start(bf16[128,256]{1,0:T(8,128)(2,1)S(1)} %slice.33), channel_id=1, source_target_pairs={{0,4},{4,8},{8,12},{12,16},{16,20},{20,24},{24,28},{28,32},{32,36}... | collective-permute-start | bytes 196616 | tf_op jit(solution)/shard_map/ppermute | solution.py:344
  191.2 14.1 %all-to-all-start.5 = ((bf16[4,272,256]{2,1,0:T(8,128)(2,1)}), bf16[4,272,256]{2,1,0:T(8,128)(2,1)}, u32[]{:S(2)}, u32[]{:S(2)}) async-start(bf16[4,272,256]{2,1,0:T(8,128)(2,1)} %copy-done.5), calls=%async_computation.5 | async-start | bytes 1114112 | tf_op jit(solution)/shard_map/all_to_all | solution.py:81
  (1 other events, 0.8 us)
where the time goes:
time: 211 us; the launch traced here: 210 us
  blocking collectives  100 us (47%)
  starting transfers between devices  47.1 us (22%)
  waiting for transfers between devices  32.7 us (15%)
  Pallas kernels  22.2 us (11%)
  local copies, waits for them, and re-layouts  5.35 us (3%)
  other arithmetic  2.2 us (1%)
    all_to_all x3, blocking collectives, to_group(): lax.all_to_all(copies, 'sp', split_axis=0, concat_axis=0, tiled=True, axi...  83.3 us
    pallas_call x8, Pallas kernels, call(): pl.pallas_call(body, out_shape=out, in_specs=[pl.BlockSpec(memory_space=p...  22.2 us
    ppermute x6, starting transfers between devices, from_all_x(): lax.ppermute(v, 'x', [(i, (i + step) % NX) for i in range(NX)])  18.7 us
    all_to_all x1, blocking collectives, exchange_x(): lax.all_to_all(copies, 'x', split_axis=0, concat_axis=0, tiled=True)  16.7 us
    ppermute x6, waiting for transfers between devices, from_all_x(): lax.ppermute(v, 'x', [(i, (i + step) % NX) for i in range(NX)])  15.9 us
    all_to_all x1, waiting for transfers between devices, exchange_x(): lax.all_to_all(copies, 'x', split_axis=0, concat_axis=0, tiled=True)  8.98 us
    ppermute x2, starting transfers between devices, to_column_owner(): return lax.ppermute(v, ('sp', 'x'), pairs)  7.21 us
    ppermute x2, waiting for transfers between devices, shards(): lax.ppermute(glu[TOK - TAPS:], 'sp', [(i, i + 1) for i in range(count - 1)])  6.83 us
  transfers between devices with their start and end apart: 15, of which 10 were waited for; matrix products, arithmetic and copies ran while one was open for 1% of the time, Pallas kernels for 6%

commit v1 on v0

v1 whole, which is shorter than its diff:
```python
import jax
import jax.numpy as jnp
from jax import lax
from jax.experimental import pallas as pl
from jax.experimental.pallas import tpu as pltpu
from jax.sharding import Mesh
from jax.sharding import PartitionSpec as P


C = 1024
LAYERS = 2
NZ, NY, NX = 8, 8, 4
TOK, CH, TAPS, FEAT = 256, 256, 128, 512
PACK = TOK + 16
HALF = TOK // 2
SPAN = HALF + TAPS - 8
BF = jnp.bfloat16
F32 = jnp.float32
INTERPRET = False


def at(z, y, c):
    return (z * NY + y) * 2 + c


ALONG_Y = [[at(z, y, 0) for y in range(NY)] for z in range(NZ)]
ALONG_Z = [[at(z, y, 1) for z in range(NZ)] for y in range(NY)]
ALONG_Y1 = [[at(z, y, 1) for y in range(NY)] for z in range(NZ)]
ALONG_Z0 = [[at(z, y, 0) for z in range(NZ)] for y in range(NY)]


def to_group(block, groups):
    n = len(groups[0])
    copies = jnp.broadcast_to(block, (n, *block.shape))
    return lax.all_to_all(
        copies, "sp", split_axis=0, concat_axis=0, tiled=True, axis_index_groups=groups
    )


def lines(block):
    return to_group(block, ALONG_Y + ALONG_Z)


def plane(once):
    return to_group(once, ALONG_Z0 + ALONG_Y1)


def after(v, earlier):
    return lax.optimization_barrier((v, earlier))[0]


def swap_cores(v):
    count = lax.axis_size("sp")
    return lax.ppermute(v, "sp", [(i, i ^ 1) for i in range(count)])


def to_column_owner(v):
    nb = NZ // NX
    pairs = []
    for z in range(NZ):
        a, b = divmod(z, nb)
        for y in range(NY):
            for c in range(2):
                for x in range(NX):
                    place = (x * nb + b, y) if c == 0 else (y, x * nb + b)
                    pairs.append((at(z, y, c) * NX + x, at(*place, c) * NX + a))
    return lax.ppermute(v, ("sp", "x"), pairs)


def from_all_x(v):
    return [v] + [
        lax.ppermute(v, "x", [(i, (i + step) % NX) for i in range(NX)]) for step in range(1, NX)
    ]


def exchange_x(copies):
    return [lax.all_to_all(copies, "x", split_axis=0, concat_axis=0, tiled=True)]


def part_of(refs, k):
    if len(refs) == 1:
        return refs[0].at[k], k
    return refs[k], (lax.axis_index("x") + NX - k) % NX


def core_here():
    return lax.axis_index("sp") % 2


def norm_kernel(layer, n, *refs):
    parts, (gain, xs, scale) = refs[:n], refs[n:]

    def squares(i, _):
        rows = pl.ds(pl.multiple_of(i * 16, 16), 16)
        total = jnp.zeros((16, 128), F32)
        for k in range(NX):
            v = part_of(parts, k)[0][rows, :].astype(F32)
            sq = v * v
            for q in range(FEAT // 128):
                total += sq[:, q * 128 : (q + 1) * 128]
        scale[rows, :] = total
        return 0

    lax.fori_loop(0, TOK // 16, squares, 0, unroll=2)
    mean = jnp.sum(scale[...], axis=1, keepdims=True) / (NX * FEAT)
    scale[...] = jnp.broadcast_to(lax.rsqrt(mean + 1e-06), (TOK, 128))

    def apply(i, _):
        rows = pl.ds(pl.multiple_of(i * 16, 16), 16)
        factor = jnp.concatenate([scale[rows, :]] * (FEAT // 128), axis=1)
        for k in range(NX):
            ref, owner = part_of(parts, k)
            xs[owner, rows, :] = (ref[rows, :].astype(F32) * factor * gain[layer * NX + owner]).astype(BF)
        return 0

    lax.fori_loop(0, TOK // 16, apply, 0, unroll=2)


def mix_kernel(xs, mine, other, glu, vs, gs):
    def fill(zy, yz):
        for z in range(NZ):
            for c, w in enumerate((zy.at[z], yz.at[:, z])):
                vs[z, :, c] = w[:, :16, :]
                gs[z, :, c] = w[:, 16:32, :]

    @pl.when(core_here() == 0)
    def _():
        fill(mine, other)

    @pl.when(core_here() == 1)
    def _():
        fill(other, mine)

    value = jnp.zeros((TOK, CH), F32)
    gate = jnp.zeros((TOK, CH), F32)
    for k in range(NX):
        planes = slice(2 * k, 2 * k + 2)
        value += jnp.dot(xs[k], vs[planes].reshape(FEAT, CH), preferred_element_type=F32)
        gate += jnp.dot(xs[k], gs[planes].reshape(FEAT, CH), preferred_element_type=F32)
    glu[...] = (value * jax.nn.sigmoid(gate)).astype(BF)


def split_three(v):
    hi = v.astype(BF).astype(F32)
    mid = (v - hi).astype(BF).astype(F32)
    return [hi, mid, v - hi - mid]


def conv_half(layer, ext, taps, conv, shifted, base):
    for b in range(8):
        shifted[b] = ext[1 + b : 1 + b + SPAN, :]
    for lane in range(0, CH, 128):

        def step(a, acc):
            start = pl.multiple_of(a * 8, 8)
            tap = taps[layer, pl.ds(start, 8), lane : lane + 128]
            for b in range(8):
                acc += shifted[b, pl.ds(start, HALF), lane : lane + 128] * tap[b : b + 1]
            return acc

        acc = lax.fori_loop(0, TAPS // 8, step, jnp.zeros((HALF, 128), F32))
        conv[base : base + HALF, lane : lane + 128] = acc


def late_kernel(layer, glu, taps, conv, ext, shifted):
    ext[...] = glu[...].astype(F32)
    conv_half(layer, ext, taps, conv, shifted, 0)


def conv_kernel(layer, copies, before, glu, late, taps, gain, out, ext, shifted, conv):
    ext[:TAPS, :] = before[...].astype(F32)
    ext[TAPS:, :] = glu[:HALF, :].astype(F32)
    conv_half(layer, ext, taps, conv, shifted, 0)
    conv[HALF:, :] = late[...]
    ones = jnp.full((8, CH), 1.0 / CH, F32)
    means = lax.dot_general(
        ones, conv[...], (((1,), (1,)), ((), ())), precision=lax.Precision.HIGHEST,
        preferred_element_type=F32,
    )[:1]
    extra = split_three(means) + split_three(gain[layer : layer + 1, :])
    extra = jnp.concatenate(extra + [jnp.zeros((10, CH), F32)], axis=0).astype(BF)
    v = conv[...]
    d = (v - jnp.mean(v, axis=1, keepdims=True)).astype(BF)
    for k in range(copies):
        out[k, TOK:, :] = extra
        out[k, :TOK, :] = d


def arrange_kernel(mine, other, wt):
    def fill(zy, yz):
        for k in range(NX):
            for c, w in enumerate((zy, yz)):
                wt[k, :, :, c] = w[2 * k : 2 * k + 2, :, 32:, :]

    @pl.when(core_here() == 0)
    def _():
        fill(mine, other)

    @pl.when(core_here() == 1)
    def _():
        fill(other, mine)


def out_kernel(n, copies, *refs):
    parts, rest = refs[:n], refs[n:]
    x, wt, out, means, scale, acts = rest
    pick = (lax.broadcasted_iota(jnp.int32, (16, 128), 0) < 3).astype(BF)
    total = jnp.zeros((TOK, 128), F32)
    for k in range(NX):
        m = lax.dot_general(
            part_of(parts, k)[0][TOK:, :], pick, (((0,), (0,)), ((), ())),
            preferred_element_type=F32,
        )
        means[k] = m
        total += m
    for k in range(NX):
        means[k] = means[k] - total / NX

    def shifted_part(k, rows):
        ref, owner = part_of(parts, k)
        v = ref[rows, :].astype(F32)
        shift = means[k, rows, :]
        return jnp.concatenate([v[:, :128] + shift, v[:, 128:] + shift], axis=1), owner

    def squares(i, _):
        rows = pl.ds(pl.multiple_of(i * 16, 16), 16)
        square = jnp.zeros((16, 128), F32)
        for k in range(NX):
            v, _ = shifted_part(k, rows)
            sq = v * v
            square += sq[:, :128] + sq[:, 128:]
        scale[rows, :] = square
        return 0

    lax.fori_loop(0, TOK // 16, squares, 0, unroll=2)
    spread = jnp.sum(scale[...], axis=1, keepdims=True) / C
    scale[...] = jnp.broadcast_to(lax.rsqrt(spread + 1e-05), (TOK, 128))
    gains = []
    for k in range(NX):
        tail = part_of(parts, k)[0][TOK:, :].astype(F32)
        gains.append(tail[3:4] + tail[4:5] + tail[5:6])

    def activate(i, _):
        rows = pl.ds(pl.multiple_of(i * 16, 16), 16)
        factor = jnp.concatenate([scale[rows, :]] * 2, axis=1)
        for k in range(NX):
            v, owner = shifted_part(k, rows)
            u = v * factor * gains[k]
            acts[owner, rows, :] = (u / (1.0 + jnp.exp(-u))).astype(BF)
        return 0

    lax.fori_loop(0, TOK // 16, activate, 0, unroll=2)
    branch = jnp.zeros((TOK, FEAT), F32)
    for k in range(NX):
        branch += lax.dot_general(
            acts[k], wt[k].reshape(FEAT, CH), (((1,), (1,)), ((), ())),
            preferred_element_type=F32,
        )
    new = (x[...].astype(F32) + branch).astype(BF)
    for k in range(copies):
        out[k] = new


def call(body, out, ins, scratch, flops):
    return pl.pallas_call(
        body,
        out_shape=out,
        in_specs=[pl.BlockSpec(memory_space=pltpu.VMEM)] * len(ins),
        out_specs=pl.BlockSpec(memory_space=pltpu.VMEM),
        scratch_shapes=scratch,
        cost_estimate=pl.CostEstimate(flops=flops, transcendentals=0, bytes_accessed=1 << 20),
        compiler_params=pltpu.CompilerParams(vmem_limit_bytes=14 << 20),
        interpret=INTERPRET,
    )(*ins)


def normalise(layer, parts, gain):
    def body(*refs):
        norm_kernel(layer, len(parts), *refs)

    return call(
        body,
        jax.ShapeDtypeStruct((NX, TOK, FEAT), BF),
        [*parts, gain],
        [pltpu.VMEM((TOK, 128), F32)],
        8 * NX * TOK * FEAT,
    )


def mix(xs, mine, other):
    return call(
        mix_kernel,
        jax.ShapeDtypeStruct((TOK, CH), BF),
        [xs, mine, other],
        [pltpu.VMEM((NZ, NY, 2, 16, CH), BF), pltpu.VMEM((NZ, NY, 2, 16, CH), BF)],
        4 * NX * TOK * FEAT * CH,
    )


def conv_late(layer, glu, taps):
    def body(*refs):
        late_kernel(layer, *refs)

    return call(
        body,
        jax.ShapeDtypeStruct((HALF, CH), F32),
        [glu, taps],
        [pltpu.VMEM((TOK, CH), F32), pltpu.VMEM((8, SPAN, CH), F32)],
        2 * HALF * CH * TAPS,
    )


def convolve(layer, copies, before, glu, late, taps, gain):
    def body(*refs):
        conv_kernel(layer, copies, *refs)

    return call(
        body,
        jax.ShapeDtypeStruct((copies, PACK, CH), BF),
        [before, glu, late, taps, gain],
        [
            pltpu.VMEM((TAPS + HALF, CH), F32),
            pltpu.VMEM((8, SPAN, CH), F32),
            pltpu.VMEM((TOK, CH), F32),
        ],
        2 * HALF * CH * TAPS,
    )


def arrange(mine, other):
    return call(
        arrange_kernel, jax.ShapeDtypeStruct((NX, 2, NY, 2, 16, CH), BF), [mine, other], [], 1 << 26
    )


def project(copies, parts, x, wt):
    def body(*refs):
        out_kernel(len(parts), copies, *refs)

    return call(
        body,
        jax.ShapeDtypeStruct((copies, TOK, FEAT), BF),
        [*parts, x, wt],
        [
            pltpu.VMEM((NX, TOK, 128), F32),
            pltpu.VMEM((TOK, 128), F32),
            pltpu.VMEM((NX, TOK, CH), BF),
        ],
        2 * NX * TOK * CH * FEAT,
    )


def shards(stream, norm_gain, w_value, w_gate, conv_taps, channel_gain, w_out):
    gain = norm_gain.reshape(LAYERS * NX, 1, FEAT)
    out_t = to_column_owner(jnp.swapaxes(w_out, 1, 2))
    blocks = jnp.concatenate([w_value, w_gate, out_t], axis=1)

    x = stream
    count = lax.axis_size("sp")
    once = lines(blocks)
    parts = from_all_x(after(x, blocks))
    gathered = plane(once[:, 0])
    for layer in range(LAYERS):
        last = layer + 1 == LAYERS
        mine = gathered
        other = swap_cores(mine)
        normed = normalise(layer, parts, gain)
        glu = mix(normed, mine, other)
        before = lax.ppermute(glu[TOK - TAPS :], "sp", [(i, i + 1) for i in range(count - 1)])
        late = conv_late(layer, glu, conv_taps)
        if not last:
            gathered = plane(after(once[:, layer + 1], before))
        packed = convolve(layer, NX if last else 1, before, glu, late, conv_taps, channel_gain)
        parts = exchange_x(packed) if last else from_all_x(packed[0])
        wt = arrange(after(mine, packed), other)
        new = project(1 if last else NX, parts, x, wt)
        x = new[0]
        if not last:
            parts = exchange_x(new)
    return x


def solution(mesh):
    flat = Mesh(mesh.devices, ("sp", "x"))
    in_specs = (
        P("sp", "x"),
        P(),
        P(None, "sp", "x"),
        P(None, "sp", "x"),
        P(None, None, "x"),
        P(None, "x"),
        P(None, "x", "sp"),
    )

    return jax.shard_map(shards, mesh=flat, in_specs=in_specs, out_specs=P("sp", "x"), check_vma=False)
```

time: 211 us -> 197 us (0.934)
  the two profiles are of different devices: /device:TPU:16 before, /device:TPU:64 now
where the time goes in v1:
time: 197 us
  blocking collectives  107 us (54%)
  starting transfers between devices  33 us (17%)
  waiting for transfers between devices  32.4 us (16%)
  Pallas kernels  16.2 us (8%)
  local copies, waits for them, and re-layouts  8.07 us (4%)
    all_to_all x3, blocking collectives, to_group(): lax.all_to_all(copies, 'sp', split_axis=0, concat_axis=0, tiled=True, axi...  88.6 us
    ppermute x6, starting transfers between devices, from_all_x(): lax.ppermute(v, 'x', [(i, (i + step) % NX) for i in range(NX)])  19.7 us
    all_to_all x1, blocking collectives, exchange_x(): lax.all_to_all(copies, 'x', split_axis=0, concat_axis=0, tiled=True)  18 us
    pallas_call x12, Pallas kernels, call(): pl.pallas_call(body, out_shape=out, in_specs=[pl.BlockSpec(memory_space=p...  16.2 us
    ppermute x6, waiting for transfers between devices, from_all_x(): lax.ppermute(v, 'x', [(i, (i + step) % NX) for i in range(NX)])  16.2 us
    ppermute x2, waiting for transfers between devices, shards(): lax.ppermute(glu[TOK - TAPS:], 'sp', [(i, i + 1) for i in range(count - 1)])  9.95 us
    all_to_all x1, waiting for transfers between devices, exchange_x(): lax.all_to_all(copies, 'x', split_axis=0, concat_axis=0, tiled=True)  6.22 us
    unnamed x28, local copies, waits for them, and re-layouts  6.08 us
  transfers between devices with their start and end apart: 12, of which 8 were waited for; matrix products, arithmetic and copies ran while one was open for 1% of the time, Pallas kernels for 5%

profile of v1, /device:TPU:64, one launch (start us, length us, event | category | flops | bytes accessed | tf_op | source)
XLA Modules:
  0.0 196.6 jit_solution(11803071173352881187)
XLA Ops:
  2.8 18.8 %all_to_all.25 = bf16[8,2,48,256]{3,2,1,0:T(8,128)(2,1)S(1)} all-to-all(bf16[8,2,48,256]{3,2,1,0:T(8,128)(2,1)S(1)} %broadcast_in_dim.9), channel_id=1, replica_groups={{0,8,16,24,32,40,48,56},{64,72,80,88,96,104,112,120},{128,136,144,152,1..., dimensions={0} | all-to-all | bytes 786432 | tf_op jit(solution)/shard_map/all_to_all | solution.py:35
  22.5 42.3 %all_to_all.26.mine = bf16[8,8,48,256]{3,2,1,0:T(8,128)(2,1)S(1)} all-to-all(bf16[8,8,48,256]{3,2,1,0:T(8,128)(2,1)S(1)} %broadcast_in_dim.10), channel_id=1, replica_groups={{0,64,128,192,256,320,384,448},{8,72,136,200,264,328,392,456},{16,80,14..., dimensions={0} | all-to-all | bytes 3145728 | tf_op jit(solution)/shard_map/all_to_all | solution.py:35
  64.8 1.9 collective-permute-start.4
  66.7 1.9 collective-permute-start.3
  68.6 5.5 %collective-permute-start.2 = (bf16[256,512]{1,0:T(8,128)(2,1)S(1)}, bf16[256,512]{1,0:T(8,128)(2,1)}, u32[]{:S(2)}, u32[]{:S(2)}) collective-permute-start(bf16[256,512]{1,0:T(8,128)(2,1)S(1)} %copy-done.9), channel_id=1, source_target_pairs={{0,2},{1,3},{2,0},{3,1},{4,6},{5,7},{6,4},{7,5},{8,10},{9,11},{10,... | collective-permute-start | bytes 786440 | tf_op jit(solution)/shard_map/ppermute | solution.py:72
  74.1 1.9 collective-permute-start.1
  77.9 3.5 %collective-permute-done.2.refs_2_ = bf16[256,512]{1,0:T(8,128)(2,1)} collective-permute-done((bf16[256,512]{1,0:T(8,128)(2,1)S(1)}, bf16[256,512]{1,0:T(8,128)(2,1)}, u32[]{:S(2)}, u32[]{:S(2)}) %collective-permute-start.2) | collective-permute-done | bytes 262176 | tf_op jit(solution)/shard_map/ppermute | solution.py:72
  81.4 5.1 %collective-permute-done.1.refs_1_ = bf16[256,512]{1,0:T(8,128)(2,1)} collective-permute-done((bf16[256,512]{1,0:T(8,128)(2,1)S(1)}, bf16[256,512]{1,0:T(8,128)(2,1)}, u32[]{:S(2)}, u32[]{:S(2)}) %collective-permute-start.1) | collective-permute-done | bytes 262176 | tf_op jit(solution)/shard_map/ppermute | solution.py:72
  89.5 1.9 collective-permute-start.5
  91.4 5.8 %collective-permute-done.5.refs_0_ = bf16[128,256]{1,0:T(8,128)(2,1)S(1)} collective-permute-done((bf16[128,256]{1,0:T(8,128)(2,1)S(1)}, bf16[128,256]{1,0:T(8,128)(2,1)S(1)}, u32[]{:S(2)}, u32[]{:S(2)}) %collective-permute-start.5) | collective-permute-done | bytes 65568 | tf_op jit(solution)/shard_map/ppermute | solution.py:369
  97.4 27.5 %all_to_all.27.mine = bf16[8,8,48,256]{3,2,1,0:T(8,128)(2,1)S(1)} all-to-all(bf16[8,8,48,256]{3,2,1,0:T(8,128)(2,1)S(1)} %broadcast_in_dim.11), channel_id=1, replica_groups={{0,64,128,192,256,320,384,448},{8,72,136,200,264,328,392,456},{16,80,14..., dimensions={0} | all-to-all | bytes 3145728 | tf_op jit(solution)/shard_map/all_to_all | solution.py:35
  124.9 1.9 collective-permute-start.9
  128.4 1.9 shard_map.76
  130.3 2.5 %collective-permute-start.8 = (bf16[272,256]{1,0:T(8,128)(2,1)S(1)}, bf16[272,256]{1,0:T(8,128)(2,1)S(1)}, u32[]{:S(2)}, u32[]{:S(2)}) collective-permute-start(bf16[272,256]{1,0:T(8,128)(2,1)S(1)} %bitcast.9), channel_id=1, source_target_pairs={{0,3},{1,0},{2,1},{3,2},{4,7},{5,4},{6,5},{7,6},{8,11},{9,8},{10,9... | collective-permute-start | bytes 417800 | tf_op jit(solution)/shard_map/ppermute | solution.py:72
  132.8 5.2 %collective-permute-start.7 = (bf16[272,256]{1,0:T(8,128)(2,1)S(1)}, bf16[272,256]{1,0:T(8,128)(2,1)S(1)}, u32[]{:S(2)}, u32[]{:S(2)}) collective-permute-start(bf16[272,256]{1,0:T(8,128)(2,1)S(1)} %bitcast.10), channel_id=1, source_target_pairs={{0,2},{1,3},{2,0},{3,1},{4,6},{5,7},{6,4},{7,5},{8,10},{9,11},{10,... | collective-permute-start | bytes 417800 | tf_op jit(solution)/shard_map/ppermute | solution.py:72
  138.0 2.7 %collective-permute-start.6 = (bf16[272,256]{1,0:T(8,128)(2,1)S(1)}, bf16[272,256]{1,0:T(8,128)(2,1)S(1)}, u32[]{:S(2)}, u32[]{:S(2)}) collective-permute-start(bf16[272,256]{1,0:T(8,128)(2,1)S(1)} %bitcast.11), channel_id=1, source_target_pairs={{0,1},{1,2},{2,3},{3,0},{4,5},{5,6},{6,7},{7,4},{8,9},{9,10},{10,1... | collective-permute-start | bytes 417800 | tf_op jit(solution)/shard_map/ppermute | solution.py:72
  142.0 4.6 %collective-permute-done.6.refs_1_ = bf16[272,256]{1,0:T(8,128)(2,1)S(1)} collective-permute-done((bf16[272,256]{1,0:T(8,128)(2,1)S(1)}, bf16[272,256]{1,0:T(8,128)(2,1)S(1)}, u32[]{:S(2)}, u32[]{:S(2)}) %collective-permute-start.6) | collective-permute-done | bytes 139296 | tf_op jit(solution)/shard_map/ppermute | solution.py:72
  149.1 18.0 %all_to_all.28.refs_0_ = bf16[4,256,512]{2,1,0:T(8,128)(2,1)S(1)} all-to-all(bf16[4,256,512]{2,1,0:T(8,128)(2,1)S(1)} %shard_map.78), channel_id=1, replica_groups=mesh['sp'=128,'tp'=4] {'tp'}, dimensions={0} | all-to-all | bytes 2097152 | tf_op jit(solution)/shard_map/all_to_all | solution.py:77
  169.0 2.0 %collective-permute-start.10 = (bf16[128,256]{1,0:T(8,128)(2,1)S(1)}, bf16[128,256]{1,0:T(8,128)(2,1)S(1)}, u32[]{:S(2)}, u32[]{:S(2)}) collective-permute-start(bf16[128,256]{1,0:T(8,128)(2,1)S(1)} %slice.23), channel_id=1, source_target_pairs={{0,4},{4,8},{8,12},{12,16},{16,20},{20,24},{24,28},{28,32},{32,36}... | collective-permute-start | bytes 196616 | tf_op jit(solution)/shard_map/ppermute | solution.py:369
  172.7 4.2 %collective-permute-done.10.refs_0_ = bf16[128,256]{1,0:T(8,128)(2,1)S(1)} collective-permute-done((bf16[128,256]{1,0:T(8,128)(2,1)S(1)}, bf16[128,256]{1,0:T(8,128)(2,1)S(1)}, u32[]{:S(2)}, u32[]{:S(2)}) %collective-permute-start.10) | collective-permute-done | bytes 65568 | tf_op jit(solution)/shard_map/ppermute | solution.py:369
  176.9 1.9 shard_map.82
  179.6 4.2 %all-to-all-start.4 = ((bf16[4,272,256]{2,1,0:T(8,128)(2,1)}), bf16[4,272,256]{2,1,0:T(8,128)(2,1)}, u32[]{:S(2)}, u32[]{:S(2)}) async-start(bf16[4,272,256]{2,1,0:T(8,128)(2,1)} %copy-done.8), calls=%async_computation.4 | async-start | bytes 1114112 | tf_op jit(solution)/shard_map/all_to_all | solution.py:77
  185.9 6.2 %all-to-all-done.4.refs_0_ = bf16[4,272,256]{2,1,0:T(8,128)(2,1)} async-done(((bf16[4,272,256]{2,1,0:T(8,128)(2,1)}), bf16[4,272,256]{2,1,0:T(8,128)(2,1)}, u32[]{:S(2)}, u32[]{:S(2)}) %all-to-all-start.4) | async-done | bytes 557088 | tf_op jit(solution)/shard_map/all_to_all | solution.py:77
  193.3 3.3 %shard_map.84 = bf16[1,256,512]{2,1,0:T(8,128)(2,1)} custom-call(bf16[4,272,256]{2,1,0:T(8,128)(2,1)} %all-to-all-done.4.refs_0_, bf16[256,512]{1,0:T(8,128)(2,1)S(1)} %slice_bitcast_fusion.refs_1_, bf16[4,2,8,2,16,256]{5,4,3,2,1,0:T(8,128)(2,1)S(1)} %copy-done.6), custom_call_target="tpu_custom_call" | custom-call | flops 268435456 | bytes 1048576 | tf_op jit(solution)/shard_map/pallas_call | solution.py:265
  (53 shorter events, 21.5 us)
Async XLA Ops:
  0.0 2.8 %collective-permute-start = (bf16[2,16,256]{2,1,0:T(8,128)(2,1)}, bf16[2,16,256]{2,1,0:T(8,128)(2,1)S(1)}, u32[]{:S(2)}, u32[]{:S(2)}) collective-permute-start(bf16[2,16,256]{2,1,0:T(8,128)(2,1)} %bitcast.13), channel_id=1, source_target_pairs={{0,0},{1,128},{2,256},{3,384},{4,4},{5,20},{6,36},{7,52},{8,8},{9,... | collective-permute-start | bytes 49160 | tf_op jit(solution)/shard_map/ppermute | solution.py:67
  22.5 44.2 %copy-start.9 = (bf16[256,512]{1,0:T(8,128)(2,1)S(1)}, bf16[256,512]{1,0:T(8,128)(2,1)}, u32[]{:S(2)}) copy-start(bf16[256,512]{1,0:T(8,128)(2,1)} %refs_4_.4) | copy-start | bytes 786436
  22.5 53.6 %copy-start.12 = (f32[2,2048]{1,0:T(2,128)S(1)}, f32[2,2048]{1,0:T(2,128)}, u32[]{:S(2)}) copy-start(f32[2,2048]{1,0:T(2,128)} %param.8) | copy-start | bytes 49156
  64.8 23.6 %collective-permute-start.4 = (bf16[8,8,48,256]{3,2,1,0:T(8,128)(2,1)S(1)}, bf16[8,8,48,256]{3,2,1,0:T(8,128)(2,1)S(1)}, u32[]{:S(2)}, u32[]{:S(2)}) collective-permute-start(bf16[8,8,48,256]{3,2,1,0:T(8,128)(2,1)S(1)} %all_to_all.26.mine), channel_id=1, source_target_pairs={{0,4},{4,0},{8,12},{12,8},{16,20},{20,16},{24,28},{28,24},{32,36},... | collective-permute-start | bytes 4718600 | tf_op jit(solution)/shard_map/ppermute | solution.py:54
  66.7 11.2 %collective-permute-start.3 = (bf16[256,512]{1,0:T(8,128)(2,1)S(1)}, bf16[256,512]{1,0:T(8,128)(2,1)}, u32[]{:S(2)}, u32[]{:S(2)}) collective-permute-start(bf16[256,512]{1,0:T(8,128)(2,1)S(1)} %copy-done.9), channel_id=1, source_target_pairs={{0,3},{1,0},{2,1},{3,2},{4,7},{5,4},{6,5},{7,6},{8,11},{9,8},{10,9... | collective-permute-start | bytes 786440 | tf_op jit(solution)/shard_map/ppermute | solution.py:72
  68.6 12.7 %collective-permute-start.2 = (bf16[256,512]{1,0:T(8,128)(2,1)S(1)}, bf16[256,512]{1,0:T(8,128)(2,1)}, u32[]{:S(2)}, u32[]{:S(2)}) collective-permute-start(bf16[256,512]{1,0:T(8,128)(2,1)S(1)} %copy-done.9), channel_id=1, source_target_pairs={{0,2},{1,3},{2,0},{3,1},{4,6},{5,7},{6,4},{7,5},{8,10},{9,11},{10,... | collective-permute-start | bytes 786440 | tf_op jit(solution)/shard_map/ppermute | solution.py:72
  74.1 12.4 %collective-permute-start.1 = (bf16[256,512]{1,0:T(8,128)(2,1)S(1)}, bf16[256,512]{1,0:T(8,128)(2,1)}, u32[]{:S(2)}, u32[]{:S(2)}) collective-permute-start(bf16[256,512]{1,0:T(8,128)(2,1)S(1)} %copy-done.9), channel_id=1, source_target_pairs={{0,1},{1,2},{2,3},{3,0},{4,5},{5,6},{6,7},{7,4},{8,9},{9,10},{10,1... | collective-permute-start | bytes 786440 | tf_op jit(solution)/shard_map/ppermute | solution.py:72
  88.3 8.9 %copy-start.11 = (bf16[8,48,256]{2,1,0:T(8,128)(2,1)S(1)}, bf16[8,48,256]{2,1,0:T(8,128)(2,1)}, u32[]{:S(2)}) copy-start(bf16[8,48,256]{2,1,0:T(8,128)(2,1)} %get-tuple-element.11) | copy-start | bytes 589828
  88.3 1.2 copy-start
  89.5 7.7 %collective-permute-start.5 = (bf16[128,256]{1,0:T(8,128)(2,1)S(1)}, bf16[128,256]{1,0:T(8,128)(2,1)S(1)}, u32[]{:S(2)}, u32[]{:S(2)}) collective-permute-start(bf16[128,256]{1,0:T(8,128)(2,1)S(1)} %slice.21), channel_id=1, source_target_pairs={{0,4},{4,8},{8,12},{12,16},{16,20},{20,24},{24,28},{28,32},{32,36}... | collective-permute-start | bytes 196616 | tf_op jit(solution)/shard_map/ppermute | solution.py:369
  97.3 29.5 %copy-start.7 = (f32[2,128,256]{2,1,0:T(8,128)S(1)}, f32[2,128,256]{2,1,0:T(8,128)}, u32[]{:S(2)}) copy-start(f32[2,128,256]{2,1,0:T(8,128)} %refs_3_.3) | copy-start | bytes 786436
  97.3 31.0 %copy-start.10 = (f32[2,256]{1,0:T(2,128)S(1)}, f32[2,256]{1,0:T(2,128)}, u32[]{:S(2)}) copy-start(f32[2,256]{1,0:T(2,128)} %refs_4_.5) | copy-start | bytes 6148
  97.4 43.4 %copy-start.1 = (bf16[8,8,48,256]{3,2,1,0:T(8,128)(2,1)S(1)}, bf16[8,8,48,256]{3,2,1,0:T(8,128)(2,1)}, u32[]{:S(2)}) copy-start(bf16[8,8,48,256]{3,2,1,0:T(8,128)(2,1)} %copy-done) | copy-start | bytes 4718596
  124.9 43.0 %collective-permute-start.9 = (bf16[8,8,48,256]{3,2,1,0:T(8,128)(2,1)S(1)}, bf16[8,8,48,256]{3,2,1,0:T(8,128)(2,1)S(1)}, u32[]{:S(2)}, u32[]{:S(2)}) collective-permute-start(bf16[8,8,48,256]{3,2,1,0:T(8,128)(2,1)S(1)} %all_to_all.27.mine), channel_id=1, source_target_pairs={{0,4},{4,0},{8,12},{12,8},{16,20},{20,16},{24,28},{28,24},{32,36},... | collective-permute-start | bytes 4718600 | tf_op jit(solution)/shard_map/ppermute | solution.py:54
  130.3 10.5 %collective-permute-start.8 = (bf16[272,256]{1,0:T(8,128)(2,1)S(1)}, bf16[272,256]{1,0:T(8,128)(2,1)S(1)}, u32[]{:S(2)}, u32[]{:S(2)}) collective-permute-start(bf16[272,256]{1,0:T(8,128)(2,1)S(1)} %bitcast.9), channel_id=1, source_target_pairs={{0,3},{1,0},{2,1},{3,2},{4,7},{5,4},{6,5},{7,6},{8,11},{9,8},{10,9... | collective-permute-start | bytes 417800 | tf_op jit(solution)/shard_map/ppermute | solution.py:72
  132.8 9.2 %collective-permute-start.7 = (bf16[272,256]{1,0:T(8,128)(2,1)S(1)}, bf16[272,256]{1,0:T(8,128)(2,1)S(1)}, u32[]{:S(2)}, u32[]{:S(2)}) collective-permute-start(bf16[272,256]{1,0:T(8,128)(2,1)S(1)} %bitcast.10), channel_id=1, source_target_pairs={{0,2},{1,3},{2,0},{3,1},{4,6},{5,7},{6,4},{7,5},{8,10},{9,11},{10,... | collective-permute-start | bytes 417800 | tf_op jit(solution)/shard_map/ppermute | solution.py:72
  138.0 8.6 %collective-permute-start.6 = (bf16[272,256]{1,0:T(8,128)(2,1)S(1)}, bf16[272,256]{1,0:T(8,128)(2,1)S(1)}, u32[]{:S(2)}, u32[]{:S(2)}) collective-permute-start(bf16[272,256]{1,0:T(8,128)(2,1)S(1)} %bitcast.11), channel_id=1, source_target_pairs={{0,1},{1,2},{2,3},{3,0},{4,5},{5,6},{6,7},{7,4},{8,9},{9,10},{10,1... | collective-permute-start | bytes 417800 | tf_op jit(solution)/shard_map/ppermute | solution.py:72
  148.2 1.0 copy-start.4
  167.8 1.2 copy-start.2
  169.0 15.7 %copy-start.3 = (bf16[8,8,48,256]{3,2,1,0:T(8,128)(2,1)S(1)}, bf16[8,8,48,256]{3,2,1,0:T(8,128)(2,1)}, u32[]{:S(2)}) copy-start(bf16[8,8,48,256]{3,2,1,0:T(8,128)(2,1)} %copy-done.2) | copy-start | bytes 4718596
  169.0 7.8 %collective-permute-start.10 = (bf16[128,256]{1,0:T(8,128)(2,1)S(1)}, bf16[128,256]{1,0:T(8,128)(2,1)S(1)}, u32[]{:S(2)}, u32[]{:S(2)}) collective-permute-start(bf16[128,256]{1,0:T(8,128)(2,1)S(1)} %slice.23), channel_id=1, source_target_pairs={{0,4},{4,8},{8,12},{12,16},{16,20},{20,24},{24,28},{28,32},{32,36}... | collective-permute-start | bytes 196616 | tf_op jit(solution)/shard_map/ppermute | solution.py:369
  179.6 12.5 %all-to-all-start.4 = ((bf16[4,272,256]{2,1,0:T(8,128)(2,1)}), bf16[4,272,256]{2,1,0:T(8,128)(2,1)}, u32[]{:S(2)}, u32[]{:S(2)}) async-start(bf16[4,272,256]{2,1,0:T(8,128)(2,1)} %copy-done.8), calls=%async_computation.4 | async-start | bytes 1114112 | tf_op jit(solution)/shard_map/all_to_all | solution.py:77
  184.9 1.0 copy-start.5
  192.1 1.2 copy-start.6
  (1 other events, 0.8 us)

commit v2 on v1

--- a/solution.py
+++ b/solution.py
@@ -41,8 +41,11 @@
     return to_group(block, ALONG_Y + ALONG_Z)
 
 
-def plane(once):
-    return to_group(once, ALONG_Z0 + ALONG_Y1)
+def plane(copies):
+    return lax.all_to_all(
+        copies, "sp", split_axis=0, concat_axis=0, tiled=True,
+        axis_index_groups=ALONG_Z0 + ALONG_Y1,
+    )
 
 
 def after(v, earlier):
@@ -73,10 +76,6 @@
     ]
 
 
-def exchange_x(copies):
-    return [lax.all_to_all(copies, "x", split_axis=0, concat_axis=0, tiled=True)]
-
-
 def part_of(refs, k):
     if len(refs) == 1:
         return refs[0].at[k], k
@@ -167,7 +166,15 @@
     conv_half(layer, ext, taps, conv, shifted, 0)
 
 
-def conv_kernel(layer, copies, before, glu, late, taps, gain, out, ext, shifted, conv):
+def spread_kernel(layer, once, out, sems):
+    copies = [pltpu.make_async_copy(once.at[:, layer], out.at[k], sems.at[k]) for k in range(NZ)]
+    for c in copies:
+        c.start()
+    for c in copies:
+        c.wait()
+
+
+def conv_kernel(layer, before, glu, late, taps, gain, out, ext, shifted, conv):
     ext[:TAPS, :] = before[...].astype(F32)
     ext[TAPS:, :] = glu[:HALF, :].astype(F32)
     conv_half(layer, ext, taps, conv, shifted, 0)
@@ -181,9 +188,8 @@
     extra = jnp.concatenate(extra + [jnp.zeros((10, CH), F32)], axis=0).astype(BF)
     v = conv[...]
     d = (v - jnp.mean(v, axis=1, keepdims=True)).astype(BF)
-    for k in range(copies):
-        out[k, TOK:, :] = extra
-        out[k, :TOK, :] = d
+    out[TOK:, :] = extra
+    out[:TOK, :] = d
 
 
 def arrange_kernel(mine, other, wt):
@@ -201,7 +207,7 @@
         fill(other, mine)
 
 
-def out_kernel(n, copies, *refs):
+def out_kernel(n, *refs):
     parts, rest = refs[:n], refs[n:]
     x, wt, out, means, scale, acts = rest
     pick = (lax.broadcasted_iota(jnp.int32, (16, 128), 0) < 3).astype(BF)
@@ -256,17 +262,15 @@
             acts[k], wt[k].reshape(FEAT, CH), (((1,), (1,)), ((), ())),
             preferred_element_type=F32,
         )
-    new = (x[...].astype(F32) + branch).astype(BF)
-    for k in range(copies):
-        out[k] = new
-
-
-def call(body, out, ins, scratch, flops):
+    out[...] = (x[...].astype(F32) + branch).astype(BF)
+
+
+def call(body, out, ins, scratch, flops, place=pltpu.VMEM):
     return pl.pallas_call(
         body,
         out_shape=out,
         in_specs=[pl.BlockSpec(memory_space=pltpu.VMEM)] * len(ins),
-        out_specs=pl.BlockSpec(memory_space=pltpu.VMEM),
+        out_specs=pl.BlockSpec(memory_space=place),
         scratch_shapes=scratch,
         cost_estimate=pl.CostEstimate(flops=flops, transcendentals=0, bytes_accessed=1 << 20),
         compiler_params=pltpu.CompilerParams(vmem_limit_bytes=14 << 20),
@@ -310,13 +314,13 @@
     )
 
 
-def convolve(layer, copies, before, glu, late, taps, gain):
+def convolve(layer, before, glu, late, taps, gain):
     def body(*refs):
-        conv_kernel(layer, copies, *refs)
-
-    return call(
-        body,
-        jax.ShapeDtypeStruct((copies, PACK, CH), BF),
+        conv_kernel(layer, *refs)
+
+    return call(
+        body,
+        jax.ShapeDtypeStruct((PACK, CH), BF),
         [before, glu, late, taps, gain],
         [
             pltpu.VMEM((TAPS + HALF, CH), F32),
@@ -327,19 +331,33 @@
     )
 
 
+def spread(layer, once):
+    def body(*refs):
+        spread_kernel(layer, *refs)
+
+    return call(
+        body,
+        jax.ShapeDtypeStruct((NZ, NZ, 48, CH), BF),
+        [once],
+        [pltpu.SemaphoreType.DMA((NZ,))],
+        1 << 26,
+        pltpu.HBM,
+    )
+
+
 def arrange(mine, other):
     return call(
         arrange_kernel, jax.ShapeDtypeStruct((NX, 2, NY, 2, 16, CH), BF), [mine, other], [], 1 << 26
     )
 
 
-def project(copies, parts, x, wt):
+def project(parts, x, wt):
     def body(*refs):
-        out_kernel(len(parts), copies, *refs)
-
-    return call(
-        body,
-        jax.ShapeDtypeStruct((copies, TOK, FEAT), BF),
+        out_kernel(len(parts), *refs)
+
+    return call(
+        body,
+        jax.ShapeDtypeStruct((TOK, FEAT), BF),
         [*parts, x, wt],
         [
             pltpu.VMEM((NX, TOK, 128), F32),
@@ -359,7 +377,9 @@
     count = lax.axis_size("sp")
     once = lines(blocks)
     parts = from_all_x(after(x, blocks))
-    gathered = plane(once[:, 0])
+    ready = spread(0, once)
+    gathered = plane(ready)
+    ready = spread(1, once)
     for layer in range(LAYERS):
         last = layer + 1 == LAYERS
         mine = gathered
@@ -368,15 +388,14 @@
         glu = mix(normed, mine, other)
         before = lax.ppermute(glu[TOK - TAPS :], "sp", [(i, i + 1) for i in range(count - 1)])
         late = conv_late(layer, glu, conv_taps)
+        packed = convolve(layer, before, glu, late, conv_taps, channel_gain)
+        parts = from_all_x(packed)
         if not last:
-            gathered = plane(after(once[:, layer + 1], before))
-        packed = convolve(layer, NX if last else 1, before, glu, late, conv_taps, channel_gain)
-        parts = exchange_x(packed) if last else from_all_x(packed[0])
+            gathered = plane(after(ready, packed))
         wt = arrange(after(mine, packed), other)
-        new = project(1 if last else NX, parts, x, wt)
-        x = new[0]
+        x = project(parts, x, wt)
         if not last:
-            parts = exchange_x(new)
+            parts = from_all_x(x)
     return x
 
 

time: 197 us -> 194 us (0.985)
  blocking collectives: 107 us -> 88.3 us
  starting transfers between devices: 33 us -> 48.8 us
  local copies, waits for them, and re-layouts: 8.07 us -> 2.24 us
  waiting for transfers between devices: 32.4 us -> 36.3 us
    all_to_all x3 -> x1, blocking collectives: 88.6 us -> 18.8 us  [to_group(): lax.all_to_all(copies, 'sp', split_axis=0, concat_axis=0, tiled=True, axi...]
    all_to_all x1 -> x2, blocking collectives: 18 us -> 69.5 us  [plane(): lax.all_to_all(copies, 'sp', split_axis=0, concat_axis=0, tiled=True, axi...]
    ppermute x6 -> x12, starting transfers between devices: 19.7 us -> 39.7 us  [from_all_x(): lax.ppermute(v, 'x', [(i, (i + step) % NX) for i in range(NX)])]
    ppermute x6 -> x12, waiting for transfers between devices: 16.2 us -> 28.3 us  [from_all_x(): lax.ppermute(v, 'x', [(i, (i + step) % NX) for i in range(NX)])]
    all_to_all x1 -> x0, waiting for transfers between devices: 6.22 us -> none  [exchange_x(): lax.all_to_all(copies, 'x', split_axis=0, concat_axis=0, tiled=True)]
    unnamed x28 -> x6, local copies, waits for them, and re-layouts: 6.08 us -> 1.45 us
    all_to_all x1 -> x0, starting transfers between devices: 4.15 us -> none  [exchange_x(): lax.all_to_all(copies, 'x', split_axis=0, concat_axis=0, tiled=True)]
    pallas_call x12 -> x14, Pallas kernels: 16.2 us -> 16.9 us  [call(): pl.pallas_call(body, out_shape=out, in_specs=[pl.BlockSpec(memory_space=p...]
  transfers between devices with their start and end apart: 12 -> 17, of which waited for: 8 -> 11; matrix products, arithmetic and copies ran while one was open for 1% -> 1% of each run, Pallas kernels for 5% -> 5%
where the time goes in v2:
time: 194 us; the launch traced here: 193 us
  blocking collectives  88.3 us (46%)
  starting transfers between devices  48.8 us (25%)
  waiting for transfers between devices  36.3 us (19%)
  Pallas kernels  16.9 us (9%)
  local copies, waits for them, and re-layouts  2.24 us (1%)
    all_to_all x2, blocking collectives, plane(): lax.all_to_all(copies, 'sp', split_axis=0, concat_axis=0, tiled=True, axi...  69.5 us
    ppermute x12, starting transfers between devices, from_all_x(): lax.ppermute(v, 'x', [(i, (i + step) % NX) for i in range(NX)])  39.7 us
    ppermute x12, waiting for transfers between devices, from_all_x(): lax.ppermute(v, 'x', [(i, (i + step) % NX) for i in range(NX)])  28.3 us
    all_to_all x1, blocking collectives, to_group(): lax.all_to_all(copies, 'sp', split_axis=0, concat_axis=0, tiled=True, axi...  18.8 us
    pallas_call x14, Pallas kernels, call(): pl.pallas_call(body, out_shape=out, in_specs=[pl.BlockSpec(memory_space=p...  16.9 us
    ppermute x2, waiting for transfers between devices, shards(): lax.ppermute(glu[TOK - TAPS:], 'sp', [(i, i + 1) for i in range(count - 1)])  8 us
    ppermute x2, starting transfers between devices, shards(): lax.ppermute(glu[TOK - TAPS:], 'sp', [(i, i + 1) for i in range(count - 1)])  3.97 us
  transfers between devices with their start and end apart: 17, of which 11 were waited for; matrix products, arithmetic and copies ran while one was open for 1% of the time, Pallas kernels for 5%

profile of v2, /device:TPU:64, one launch (start us, length us, event | category | flops | bytes accessed | tf_op | source)
XLA Modules:
  0.0 192.9 jit_solution(5192653294987005523)
XLA Ops:
  2.8 18.8 %all_to_all.15.refs_0_ = bf16[8,2,48,256]{3,2,1,0:T(8,128)(2,1)S(1)} all-to-all(bf16[8,2,48,256]{3,2,1,0:T(8,128)(2,1)S(1)} %broadcast_in_dim.3), channel_id=1, replica_groups={{0,8,16,24,32,40,48,56},{64,72,80,88,96,104,112,120},{128,136,144,152,1..., dimensions={0} | all-to-all | bytes 786432 | tf_op jit(solution)/shard_map/all_to_all | solution.py:35
  22.0 42.1 %all_to_all.16.mine = bf16[8,8,48,256]{3,2,1,0:T(8,128)(2,1)S(1)} all-to-all(bf16[8,8,48,256]{3,2,1,0:T(8,128)(2,1)S(1)} %shard_map.74), channel_id=1, replica_groups={{0,64,128,192,256,320,384,448},{8,72,136,200,264,328,392,456},{16,80,14..., dimensions={0} | all-to-all | bytes 3145728 | tf_op jit(solution)/shard_map/all_to_all | solution.py:45
  66.0 3.4 %collective-permute-start.1 = (bf16[256,512]{1,0:T(8,128)(2,1)}, bf16[256,512]{1,0:T(8,128)(2,1)}, u32[]{:S(2)}, u32[]{:S(2)}) collective-permute-start(bf16[256,512]{1,0:T(8,128)(2,1)} %refs_4_.4), channel_id=1, source_target_pairs={{0,1},{1,2},{2,3},{3,0},{4,5},{5,6},{6,7},{7,4},{8,9},{9,10},{10,1... | collective-permute-start | bytes 786440 | tf_op jit(solution)/shard_map/ppermute | solution.py:75
  71.4 4.6 %collective-permute-start.3 = (bf16[256,512]{1,0:T(8,128)(2,1)}, bf16[256,512]{1,0:T(8,128)(2,1)}, u32[]{:S(2)}, u32[]{:S(2)}) collective-permute-start(bf16[256,512]{1,0:T(8,128)(2,1)} %refs_4_.4), channel_id=1, source_target_pairs={{0,3},{1,0},{2,1},{3,2},{4,7},{5,4},{6,5},{7,6},{8,11},{9,8},{10,9... | collective-permute-start | bytes 786440 | tf_op jit(solution)/shard_map/ppermute | solution.py:75
  76.7 7.0 %collective-permute-done.1.refs_1_ = bf16[256,512]{1,0:T(8,128)(2,1)} collective-permute-done((bf16[256,512]{1,0:T(8,128)(2,1)}, bf16[256,512]{1,0:T(8,128)(2,1)}, u32[]{:S(2)}, u32[]{:S(2)}) %collective-permute-start.1) | collective-permute-done | bytes 262176 | tf_op jit(solution)/shard_map/ppermute | solution.py:75
  83.8 2.5 %collective-permute-done.3.refs_3_ = bf16[256,512]{1,0:T(8,128)(2,1)} collective-permute-done((bf16[256,512]{1,0:T(8,128)(2,1)}, bf16[256,512]{1,0:T(8,128)(2,1)}, u32[]{:S(2)}, u32[]{:S(2)}) %collective-permute-start.3) | collective-permute-done | bytes 262176 | tf_op jit(solution)/shard_map/ppermute | solution.py:75
  93.2 3.8 %collective-permute-done.5.refs_0_ = bf16[128,256]{1,0:T(8,128)(2,1)S(1)} collective-permute-done((bf16[128,256]{1,0:T(8,128)(2,1)S(1)}, bf16[128,256]{1,0:T(8,128)(2,1)S(1)}, u32[]{:S(2)}, u32[]{:S(2)}) %collective-permute-start.5) | collective-permute-done | bytes 65568 | tf_op jit(solution)/shard_map/ppermute | solution.py:389
  98.9 27.4 %all_to_all.17.mine = bf16[8,8,48,256]{3,2,1,0:T(8,128)(2,1)S(1)} all-to-all(bf16[8,8,48,256]{3,2,1,0:T(8,128)(2,1)S(1)} %shard_map.81), channel_id=1, replica_groups={{0,64,128,192,256,320,384,448},{8,72,136,200,264,328,392,456},{16,80,14..., dimensions={0} | all-to-all | bytes 3145728 | tf_op jit(solution)/shard_map/all_to_all | solution.py:45
  128.2 3.1 %collective-permute-start.6 = (bf16[272,256]{1,0:T(8,128)(2,1)S(1)}, bf16[272,256]{1,0:T(8,128)(2,1)S(1)}, u32[]{:S(2)}, u32[]{:S(2)}) collective-permute-start(bf16[272,256]{1,0:T(8,128)(2,1)S(1)} %shard_map.77.refs_0_), channel_id=1, source_target_pairs={{0,1},{1,2},{2,3},{3,0},{4,5},{5,6},{6,7},{7,4},{8,9},{9,10},{10,1... | collective-permute-start | bytes 417800 | tf_op jit(solution)/shard_map/ppermute | solution.py:75
  131.3 4.8 %collective-permute-start.7 = (bf16[272,256]{1,0:T(8,128)(2,1)S(1)}, bf16[272,256]{1,0:T(8,128)(2,1)S(1)}, u32[]{:S(2)}, u32[]{:S(2)}) collective-permute-start(bf16[272,256]{1,0:T(8,128)(2,1)S(1)} %shard_map.77.refs_0_), channel_id=1, source_target_pairs={{0,2},{1,3},{2,0},{3,1},{4,6},{5,7},{6,4},{7,5},{8,10},{9,11},{10,... | collective-permute-start | bytes 417800 | tf_op jit(solution)/shard_map/ppermute | solution.py:75
  136.1 2.3 %collective-permute-start.8 = (bf16[272,256]{1,0:T(8,128)(2,1)S(1)}, bf16[272,256]{1,0:T(8,128)(2,1)S(1)}, u32[]{:S(2)}, u32[]{:S(2)}) collective-permute-start(bf16[272,256]{1,0:T(8,128)(2,1)S(1)} %shard_map.77.refs_0_), channel_id=1, source_target_pairs={{0,3},{1,0},{2,1},{3,2},{4,7},{5,4},{6,5},{7,6},{8,11},{9,8},{10,9... | collective-permute-start | bytes 417800 | tf_op jit(solution)/shard_map/ppermute | solution.py:75
  138.5 2.7 %collective-permute-done.7.refs_2_ = bf16[272,256]{1,0:T(8,128)(2,1)S(1)} collective-permute-done((bf16[272,256]{1,0:T(8,128)(2,1)S(1)}, bf16[272,256]{1,0:T(8,128)(2,1)S(1)}, u32[]{:S(2)}, u32[]{:S(2)}) %collective-permute-start.7) | collective-permute-done | bytes 139296 | tf_op jit(solution)/shard_map/ppermute | solution.py:75
  141.2 2.3 %collective-permute-done.8.refs_3_ = bf16[272,256]{1,0:T(8,128)(2,1)S(1)} collective-permute-done((bf16[272,256]{1,0:T(8,128)(2,1)S(1)}, bf16[272,256]{1,0:T(8,128)(2,1)S(1)}, u32[]{:S(2)}, u32[]{:S(2)}) %collective-permute-start.8) | collective-permute-done | bytes 139296 | tf_op jit(solution)/shard_map/ppermute | solution.py:75
  143.5 2.5 %shard_map.79.refs_0_.refs_4_ = bf16[256,512]{1,0:T(8,128)(2,1)S(1)} custom-call(bf16[272,256]{1,0:T(8,128)(2,1)S(1)} %shard_map.77.refs_0_, bf16[272,256]{1,0:T(8,128)(2,1)S(1)} %collective-permute-done.6.refs_1_, bf16[272,256]{1,0:T(8,128)(2,1)S(1)} %collective-permute-done.7.refs_2_, bf16[272,256]{1,0:T(8,128)(2,1)S(1)} %collective-permute-done.8.refs_3_, ...), custom_call_target="tpu_custom_call" | custom-call | flops 268435456 | bytes 1048576 | tf_op jit(solution)/shard_map/pallas_call | solution.py:269
  146.0 2.5 %collective-permute-start.9 = (bf16[256,512]{1,0:T(8,128)(2,1)S(1)}, bf16[256,512]{1,0:T(8,128)(2,1)S(1)}, u32[]{:S(2)}, u32[]{:S(2)}) collective-permute-start(bf16[256,512]{1,0:T(8,128)(2,1)S(1)} %shard_map.79.refs_0_.refs_4_), channel_id=1, source_target_pairs={{0,1},{1,2},{2,3},{3,0},{4,5},{5,6},{6,7},{7,4},{8,9},{9,10},{10,1... | collective-permute-start | bytes 786440 | tf_op jit(solution)/shard_map/ppermute | solution.py:75
  148.5 4.8 %collective-permute-start.10 = (bf16[256,512]{1,0:T(8,128)(2,1)S(1)}, bf16[256,512]{1,0:T(8,128)(2,1)S(1)}, u32[]{:S(2)}, u32[]{:S(2)}) collective-permute-start(bf16[256,512]{1,0:T(8,128)(2,1)S(1)} %shard_map.79.refs_0_.refs_4_), channel_id=1, source_target_pairs={{0,2},{1,3},{2,0},{3,1},{4,6},{5,7},{6,4},{7,5},{8,10},{9,11},{10,... | collective-permute-start | bytes 786440 | tf_op jit(solution)/shard_map/ppermute | solution.py:75
  153.3 2.2 %collective-permute-start.11 = (bf16[256,512]{1,0:T(8,128)(2,1)S(1)}, bf16[256,512]{1,0:T(8,128)(2,1)S(1)}, u32[]{:S(2)}, u32[]{:S(2)}) collective-permute-start(bf16[256,512]{1,0:T(8,128)(2,1)S(1)} %shard_map.79.refs_0_.refs_4_), channel_id=1, source_target_pairs={{0,3},{1,0},{2,1},{3,2},{4,7},{5,4},{6,5},{7,6},{8,11},{9,8},{10,9... | collective-permute-start | bytes 786440 | tf_op jit(solution)/shard_map/ppermute | solution.py:75
  157.3 5.4 %collective-permute-done.10.refs_2_ = bf16[256,512]{1,0:T(8,128)(2,1)S(1)} collective-permute-done((bf16[256,512]{1,0:T(8,128)(2,1)S(1)}, bf16[256,512]{1,0:T(8,128)(2,1)S(1)}, u32[]{:S(2)}, u32[]{:S(2)}) %collective-permute-start.10) | collective-permute-done | bytes 262176 | tf_op jit(solution)/shard_map/ppermute | solution.py:75
  169.6 4.2 %collective-permute-done.13.refs_0_ = bf16[128,256]{1,0:T(8,128)(2,1)S(1)} collective-permute-done((bf16[128,256]{1,0:T(8,128)(2,1)S(1)}, bf16[128,256]{1,0:T(8,128)(2,1)S(1)}, u32[]{:S(2)}, u32[]{:S(2)}) %collective-permute-start.13) | collective-permute-done | bytes 65568 | tf_op jit(solution)/shard_map/ppermute | solution.py:389
  175.8 3.0 %collective-permute-start.14 = (bf16[272,256]{1,0:T(8,128)(2,1)S(1)}, bf16[272,256]{1,0:T(8,128)(2,1)S(1)}, u32[]{:S(2)}, u32[]{:S(2)}) collective-permute-start(bf16[272,256]{1,0:T(8,128)(2,1)S(1)} %shard_map.84.refs_0_), channel_id=1, source_target_pairs={{0,1},{1,2},{2,3},{3,0},{4,5},{5,6},{6,7},{7,4},{8,9},{9,10},{10,1... | collective-permute-start | bytes 417800 | tf_op jit(solution)/shard_map/ppermute | solution.py:75
  178.7 5.0 %collective-permute-start.15 = (bf16[272,256]{1,0:T(8,128)(2,1)S(1)}, bf16[272,256]{1,0:T(8,128)(2,1)S(1)}, u32[]{:S(2)}, u32[]{:S(2)}) collective-permute-start(bf16[272,256]{1,0:T(8,128)(2,1)S(1)} %shard_map.84.refs_0_), channel_id=1, source_target_pairs={{0,2},{1,3},{2,0},{3,1},{4,6},{5,7},{6,4},{7,5},{8,10},{9,11},{10,... | collective-permute-start | bytes 417800 | tf_op jit(solution)/shard_map/ppermute | solution.py:75
  183.7 2.1 %collective-permute-start.16 = (bf16[272,256]{1,0:T(8,128)(2,1)S(1)}, bf16[272,256]{1,0:T(8,128)(2,1)S(1)}, u32[]{:S(2)}, u32[]{:S(2)}) collective-permute-start(bf16[272,256]{1,0:T(8,128)(2,1)S(1)} %shard_map.84.refs_0_), channel_id=1, source_target_pairs={{0,3},{1,0},{2,1},{3,2},{4,7},{5,4},{6,5},{7,6},{8,11},{9,8},{10,9... | collective-permute-start | bytes 417800 | tf_op jit(solution)/shard_map/ppermute | solution.py:75
  187.2 3.5 %collective-permute-done.16.refs_3_ = bf16[272,256]{1,0:T(8,128)(2,1)S(1)} collective-permute-done((bf16[272,256]{1,0:T(8,128)(2,1)S(1)}, bf16[272,256]{1,0:T(8,128)(2,1)S(1)}, u32[]{:S(2)}, u32[]{:S(2)}) %collective-permute-start.16) | collective-permute-done | bytes 139296 | tf_op jit(solution)/shard_map/ppermute | solution.py:75
  190.7 2.2 %shard_map.86 = bf16[256,512]{1,0:T(8,128)(2,1)} custom-call(bf16[272,256]{1,0:T(8,128)(2,1)S(1)} %shard_map.84.refs_0_, bf16[272,256]{1,0:T(8,128)(2,1)S(1)} %collective-permute-done.14.refs_1_, bf16[272,256]{1,0:T(8,128)(2,1)S(1)} %collective-permute-done.15.refs_2_, bf16[272,256]{1,0:T(8,128)(2,1)S(1)} %collective-permute-done.16.refs_3_, ...), custom_call_target="tpu_custom_call" | custom-call | flops 268435456 | bytes 1048576 | tf_op jit(solution)/shard_map/pallas_call | solution.py:269
  (38 shorter events, 30.4 us)
Async XLA Ops:
  0.0 2.8 %collective-permute-start = (bf16[2,16,256]{2,1,0:T(8,128)(2,1)}, bf16[2,16,256]{2,1,0:T(8,128)(2,1)S(1)}, u32[]{:S(2)}, u32[]{:S(2)}) collective-permute-start(bf16[2,16,256]{2,1,0:T(8,128)(2,1)} %bitcast.1), channel_id=1, source_target_pairs={{0,0},{1,128},{2,256},{3,384},{4,4},{5,20},{6,36},{7,52},{8,8},{9,... | collective-permute-start | bytes 49160 | tf_op jit(solution)/shard_map/ppermute | solution.py:70
  64.1 24.1 %collective-permute-start.4 = (bf16[8,8,48,256]{3,2,1,0:T(8,128)(2,1)S(1)}, bf16[8,8,48,256]{3,2,1,0:T(8,128)(2,1)S(1)}, u32[]{:S(2)}, u32[]{:S(2)}) collective-permute-start(bf16[8,8,48,256]{3,2,1,0:T(8,128)(2,1)S(1)} %all_to_all.16.mine), channel_id=1, source_target_pairs={{0,4},{4,0},{8,12},{12,8},{16,20},{20,16},{24,28},{28,24},{32,36},... | collective-permute-start | bytes 4718600 | tf_op jit(solution)/shard_map/ppermute | solution.py:57
  66.0 17.8 %collective-permute-start.1 = (bf16[256,512]{1,0:T(8,128)(2,1)}, bf16[256,512]{1,0:T(8,128)(2,1)}, u32[]{:S(2)}, u32[]{:S(2)}) collective-permute-start(bf16[256,512]{1,0:T(8,128)(2,1)} %refs_4_.4), channel_id=1, source_target_pairs={{0,1},{1,2},{2,3},{3,0},{4,5},{5,6},{6,7},{7,4},{8,9},{9,10},{10,1... | collective-permute-start | bytes 786440 | tf_op jit(solution)/shard_map/ppermute | solution.py:75
  69.5 14.3 %collective-permute-start.2 = (bf16[256,512]{1,0:T(8,128)(2,1)}, bf16[256,512]{1,0:T(8,128)(2,1)}, u32[]{:S(2)}, u32[]{:S(2)}) collective-permute-start(bf16[256,512]{1,0:T(8,128)(2,1)} %refs_4_.4), channel_id=1, source_target_pairs={{0,2},{1,3},{2,0},{3,1},{4,6},{5,7},{6,4},{7,5},{8,10},{9,11},{10,... | collective-permute-start | bytes 786440 | tf_op jit(solution)/shard_map/ppermute | solution.py:75
  71.4 14.9 %collective-permute-start.3 = (bf16[256,512]{1,0:T(8,128)(2,1)}, bf16[256,512]{1,0:T(8,128)(2,1)}, u32[]{:S(2)}, u32[]{:S(2)}) collective-permute-start(bf16[256,512]{1,0:T(8,128)(2,1)} %refs_4_.4), channel_id=1, source_target_pairs={{0,3},{1,0},{2,1},{3,2},{4,7},{5,4},{6,5},{7,6},{8,11},{9,8},{10,9... | collective-permute-start | bytes 786440 | tf_op jit(solution)/shard_map/ppermute | solution.py:75
  89.1 2.5 %copy-start = (f32[2,128,256]{2,1,0:T(8,128)S(1)}, f32[2,128,256]{2,1,0:T(8,128)}, u32[]{:S(2)}) copy-start(f32[2,128,256]{2,1,0:T(8,128)} %refs_3_.3) | copy-start | bytes 786436
  89.1 7.9 %copy-start.1 = (f32[2,256]{1,0:T(2,128)S(1)}, f32[2,256]{1,0:T(2,128)}, u32[]{:S(2)}) copy-start(f32[2,256]{1,0:T(2,128)} %refs_4_.5) | copy-start | bytes 6148
  89.1 7.8 %collective-permute-start.5 = (bf16[128,256]{1,0:T(8,128)(2,1)S(1)}, bf16[128,256]{1,0:T(8,128)(2,1)S(1)}, u32[]{:S(2)}, u32[]{:S(2)}) collective-permute-start(bf16[128,256]{1,0:T(8,128)(2,1)S(1)} %slice.8), channel_id=1, source_target_pairs={{0,4},{4,8},{8,12},{12,16},{16,20},{20,24},{24,28},{28,32},{32,36}... | collective-permute-start | bytes 196616 | tf_op jit(solution)/shard_map/ppermute | solution.py:389
  126.3 38.9 %collective-permute-start.12 = (bf16[8,8,48,256]{3,2,1,0:T(8,128)(2,1)S(1)}, bf16[8,8,48,256]{3,2,1,0:T(8,128)(2,1)S(1)}, u32[]{:S(2)}, u32[]{:S(2)}) collective-permute-start(bf16[8,8,48,256]{3,2,1,0:T(8,128)(2,1)S(1)} %all_to_all.17.mine), channel_id=1, source_target_pairs={{0,4},{4,0},{8,12},{12,8},{16,20},{20,16},{24,28},{28,24},{32,36},... | collective-permute-start | bytes 4718600 | tf_op jit(solution)/shard_map/ppermute | solution.py:57
  128.2 10.3 %collective-permute-start.6 = (bf16[272,256]{1,0:T(8,128)(2,1)S(1)}, bf16[272,256]{1,0:T(8,128)(2,1)S(1)}, u32[]{:S(2)}, u32[]{:S(2)}) collective-permute-start(bf16[272,256]{1,0:T(8,128)(2,1)S(1)} %shard_map.77.refs_0_), channel_id=1, source_target_pairs={{0,1},{1,2},{2,3},{3,0},{4,5},{5,6},{6,7},{7,4},{8,9},{9,10},{10,1... | collective-permute-start | bytes 417800 | tf_op jit(solution)/shard_map/ppermute | solution.py:75
  131.3 9.9 %collective-permute-start.7 = (bf16[272,256]{1,0:T(8,128)(2,1)S(1)}, bf16[272,256]{1,0:T(8,128)(2,1)S(1)}, u32[]{:S(2)}, u32[]{:S(2)}) collective-permute-start(bf16[272,256]{1,0:T(8,128)(2,1)S(1)} %shard_map.77.refs_0_), channel_id=1, source_target_pairs={{0,2},{1,3},{2,0},{3,1},{4,6},{5,7},{6,4},{7,5},{8,10},{9,11},{10,... | collective-permute-start | bytes 417800 | tf_op jit(solution)/shard_map/ppermute | solution.py:75
  136.1 7.4 %collective-permute-start.8 = (bf16[272,256]{1,0:T(8,128)(2,1)S(1)}, bf16[272,256]{1,0:T(8,128)(2,1)S(1)}, u32[]{:S(2)}, u32[]{:S(2)}) collective-permute-start(bf16[272,256]{1,0:T(8,128)(2,1)S(1)} %shard_map.77.refs_0_), channel_id=1, source_target_pairs={{0,3},{1,0},{2,1},{3,2},{4,7},{5,4},{6,5},{7,6},{8,11},{9,8},{10,9... | collective-permute-start | bytes 417800 | tf_op jit(solution)/shard_map/ppermute | solution.py:75
  146.0 11.2 %collective-permute-start.9 = (bf16[256,512]{1,0:T(8,128)(2,1)S(1)}, bf16[256,512]{1,0:T(8,128)(2,1)S(1)}, u32[]{:S(2)}, u32[]{:S(2)}) collective-permute-start(bf16[256,512]{1,0:T(8,128)(2,1)S(1)} %shard_map.79.refs_0_.refs_4_), channel_id=1, source_target_pairs={{0,1},{1,2},{2,3},{3,0},{4,5},{5,6},{6,7},{7,4},{8,9},{9,10},{10,1... | collective-permute-start | bytes 786440 | tf_op jit(solution)/shard_map/ppermute | solution.py:75
  148.5 14.2 %collective-permute-start.10 = (bf16[256,512]{1,0:T(8,128)(2,1)S(1)}, bf16[256,512]{1,0:T(8,128)(2,1)S(1)}, u32[]{:S(2)}, u32[]{:S(2)}) collective-permute-start(bf16[256,512]{1,0:T(8,128)(2,1)S(1)} %shard_map.79.refs_0_.refs_4_), channel_id=1, source_target_pairs={{0,2},{1,3},{2,0},{3,1},{4,6},{5,7},{6,4},{7,5},{8,10},{9,11},{10,... | collective-permute-start | bytes 786440 | tf_op jit(solution)/shard_map/ppermute | solution.py:75
  153.3 11.2 %collective-permute-start.11 = (bf16[256,512]{1,0:T(8,128)(2,1)S(1)}, bf16[256,512]{1,0:T(8,128)(2,1)S(1)}, u32[]{:S(2)}, u32[]{:S(2)}) collective-permute-start(bf16[256,512]{1,0:T(8,128)(2,1)S(1)} %shard_map.79.refs_0_.refs_4_), channel_id=1, source_target_pairs={{0,3},{1,0},{2,1},{3,2},{4,7},{5,4},{6,5},{7,6},{8,11},{9,8},{10,9... | collective-permute-start | bytes 786440 | tf_op jit(solution)/shard_map/ppermute | solution.py:75
  166.1 7.7 %collective-permute-start.13 = (bf16[128,256]{1,0:T(8,128)(2,1)S(1)}, bf16[128,256]{1,0:T(8,128)(2,1)S(1)}, u32[]{:S(2)}, u32[]{:S(2)}) collective-permute-start(bf16[128,256]{1,0:T(8,128)(2,1)S(1)} %slice.9), channel_id=1, source_target_pairs={{0,4},{4,8},{8,12},{12,16},{16,20},{20,24},{24,28},{28,32},{32,36}... | collective-permute-start | bytes 196616 | tf_op jit(solution)/shard_map/ppermute | solution.py:389
  175.8 10.2 %collective-permute-start.14 = (bf16[272,256]{1,0:T(8,128)(2,1)S(1)}, bf16[272,256]{1,0:T(8,128)(2,1)S(1)}, u32[]{:S(2)}, u32[]{:S(2)}) collective-permute-start(bf16[272,256]{1,0:T(8,128)(2,1)S(1)} %shard_map.84.refs_0_), channel_id=1, source_target_pairs={{0,1},{1,2},{2,3},{3,0},{4,5},{5,6},{6,7},{7,4},{8,9},{9,10},{10,1... | collective-permute-start | bytes 417800 | tf_op jit(solution)/shard_map/ppermute | solution.py:75
  178.7 8.5 %collective-permute-start.15 = (bf16[272,256]{1,0:T(8,128)(2,1)S(1)}, bf16[272,256]{1,0:T(8,128)(2,1)S(1)}, u32[]{:S(2)}, u32[]{:S(2)}) collective-permute-start(bf16[272,256]{1,0:T(8,128)(2,1)S(1)} %shard_map.84.refs_0_), channel_id=1, source_target_pairs={{0,2},{1,3},{2,0},{3,1},{4,6},{5,7},{6,4},{7,5},{8,10},{9,11},{10,... | collective-permute-start | bytes 417800 | tf_op jit(solution)/shard_map/ppermute | solution.py:75
  183.7 6.9 %collective-permute-start.16 = (bf16[272,256]{1,0:T(8,128)(2,1)S(1)}, bf16[272,256]{1,0:T(8,128)(2,1)S(1)}, u32[]{:S(2)}, u32[]{:S(2)}) collective-permute-start(bf16[272,256]{1,0:T(8,128)(2,1)S(1)} %shard_map.84.refs_0_), channel_id=1, source_target_pairs={{0,3},{1,0},{2,1},{3,2},{4,7},{5,4},{6,5},{7,6},{8,11},{9,8},{10,9... | collective-permute-start | bytes 417800 | tf_op jit(solution)/shard_map/ppermute | solution.py:75

commit v3 on v2

--- a/solution.py
+++ b/solution.py
@@ -100,9 +100,10 @@
         scale[rows, :] = total
         return 0
 
-    lax.fori_loop(0, TOK // 16, squares, 0, unroll=2)
+    steps = scale.shape[0] // 16
+    lax.fori_loop(0, steps, squares, 0, unroll=2)
     mean = jnp.sum(scale[...], axis=1, keepdims=True) / (NX * FEAT)
-    scale[...] = jnp.broadcast_to(lax.rsqrt(mean + 1e-06), (TOK, 128))
+    scale[...] = jnp.broadcast_to(lax.rsqrt(mean + 1e-06), scale.shape)
 
     def apply(i, _):
         rows = pl.ds(pl.multiple_of(i * 16, 16), 16)
@@ -112,15 +113,18 @@
             xs[owner, rows, :] = (ref[rows, :].astype(F32) * factor * gain[layer * NX + owner]).astype(BF)
         return 0
 
-    lax.fori_loop(0, TOK // 16, apply, 0, unroll=2)
-
-
-def mix_kernel(xs, mine, other, glu, vs, gs):
+    lax.fori_loop(0, steps, apply, 0, unroll=2)
+
+
+def mix_kernel(xs, mine, other, glu, wt, vs, gs):
     def fill(zy, yz):
         for z in range(NZ):
             for c, w in enumerate((zy.at[z], yz.at[:, z])):
                 vs[z, :, c] = w[:, :16, :]
                 gs[z, :, c] = w[:, 16:32, :]
+        for k in range(NX):
+            for c, w in enumerate((zy, yz)):
+                wt[k, :, :, c] = w[2 * k : 2 * k + 2, :, 32:, :]
 
     @pl.when(core_here() == 0)
     def _():
@@ -130,8 +134,8 @@
     def _():
         fill(other, mine)
 
-    value = jnp.zeros((TOK, CH), F32)
-    gate = jnp.zeros((TOK, CH), F32)
+    value = jnp.zeros(glu.shape, F32)
+    gate = jnp.zeros(glu.shape, F32)
     for k in range(NX):
         planes = slice(2 * k, 2 * k + 2)
         value += jnp.dot(xs[k], vs[planes].reshape(FEAT, CH), preferred_element_type=F32)
@@ -145,71 +149,75 @@
     return [hi, mid, v - hi - mid]
 
 
-def conv_half(layer, ext, taps, conv, shifted, base):
-    for b in range(8):
-        shifted[b] = ext[1 + b : 1 + b + SPAN, :]
-    for lane in range(0, CH, 128):
-
-        def step(a, acc):
-            start = pl.multiple_of(a * 8, 8)
-            tap = taps[layer, pl.ds(start, 8), lane : lane + 128]
-            for b in range(8):
-                acc += shifted[b, pl.ds(start, HALF), lane : lane + 128] * tap[b : b + 1]
-            return acc
-
-        acc = lax.fori_loop(0, TAPS // 8, step, jnp.zeros((HALF, 128), F32))
-        conv[base : base + HALF, lane : lane + 128] = acc
-
-
-def late_kernel(layer, glu, taps, conv, ext, shifted):
-    ext[...] = glu[...].astype(F32)
-    conv_half(layer, ext, taps, conv, shifted, 0)
-
-
-def spread_kernel(layer, once, out, sems):
-    copies = [pltpu.make_async_copy(once.at[:, layer], out.at[k], sems.at[k]) for k in range(NZ)]
+def send_all(src, out, sems):
+    copies = [pltpu.make_async_copy(src, out.at[k], sems.at[k]) for k in range(out.shape[0])]
     for c in copies:
         c.start()
     for c in copies:
         c.wait()
 
 
-def conv_kernel(layer, before, glu, late, taps, gain, out, ext, shifted, conv):
-    ext[:TAPS, :] = before[...].astype(F32)
-    ext[TAPS:, :] = glu[:HALF, :].astype(F32)
-    conv_half(layer, ext, taps, conv, shifted, 0)
-    conv[HALF:, :] = late[...]
+def spread_kernel(layer, once, out, sems):
+    send_all(once.at[:, layer], out, sems)
+
+
+def taps_over(layer, ext, taps, conv, shifted):
+    rows = conv.shape[0]
+    for b in range(8):
+        shifted[b] = ext[1 + b : 1 + b + rows + TAPS - 8, :]
+    for lane in range(0, CH, 128):
+        for base in range(0, rows, HALF):
+
+            def step(a, acc):
+                start = pl.multiple_of(a * 8, 8)
+                tap = taps[layer, pl.ds(start, 8), lane : lane + 128]
+                for b in range(8):
+                    window = shifted[b, pl.ds(start + base, HALF), lane : lane + 128]
+                    acc += window * tap[b : b + 1]
+                return acc
+
+            acc = lax.fori_loop(0, TAPS // 8, step, jnp.zeros((HALF, 128), F32))
+            conv[base : base + HALF, lane : lane + 128] = acc
+
+
+def pack(layer, conv, gain, out):
     ones = jnp.full((8, CH), 1.0 / CH, F32)
     means = lax.dot_general(
         ones, conv[...], (((1,), (1,)), ((), ())), precision=lax.Precision.HIGHEST,
         preferred_element_type=F32,
     )[:1]
     extra = split_three(means) + split_three(gain[layer : layer + 1, :])
-    extra = jnp.concatenate(extra + [jnp.zeros((10, CH), F32)], axis=0).astype(BF)
+    out[TOK:, :] = jnp.concatenate(extra + [jnp.zeros((10, CH), F32)], axis=0).astype(BF)
     v = conv[...]
-    d = (v - jnp.mean(v, axis=1, keepdims=True)).astype(BF)
-    out[TOK:, :] = extra
-    out[:TOK, :] = d
-
-
-def arrange_kernel(mine, other, wt):
-    def fill(zy, yz):
-        for k in range(NX):
-            for c, w in enumerate((zy, yz)):
-                wt[k, :, :, c] = w[2 * k : 2 * k + 2, :, 32:, :]
-
-    @pl.when(core_here() == 0)
-    def _():
-        fill(mine, other)
-
-    @pl.when(core_here() == 1)
-    def _():
-        fill(other, mine)
+    out[:TOK, :] = (v - jnp.mean(v, axis=1, keepdims=True)).astype(BF)
+
+
+def whole_kernel(layer, glu, taps, gain, out, ext, shifted, conv):
+    ext[...] = glu[...].astype(F32)
+    taps_over(layer, ext, taps, conv, shifted)
+    pack(layer, conv, gain, out)
+
+
+def late_kernel(layer, glu, taps, conv, ext, shifted):
+    ext[...] = glu[...].astype(F32)
+    taps_over(layer, ext, taps, conv, shifted)
+
+
+def conv_kernel(layer, before, glu, late, taps, gain, out, ext, shifted, conv):
+    ext[:TAPS, :] = before[...].astype(F32)
+    ext[TAPS:, :] = glu[:HALF, :].astype(F32)
+    taps_over(layer, ext, taps, conv.at[:HALF], shifted)
+    conv[HALF:, :] = late[...]
+    pack(layer, conv, gain, out)
 
 
 def out_kernel(n, *refs):
     parts, rest = refs[:n], refs[n:]
-    x, wt, out, means, scale, acts = rest
+    x, wt, out, *rest = rest
+    copies = rest[0] if len(rest) == 6 else None
+    means, scale, acts, held, sems = rest[-5:]
+    fetch = pltpu.make_async_copy(x, held, sems.at[0])
+    fetch.start()
     pick = (lax.broadcasted_iota(jnp.int32, (16, 128), 0) < 3).astype(BF)
     total = jnp.zeros((TOK, 128), F32)
     for k in range(NX):
@@ -262,15 +270,19 @@
             acts[k], wt[k].reshape(FEAT, CH), (((1,), (1,)), ((), ())),
             preferred_element_type=F32,
         )
-    out[...] = (x[...].astype(F32) + branch).astype(BF)
+    fetch.wait()
+    out[...] = (held[...].astype(F32) + branch).astype(BF)
+    if copies is not None:
+        send_all(out, copies, sems)
 
 
 def call(body, out, ins, scratch, flops, place=pltpu.VMEM):
+    spec = pl.BlockSpec(memory_space=place)
     return pl.pallas_call(
         body,
         out_shape=out,
         in_specs=[pl.BlockSpec(memory_space=pltpu.VMEM)] * len(ins),
-        out_specs=pl.BlockSpec(memory_space=place),
+        out_specs=(spec,) * len(out) if isinstance(out, tuple) else spec,
         scratch_shapes=scratch,
         cost_estimate=pl.CostEstimate(flops=flops, transcendentals=0, bytes_accessed=1 << 20),
         compiler_params=pltpu.CompilerParams(vmem_limit_bytes=14 << 20),
@@ -284,9 +296,9 @@
 
     return call(
         body,
-        jax.ShapeDtypeStruct((NX, TOK, FEAT), BF),
+        jax.ShapeDtypeStruct((NX, parts[0].shape[-2], FEAT), BF),
         [*parts, gain],
-        [pltpu.VMEM((TOK, 128), F32)],
+        [pltpu.VMEM((parts[0].shape[-2], 128), F32)],
         8 * NX * TOK * FEAT,
     )
 
@@ -294,7 +306,10 @@
 def mix(xs, mine, other):
     return call(
         mix_kernel,
-        jax.ShapeDtypeStruct((TOK, CH), BF),
+        (
+            jax.ShapeDtypeStruct((xs.shape[1], CH), BF),
+            jax.ShapeDtypeStruct((NX, 2, NY, 2, 16, CH), BF),
+        ),
         [xs, mine, other],
         [pltpu.VMEM((NZ, NY, 2, 16, CH), BF), pltpu.VMEM((NZ, NY, 2, 16, CH), BF)],
         4 * NX * TOK * FEAT * CH,
@@ -311,6 +326,23 @@
         [glu, taps],
         [pltpu.VMEM((TOK, CH), F32), pltpu.VMEM((8, SPAN, CH), F32)],
         2 * HALF * CH * TAPS,
+    )
+
+
+def conv_whole(layer, glu, taps, gain):
+    def body(*refs):
+        whole_kernel(layer, *refs)
+
+    return call(
+        body,
+        jax.ShapeDtypeStruct((PACK, CH), BF),
+        [glu, taps, gain],
+        [
+            pltpu.VMEM((TAPS + TOK, CH), F32),
+            pltpu.VMEM((8, TOK + TAPS - 8, CH), F32),
+            pltpu.VMEM((TOK, CH), F32),
+        ],
+        2 * TOK * CH * TAPS,
     )
 
 
@@ -345,27 +377,31 @@
     )
 
 
-def arrange(mine, other):
-    return call(
-        arrange_kernel, jax.ShapeDtypeStruct((NX, 2, NY, 2, 16, CH), BF), [mine, other], [], 1 << 26
-    )
-
-
-def project(parts, x, wt):
+def project(parts, x, wt, to_all):
     def body(*refs):
         out_kernel(len(parts), *refs)
 
-    return call(
-        body,
-        jax.ShapeDtypeStruct((TOK, FEAT), BF),
-        [*parts, x, wt],
-        [
+    shape = jax.ShapeDtypeStruct((TOK, FEAT), BF)
+    copies = pltpu.HBM((NX, TOK, FEAT), BF)
+    inside, anywhere = pl.BlockSpec(memory_space=pltpu.VMEM), pl.BlockSpec(memory_space=pl.ANY)
+    return pl.pallas_call(
+        body,
+        out_shape=(shape, copies) if to_all else shape,
+        in_specs=[inside] * len(parts) + [anywhere, inside],
+        out_specs=(inside, pl.BlockSpec(memory_space=pltpu.HBM)) if to_all else inside,
+        scratch_shapes=[
             pltpu.VMEM((NX, TOK, 128), F32),
             pltpu.VMEM((TOK, 128), F32),
             pltpu.VMEM((NX, TOK, CH), BF),
+            pltpu.VMEM((TOK, FEAT), BF),
+            pltpu.SemaphoreType.DMA((NX,)),
         ],
-        2 * NX * TOK * CH * FEAT,
-    )
+        cost_estimate=pl.CostEstimate(
+            flops=2 * NX * TOK * CH * FEAT, transcendentals=0, bytes_accessed=1 << 20
+        ),
+        compiler_params=pltpu.CompilerParams(vmem_limit_bytes=14 << 20),
+        interpret=INTERPRET,
+    )(*parts, x, wt)
 
 
 def shards(stream, norm_gain, w_value, w_gate, conv_taps, channel_gain, w_out):
@@ -375,27 +411,30 @@
 
     x = stream
     count = lax.axis_size("sp")
+    chain = [(i, i + 1) for i in range(count - 1)]
+    extended = jnp.concatenate([lax.ppermute(x[TOK - TAPS :], "sp", chain), x])
     once = lines(blocks)
-    parts = from_all_x(after(x, blocks))
+    parts = from_all_x(after(extended, blocks))
     ready = spread(0, once)
     gathered = plane(ready)
     ready = spread(1, once)
-    for layer in range(LAYERS):
-        last = layer + 1 == LAYERS
-        mine = gathered
-        other = swap_cores(mine)
-        normed = normalise(layer, parts, gain)
-        glu = mix(normed, mine, other)
-        before = lax.ppermute(glu[TOK - TAPS :], "sp", [(i, i + 1) for i in range(count - 1)])
-        late = conv_late(layer, glu, conv_taps)
-        packed = convolve(layer, before, glu, late, conv_taps, channel_gain)
-        parts = from_all_x(packed)
-        if not last:
-            gathered = plane(after(ready, packed))
-        wt = arrange(after(mine, packed), other)
-        x = project(parts, x, wt)
-        if not last:
-            parts = from_all_x(x)
+    normed = normalise(0, parts, gain)
+    other = swap_cores(gathered)
+    following = plane(after(ready, gathered))
+    glu, wt = mix(normed, gathered, other)
+    packed = conv_whole(0, glu, conv_taps, channel_gain)
+    parts = from_all_x(packed)
+    x, copies = project(parts, x, wt, True)
+
+    parts = [lax.all_to_all(copies, "x", split_axis=0, concat_axis=0, tiled=True)]
+    other = swap_cores(following)
+    normed = normalise(1, parts, gain)
+    glu, wt = mix(normed, following, other)
+    before = lax.ppermute(glu[TOK - TAPS :], "sp", chain)
+    late = conv_late(1, glu, conv_taps)
+    packed = convolve(1, before, glu, late, conv_taps, channel_gain)
+    parts = from_all_x(packed)
+    x = project(parts, x, wt, False)
     return x
 
 

time: 194 us -> 196 us (1.010)
  blocking collectives: 88.3 us -> 36.4 us
  waiting for transfers between devices: 36.3 us -> 69.1 us
  starting transfers between devices: 48.8 us -> 63.1 us
  Pallas kernels: 16.9 us -> 21.5 us
    all_to_all x2 -> x1, blocking collectives: 69.5 us -> 17.7 us  [shards(): lax.all_to_all(copies, 'x', split_axis=0, concat_axis=0, tiled=True)]
    all_to_all x0 -> x2, waiting for transfers between devices: none -> 40.1 us  [plane(): lax.all_to_all(copies, 'sp', split_axis=0, concat_axis=0, tiled=True, axi...]
    all_to_all x0 -> x2, starting transfers between devices: none -> 24.3 us  [plane(): lax.all_to_all(copies, 'sp', split_axis=0, concat_axis=0, tiled=True, axi...]
    ppermute x12 -> x9, starting transfers between devices: 39.7 us -> 29.3 us  [from_all_x(): lax.ppermute(v, 'x', [(i, (i + step) % NX) for i in range(NX)])]
    pallas_call x0 -> x2, Pallas kernels: none -> 4.97 us  [project(): pl.pallas_call(body, out_shape=(shape, copies) if to_all else shape, in_s...]
    ppermute x2, waiting for transfers between devices: 8 us -> 4.19 us  [the longest x1 4.18 us: shards(): before = lax.ppermute(glu[TOK - TAPS:], 'sp', chain)]
    ppermute x12 -> x9, waiting for transfers between devices: 28.3 us -> 24.8 us  [from_all_x(): lax.ppermute(v, 'x', [(i, (i + step) % NX) for i in range(NX)])]
    pallas_call x14 -> x9, Pallas kernels: 16.9 us -> 16.5 us  [call(): pl.pallas_call(body, out_shape=out, in_specs=[pl.BlockSpec(memory_space=p...]
  transfers between devices with their start and end apart: 17 -> 16, of which waited for: 11 -> 9; matrix products, arithmetic and copies ran while one was open for 1% -> 2% of each run, Pallas kernels for 5% -> 7%
where the time goes in v3:
time: 196 us; the launch traced here: 195 us
  waiting for transfers between devices  69.1 us (35%)
  starting transfers between devices  63.1 us (32%)
  blocking collectives  36.4 us (19%)
  Pallas kernels  21.5 us (11%)
  local copies, waits for them, and re-layouts  2.67 us (1%)
    all_to_all x2, waiting for transfers between devices, plane(): lax.all_to_all(copies, 'sp', split_axis=0, concat_axis=0, tiled=True, axi...  40.1 us
    ppermute x9, starting transfers between devices, from_all_x(): lax.ppermute(v, 'x', [(i, (i + step) % NX) for i in range(NX)])  29.3 us
    ppermute x9, waiting for transfers between devices, from_all_x(): lax.ppermute(v, 'x', [(i, (i + step) % NX) for i in range(NX)])  24.8 us
    all_to_all x2, starting transfers between devices, plane(): lax.all_to_all(copies, 'sp', split_axis=0, concat_axis=0, tiled=True, axi...  24.3 us
    all_to_all x1, blocking collectives, to_group(): lax.all_to_all(copies, 'sp', split_axis=0, concat_axis=0, tiled=True, axi...  18.8 us
    all_to_all x1, blocking collectives, shards(): lax.all_to_all(copies, 'x', split_axis=0, concat_axis=0, tiled=True)  17.7 us
    pallas_call x9, Pallas kernels, call(): pl.pallas_call(body, out_shape=out, in_specs=[pl.BlockSpec(memory_space=p...  16.5 us
    pallas_call x2, Pallas kernels, project(): pl.pallas_call(body, out_shape=(shape, copies) if to_all else shape, in_s...  4.97 us
  transfers between devices with their start and end apart: 16, of which 9 were waited for; matrix products, arithmetic and copies ran while one was open for 2% of the time, Pallas kernels for 7%

profile of v3, /device:TPU:64, one launch (start us, length us, event | category | flops | bytes accessed | tf_op | source)
XLA Modules:
  0.0 194.7 jit_solution(8914843139904956987)
XLA Ops:
  2.8 18.8 %all_to_all.20.refs_0_ = bf16[8,2,48,256]{3,2,1,0:T(8,128)(2,1)S(1)} all-to-all(bf16[8,2,48,256]{3,2,1,0:T(8,128)(2,1)S(1)} %broadcast_in_dim.3), channel_id=1, replica_groups={{0,8,16,24,32,40,48,56},{64,72,80,88,96,104,112,120},{128,136,144,152,1..., dimensions={0} | all-to-all | bytes 786432 | tf_op jit(solution)/shard_map/all_to_all | solution.py:35
  22.9 19.3 %all-to-all-start.1 = ((bf16[8,8,48,256]{3,2,1,0:T(8,128)(2,1)}), bf16[8,8,48,256]{3,2,1,0:T(8,128)(2,1)S(1)}, u32[]{:S(2)}, u32[]{:S(2)}) async-start(bf16[8,8,48,256]{3,2,1,0:T(8,128)(2,1)} %shard_map.74), calls=%async_computation.1 | async-start | bytes 3145728 | tf_op jit(solution)/shard_map/all_to_all | solution.py:45
  43.7 21.5 %all-to-all-done.1.mine = bf16[8,8,48,256]{3,2,1,0:T(8,128)(2,1)S(1)} async-done(((bf16[8,8,48,256]{3,2,1,0:T(8,128)(2,1)}), bf16[8,8,48,256]{3,2,1,0:T(8,128)(2,1)S(1)}, u32[]{:S(2)}, u32[]{:S(2)}) %all-to-all-start.1) | async-done | bytes 1572896 | tf_op jit(solution)/shard_map/all_to_all | solution.py:45
  65.1 5.0 %all-to-all-start.3 = ((bf16[8,8,48,256]{3,2,1,0:T(8,128)(2,1)}), bf16[8,8,48,256]{3,2,1,0:T(8,128)(2,1)S(1)}, u32[]{:S(2)}, u32[]{:S(2)}) async-start(bf16[8,8,48,256]{3,2,1,0:T(8,128)(2,1)} %copy-done), calls=%async_computation.3 | async-start | bytes 3145728 | tf_op jit(solution)/shard_map/all_to_all | solution.py:45
  72.1 2.4 %collective-permute-start = (bf16[128,512]{1,0:T(8,128)(2,1)S(1)}, bf16[128,512]{1,0:T(8,128)(2,1)}, u32[]{:S(2)}, u32[]{:S(2)}) collective-permute-start(bf16[128,512]{1,0:T(8,128)(2,1)S(1)} %slice.6), channel_id=1, source_target_pairs={{0,4},{4,8},{8,12},{12,16},{16,20},{20,24},{24,28},{28,32},{32,36}... | collective-permute-start | bytes 393224 | tf_op jit(solution)/shard_map/ppermute | solution.py:415
  74.5 18.6 %all-to-all-done.3.mine = bf16[8,8,48,256]{3,2,1,0:T(8,128)(2,1)S(1)} async-done(((bf16[8,8,48,256]{3,2,1,0:T(8,128)(2,1)}), bf16[8,8,48,256]{3,2,1,0:T(8,128)(2,1)S(1)}, u32[]{:S(2)}, u32[]{:S(2)}) %all-to-all-start.3) | async-done | bytes 1572896 | tf_op jit(solution)/shard_map/all_to_all | solution.py:45
  96.8 3.4 %collective-permute-start.2 = (bf16[384,512]{1,0:T(8,128)(2,1)}, bf16[384,512]{1,0:T(8,128)(2,1)}, u32[]{:S(2)}, u32[]{:S(2)}) collective-permute-start(bf16[384,512]{1,0:T(8,128)(2,1)} %pad_maximum_fusion.refs_0_), channel_id=1, source_target_pairs={{0,1},{1,2},{2,3},{3,0},{4,5},{5,6},{6,7},{7,4},{8,9},{9,10},{10,1... | collective-permute-start | bytes 1179656 | tf_op jit(solution)/shard_map/ppermute | solution.py:75
  102.1 4.6 %collective-permute-start.4 = (bf16[384,512]{1,0:T(8,128)(2,1)}, bf16[384,512]{1,0:T(8,128)(2,1)}, u32[]{:S(2)}, u32[]{:S(2)}) collective-permute-start(bf16[384,512]{1,0:T(8,128)(2,1)} %pad_maximum_fusion.refs_0_), channel_id=1, source_target_pairs={{0,3},{1,0},{2,1},{3,2},{4,7},{5,4},{6,5},{7,6},{8,11},{9,8},{10,9... | collective-permute-start | bytes 1179656 | tf_op jit(solution)/shard_map/ppermute | solution.py:75
  106.7 13.4 %collective-permute-done.2.refs_1_ = bf16[384,512]{1,0:T(8,128)(2,1)} collective-permute-done((bf16[384,512]{1,0:T(8,128)(2,1)}, bf16[384,512]{1,0:T(8,128)(2,1)}, u32[]{:S(2)}, u32[]{:S(2)}) %collective-permute-start.2) | collective-permute-done | bytes 393248 | tf_op jit(solution)/shard_map/ppermute | solution.py:75
  120.1 2.5 %collective-permute-done.4.refs_3_ = bf16[384,512]{1,0:T(8,128)(2,1)} collective-permute-done((bf16[384,512]{1,0:T(8,128)(2,1)}, bf16[384,512]{1,0:T(8,128)(2,1)}, u32[]{:S(2)}, u32[]{:S(2)}) %collective-permute-start.4) | collective-permute-done | bytes 393248 | tf_op jit(solution)/shard_map/ppermute | solution.py:75
  122.7 2.4 %shard_map.73.xs = bf16[4,384,512]{2,1,0:T(8,128)(2,1)S(1)} custom-call(bf16[384,512]{1,0:T(8,128)(2,1)} %pad_maximum_fusion.refs_0_, bf16[384,512]{1,0:T(8,128)(2,1)} %collective-permute-done.2.refs_1_, bf16[384,512]{1,0:T(8,128)(2,1)} %collective-permute-done.3.refs_2_, bf16[384,512]{1,0:T(8,128)(2,1)} %collective-permute-done.4.refs_3_, ...), custom_call_target="tpu_custom_call" | custom-call | flops 4194304 | bytes 1048576 | tf_op jit(solution)/shard_map/pallas_call | solution.py:281
  125.1 2.6 %shard_map.75 = (bf16[384,256]{1,0:T(8,128)(2,1)S(1)}, bf16[4,2,8,2,16,256]{5,4,3,2,1,0:T(8,128)(2,1)S(1)}) custom-call(bf16[4,384,512]{2,1,0:T(8,128)(2,1)S(1)} %shard_map.73.xs, bf16[8,8,48,256]{3,2,1,0:T(8,128)(2,1)S(1)} %all-to-all-done.1.mine, bf16[8,8,48,256]{3,2,1,0:T(8,128)(2,1)} %collective-permute-done.5.other), custom_call_target="tpu_custom_call" | custom-call | flops 536870912 | bytes 1048576 | tf_op jit(solution)/shard_map/pallas_call | solution.py:281
  127.7 3.4 %shard_map.76.refs_0_ = bf16[272,256]{1,0:T(8,128)(2,1)S(1)} custom-call(bf16[384,256]{1,0:T(8,128)(2,1)S(1)} %get-tuple-element.14.refs_0_, f32[2,128,256]{2,1,0:T(8,128)S(1)} %copy-done.1, f32[2,256]{1,0:T(2,128)S(1)} %copy-done.3), custom_call_target="tpu_custom_call" | custom-call | flops 16777216 | bytes 1048576 | tf_op jit(solution)/shard_map/pallas_call | solution.py:281
  131.1 3.1 %collective-permute-start.6 = (bf16[272,256]{1,0:T(8,128)(2,1)S(1)}, bf16[272,256]{1,0:T(8,128)(2,1)S(1)}, u32[]{:S(2)}, u32[]{:S(2)}) collective-permute-start(bf16[272,256]{1,0:T(8,128)(2,1)S(1)} %shard_map.76.refs_0_), channel_id=1, source_target_pairs={{0,1},{1,2},{2,3},{3,0},{4,5},{5,6},{6,7},{7,4},{8,9},{9,10},{10,1... | collective-permute-start | bytes 417800 | tf_op jit(solution)/shard_map/ppermute | solution.py:75
  134.2 4.8 %collective-permute-start.7 = (bf16[272,256]{1,0:T(8,128)(2,1)S(1)}, bf16[272,256]{1,0:T(8,128)(2,1)S(1)}, u32[]{:S(2)}, u32[]{:S(2)}) collective-permute-start(bf16[272,256]{1,0:T(8,128)(2,1)S(1)} %shard_map.76.refs_0_), channel_id=1, source_target_pairs={{0,2},{1,3},{2,0},{3,1},{4,6},{5,7},{6,4},{7,5},{8,10},{9,11},{10,... | collective-permute-start | bytes 417800 | tf_op jit(solution)/shard_map/ppermute | solution.py:75
  146.0 2.6 %shard_map.77 = (bf16[256,512]{1,0:T(8,128)(2,1)S(1)}, bf16[4,256,512]{2,1,0:T(8,128)(2,1)}) custom-call(bf16[272,256]{1,0:T(8,128)(2,1)S(1)} %shard_map.76.refs_0_, bf16[272,256]{1,0:T(8,128)(2,1)S(1)} %collective-permute-done.6.refs_1_, bf16[272,256]{1,0:T(8,128)(2,1)S(1)} %collective-permute-done.7.refs_2_, ...), custom_call_target="tpu_custom_call" | custom-call | flops 268435456 | bytes 1048576 | tf_op jit(solution)/shard_map/pallas_call | solution.py:387
  148.6 17.7 %all_to_all.21.refs_0_ = bf16[4,256,512]{2,1,0:T(8,128)(2,1)S(1)} all-to-all(bf16[4,256,512]{2,1,0:T(8,128)(2,1)} %get-tuple-element.16), channel_id=1, replica_groups=mesh['sp'=128,'tp'=4] {'tp'}, dimensions={0} | all-to-all | bytes 2097152 | tf_op jit(solution)/shard_map/all_to_all | solution.py:429
  167.0 2.3 %shard_map.80 = (bf16[256,256]{1,0:T(8,128)(2,1)S(1)}, bf16[4,2,8,2,16,256]{5,4,3,2,1,0:T(8,128)(2,1)S(1)}) custom-call(bf16[4,256,512]{2,1,0:T(8,128)(2,1)S(1)} %shard_map.78.xs, bf16[8,8,48,256]{3,2,1,0:T(8,128)(2,1)S(1)} %all-to-all-done.3.mine, bf16[8,8,48,256]{3,2,1,0:T(8,128)(2,1)} %collective-permute-done.9.other), custom_call_target="tpu_custom_call" | custom-call | flops 536870912 | bytes 1048576 | tf_op jit(solution)/shard_map/pallas_call | solution.py:281
  172.9 4.2 %collective-permute-done.10.refs_0_ = bf16[128,256]{1,0:T(8,128)(2,1)S(1)} collective-permute-done((bf16[128,256]{1,0:T(8,128)(2,1)S(1)}, bf16[128,256]{1,0:T(8,128)(2,1)S(1)}, u32[]{:S(2)}, u32[]{:S(2)}) %collective-permute-start.10) | collective-permute-done | bytes 65568 | tf_op jit(solution)/shard_map/ppermute | solution.py:433
  179.0 2.5 %collective-permute-start.11 = (bf16[272,256]{1,0:T(8,128)(2,1)S(1)}, bf16[272,256]{1,0:T(8,128)(2,1)S(1)}, u32[]{:S(2)}, u32[]{:S(2)}) collective-permute-start(bf16[272,256]{1,0:T(8,128)(2,1)S(1)} %shard_map.82.refs_0_), channel_id=1, source_target_pairs={{0,1},{1,2},{2,3},{3,0},{4,5},{5,6},{6,7},{7,4},{8,9},{9,10},{10,1... | collective-permute-start | bytes 417800 | tf_op jit(solution)/shard_map/ppermute | solution.py:75
  181.5 4.0 %collective-permute-start.12 = (bf16[272,256]{1,0:T(8,128)(2,1)S(1)}, bf16[272,256]{1,0:T(8,128)(2,1)S(1)}, u32[]{:S(2)}, u32[]{:S(2)}) collective-permute-start(bf16[272,256]{1,0:T(8,128)(2,1)S(1)} %shard_map.82.refs_0_), channel_id=1, source_target_pairs={{0,2},{1,3},{2,0},{3,1},{4,6},{5,7},{6,4},{7,5},{8,10},{9,11},{10,... | collective-permute-start | bytes 417800 | tf_op jit(solution)/shard_map/ppermute | solution.py:75
  185.5 2.7 %collective-permute-start.13 = (bf16[272,256]{1,0:T(8,128)(2,1)S(1)}, bf16[272,256]{1,0:T(8,128)(2,1)S(1)}, u32[]{:S(2)}, u32[]{:S(2)}) collective-permute-start(bf16[272,256]{1,0:T(8,128)(2,1)S(1)} %shard_map.82.refs_0_), channel_id=1, source_target_pairs={{0,3},{1,0},{2,1},{3,2},{4,7},{5,4},{6,5},{7,6},{8,11},{9,8},{10,9... | collective-permute-start | bytes 417800 | tf_op jit(solution)/shard_map/ppermute | solution.py:75
  189.9 2.5 %collective-permute-done.13.refs_3_ = bf16[272,256]{1,0:T(8,128)(2,1)S(1)} collective-permute-done((bf16[272,256]{1,0:T(8,128)(2,1)S(1)}, bf16[272,256]{1,0:T(8,128)(2,1)S(1)}, u32[]{:S(2)}, u32[]{:S(2)}) %collective-permute-start.13) | collective-permute-done | bytes 139296 | tf_op jit(solution)/shard_map/ppermute | solution.py:75
  192.4 2.3 %shard_map.83 = bf16[256,512]{1,0:T(8,128)(2,1)} custom-call(bf16[272,256]{1,0:T(8,128)(2,1)S(1)} %shard_map.82.refs_0_, bf16[272,256]{1,0:T(8,128)(2,1)S(1)} %collective-permute-done.11.refs_1_, bf16[272,256]{1,0:T(8,128)(2,1)S(1)} %collective-permute-done.12.refs_2_, bf16[272,256]{1,0:T(8,128)(2,1)S(1)} %collective-permute-done.13.refs_3_, ...), custom_call_target="tpu_custom_call" | custom-call | flops 268435456 | bytes 1048576 | tf_op jit(solution)/shard_map/pallas_call | solution.py:387
  (39 shorter events, 27.8 us)
Async XLA Ops:
  0.0 2.8 %collective-permute-start.1 = (bf16[2,16,256]{2,1,0:T(8,128)(2,1)}, bf16[2,16,256]{2,1,0:T(8,128)(2,1)S(1)}, u32[]{:S(2)}, u32[]{:S(2)}) collective-permute-start(bf16[2,16,256]{2,1,0:T(8,128)(2,1)} %bitcast.1), channel_id=1, source_target_pairs={{0,0},{1,128},{2,256},{3,384},{4,4},{5,20},{6,36},{7,52},{8,8},{9,... | collective-permute-start | bytes 49160 | tf_op jit(solution)/shard_map/ppermute | solution.py:70
  22.9 42.3 %all-to-all-start.1 = ((bf16[8,8,48,256]{3,2,1,0:T(8,128)(2,1)}), bf16[8,8,48,256]{3,2,1,0:T(8,128)(2,1)S(1)}, u32[]{:S(2)}, u32[]{:S(2)}) async-start(bf16[8,8,48,256]{3,2,1,0:T(8,128)(2,1)} %shard_map.74), calls=%async_computation.1 | async-start | bytes 3145728 | tf_op jit(solution)/shard_map/all_to_all | solution.py:45
  42.5 1.1 copy-start
  43.7 28.4 %copy-start.2 = (bf16[256,512]{1,0:T(8,128)(2,1)S(1)}, bf16[256,512]{1,0:T(8,128)(2,1)}, u32[]{:S(2)}) copy-start(bf16[256,512]{1,0:T(8,128)(2,1)} %refs_4_.2) | copy-start | bytes 786436
  43.7 63.0 %copy-start.4 = (f32[2,2048]{1,0:T(2,128)S(1)}, f32[2,2048]{1,0:T(2,128)}, u32[]{:S(2)}) copy-start(f32[2,2048]{1,0:T(2,128)} %param.8) | copy-start | bytes 49156
  65.1 28.0 %all-to-all-start.3 = ((bf16[8,8,48,256]{3,2,1,0:T(8,128)(2,1)}), bf16[8,8,48,256]{3,2,1,0:T(8,128)(2,1)S(1)}, u32[]{:S(2)}, u32[]{:S(2)}) async-start(bf16[8,8,48,256]{3,2,1,0:T(8,128)(2,1)} %copy-done), calls=%async_computation.3 | async-start | bytes 3145728 | tf_op jit(solution)/shard_map/all_to_all | solution.py:45
  70.2 54.9 %collective-permute-start.5 = (bf16[8,8,48,256]{3,2,1,0:T(8,128)(2,1)S(1)}, bf16[8,8,48,256]{3,2,1,0:T(8,128)(2,1)}, u32[]{:S(2)}, u32[]{:S(2)}) collective-permute-start(bf16[8,8,48,256]{3,2,1,0:T(8,128)(2,1)S(1)} %all-to-all-done.1.mine), channel_id=1, source_target_pairs={{0,4},{4,0},{8,12},{12,8},{16,20},{20,16},{24,28},{28,24},{32,36},... | collective-permute-start | bytes 4718600 | tf_op jit(solution)/shard_map/ppermute | solution.py:57
  72.1 23.0 %collective-permute-start = (bf16[128,512]{1,0:T(8,128)(2,1)S(1)}, bf16[128,512]{1,0:T(8,128)(2,1)}, u32[]{:S(2)}, u32[]{:S(2)}) collective-permute-start(bf16[128,512]{1,0:T(8,128)(2,1)S(1)} %slice.6), channel_id=1, source_target_pairs={{0,4},{4,8},{8,12},{12,16},{16,20},{20,24},{24,28},{28,32},{32,36}... | collective-permute-start | bytes 393224 | tf_op jit(solution)/shard_map/ppermute | solution.py:415
  93.2 73.8 %collective-permute-start.9 = (bf16[8,8,48,256]{3,2,1,0:T(8,128)(2,1)S(1)}, bf16[8,8,48,256]{3,2,1,0:T(8,128)(2,1)}, u32[]{:S(2)}, u32[]{:S(2)}) collective-permute-start(bf16[8,8,48,256]{3,2,1,0:T(8,128)(2,1)S(1)} %all-to-all-done.3.mine), channel_id=1, source_target_pairs={{0,4},{4,0},{8,12},{12,8},{16,20},{20,16},{24,28},{28,24},{32,36},... | collective-permute-start | bytes 4718600 | tf_op jit(solution)/shard_map/ppermute | solution.py:57
  96.8 23.4 %collective-permute-start.2 = (bf16[384,512]{1,0:T(8,128)(2,1)}, bf16[384,512]{1,0:T(8,128)(2,1)}, u32[]{:S(2)}, u32[]{:S(2)}) collective-permute-start(bf16[384,512]{1,0:T(8,128)(2,1)} %pad_maximum_fusion.refs_0_), channel_id=1, source_target_pairs={{0,1},{1,2},{2,3},{3,0},{4,5},{5,6},{6,7},{7,4},{8,9},{9,10},{10,1... | collective-permute-start | bytes 1179656 | tf_op jit(solution)/shard_map/ppermute | solution.py:75
  100.2 19.9 %collective-permute-start.3 = (bf16[384,512]{1,0:T(8,128)(2,1)}, bf16[384,512]{1,0:T(8,128)(2,1)}, u32[]{:S(2)}, u32[]{:S(2)}) collective-permute-start(bf16[384,512]{1,0:T(8,128)(2,1)} %pad_maximum_fusion.refs_0_), channel_id=1, source_target_pairs={{0,2},{1,3},{2,0},{3,1},{4,6},{5,7},{6,4},{7,5},{8,10},{9,11},{10,... | collective-permute-start | bytes 1179656 | tf_op jit(solution)/shard_map/ppermute | solution.py:75
  102.1 20.5 %collective-permute-start.4 = (bf16[384,512]{1,0:T(8,128)(2,1)}, bf16[384,512]{1,0:T(8,128)(2,1)}, u32[]{:S(2)}, u32[]{:S(2)}) collective-permute-start(bf16[384,512]{1,0:T(8,128)(2,1)} %pad_maximum_fusion.refs_0_), channel_id=1, source_target_pairs={{0,3},{1,0},{2,1},{3,2},{4,7},{5,4},{6,5},{7,6},{8,11},{9,8},{10,9... | collective-permute-start | bytes 1179656 | tf_op jit(solution)/shard_map/ppermute | solution.py:75
  125.0 2.7 %copy-start.1 = (f32[2,128,256]{2,1,0:T(8,128)S(1)}, f32[2,128,256]{2,1,0:T(8,128)}, u32[]{:S(2)}) copy-start(f32[2,128,256]{2,1,0:T(8,128)} %refs_3_.1) | copy-start | bytes 786436
  125.0 2.7 %copy-start.3 = (f32[2,256]{1,0:T(2,128)S(1)}, f32[2,256]{1,0:T(2,128)}, u32[]{:S(2)}) copy-start(f32[2,256]{1,0:T(2,128)} %refs_4_.3) | copy-start | bytes 6148
  131.1 10.2 %collective-permute-start.6 = (bf16[272,256]{1,0:T(8,128)(2,1)S(1)}, bf16[272,256]{1,0:T(8,128)(2,1)S(1)}, u32[]{:S(2)}, u32[]{:S(2)}) collective-permute-start(bf16[272,256]{1,0:T(8,128)(2,1)S(1)} %shard_map.76.refs_0_), channel_id=1, source_target_pairs={{0,1},{1,2},{2,3},{3,0},{4,5},{5,6},{6,7},{7,4},{8,9},{9,10},{10,1... | collective-permute-start | bytes 417800 | tf_op jit(solution)/shard_map/ppermute | solution.py:75
  134.2 9.5 %collective-permute-start.7 = (bf16[272,256]{1,0:T(8,128)(2,1)S(1)}, bf16[272,256]{1,0:T(8,128)(2,1)S(1)}, u32[]{:S(2)}, u32[]{:S(2)}) collective-permute-start(bf16[272,256]{1,0:T(8,128)(2,1)S(1)} %shard_map.76.refs_0_), channel_id=1, source_target_pairs={{0,2},{1,3},{2,0},{3,1},{4,6},{5,7},{6,4},{7,5},{8,10},{9,11},{10,... | collective-permute-start | bytes 417800 | tf_op jit(solution)/shard_map/ppermute | solution.py:75
  139.0 7.0 %collective-permute-start.8 = (bf16[272,256]{1,0:T(8,128)(2,1)S(1)}, bf16[272,256]{1,0:T(8,128)(2,1)S(1)}, u32[]{:S(2)}, u32[]{:S(2)}) collective-permute-start(bf16[272,256]{1,0:T(8,128)(2,1)S(1)} %shard_map.76.refs_0_), channel_id=1, source_target_pairs={{0,3},{1,0},{2,1},{3,2},{4,7},{5,4},{6,5},{7,6},{8,11},{9,8},{10,9... | collective-permute-start | bytes 417800 | tf_op jit(solution)/shard_map/ppermute | solution.py:75
  169.4 7.7 %collective-permute-start.10 = (bf16[128,256]{1,0:T(8,128)(2,1)S(1)}, bf16[128,256]{1,0:T(8,128)(2,1)S(1)}, u32[]{:S(2)}, u32[]{:S(2)}) collective-permute-start(bf16[128,256]{1,0:T(8,128)(2,1)S(1)} %slice.7), channel_id=1, source_target_pairs={{0,4},{4,8},{8,12},{12,16},{16,20},{20,24},{24,28},{28,32},{32,36}... | collective-permute-start | bytes 196616 | tf_op jit(solution)/shard_map/ppermute | solution.py:433
  179.0 9.2 %collective-permute-start.11 = (bf16[272,256]{1,0:T(8,128)(2,1)S(1)}, bf16[272,256]{1,0:T(8,128)(2,1)S(1)}, u32[]{:S(2)}, u32[]{:S(2)}) collective-permute-start(bf16[272,256]{1,0:T(8,128)(2,1)S(1)} %shard_map.82.refs_0_), channel_id=1, source_target_pairs={{0,1},{1,2},{2,3},{3,0},{4,5},{5,6},{6,7},{7,4},{8,9},{9,10},{10,1... | collective-permute-start | bytes 417800 | tf_op jit(solution)/shard_map/ppermute | solution.py:75
  181.5 8.5 %collective-permute-start.12 = (bf16[272,256]{1,0:T(8,128)(2,1)S(1)}, bf16[272,256]{1,0:T(8,128)(2,1)S(1)}, u32[]{:S(2)}, u32[]{:S(2)}) collective-permute-start(bf16[272,256]{1,0:T(8,128)(2,1)S(1)} %shard_map.82.refs_0_), channel_id=1, source_target_pairs={{0,2},{1,3},{2,0},{3,1},{4,6},{5,7},{6,4},{7,5},{8,10},{9,11},{10,... | collective-permute-start | bytes 417800 | tf_op jit(solution)/shard_map/ppermute | solution.py:75
  185.5 6.9 %collective-permute-start.13 = (bf16[272,256]{1,0:T(8,128)(2,1)S(1)}, bf16[272,256]{1,0:T(8,128)(2,1)S(1)}, u32[]{:S(2)}, u32[]{:S(2)}) collective-permute-start(bf16[272,256]{1,0:T(8,128)(2,1)S(1)} %shard_map.82.refs_0_), channel_id=1, source_target_pairs={{0,3},{1,0},{2,1},{3,2},{4,7},{5,4},{6,5},{7,6},{8,11},{9,8},{10,9... | collective-permute-start | bytes 417800 | tf_op jit(solution)/shard_map/ppermute | solution.py:75

commit v4 on v3

--- a/solution.py
+++ b/solution.py
@@ -70,10 +70,16 @@
     return lax.ppermute(v, ("sp", "x"), pairs)
 
 
+def along_x(v, step):
+    return lax.ppermute(v, "x", [(i, (i + step) % NX) for i in range(NX)])
+
+
 def from_all_x(v):
-    return [v] + [
-        lax.ppermute(v, "x", [(i, (i + step) % NX) for i in range(NX)]) for step in range(1, NX)
-    ]
+    return [v] + [along_x(v, step) for step in range(1, NX)]
+
+
+def exchange_x(copies):
+    return [lax.all_to_all(copies, "x", split_axis=0, concat_axis=0, tiled=True)]
 
 
 def part_of(refs, k):
@@ -87,7 +93,7 @@
 
 
 def norm_kernel(layer, n, *refs):
-    parts, (gain, xs, scale) = refs[:n], refs[n:]
+    parts, (gain, out, scale, xs, sem) = refs[:n], refs[n:]
 
     def squares(i, _):
         rows = pl.ds(pl.multiple_of(i * 16, 16), 16)
@@ -114,17 +120,20 @@
         return 0
 
     lax.fori_loop(0, steps, apply, 0, unroll=2)
-
-
-def mix_kernel(xs, mine, other, glu, wt, vs, gs):
+    done = pltpu.make_async_copy(xs, out, sem)
+    done.start()
+    done.wait()
+
+
+def mix_kernel(source, mine, other, glu, vs, gs, xs, sem):
+    fetch = pltpu.make_async_copy(source, xs, sem)
+    fetch.start()
+
     def fill(zy, yz):
         for z in range(NZ):
             for c, w in enumerate((zy.at[z], yz.at[:, z])):
                 vs[z, :, c] = w[:, :16, :]
                 gs[z, :, c] = w[:, 16:32, :]
-        for k in range(NX):
-            for c, w in enumerate((zy, yz)):
-                wt[k, :, :, c] = w[2 * k : 2 * k + 2, :, 32:, :]
 
     @pl.when(core_here() == 0)
     def _():
@@ -134,6 +143,7 @@
     def _():
         fill(other, mine)
 
+    fetch.wait()
     value = jnp.zeros(glu.shape, F32)
     gate = jnp.zeros(glu.shape, F32)
     for k in range(NX):
@@ -203,20 +213,22 @@
     taps_over(layer, ext, taps, conv, shifted)
 
 
-def conv_kernel(layer, before, glu, late, taps, gain, out, ext, shifted, conv):
+def conv_kernel(layer, before, glu, late, taps, gain, out, ext, shifted, conv, packed, sems):
     ext[:TAPS, :] = before[...].astype(F32)
     ext[TAPS:, :] = glu[:HALF, :].astype(F32)
     taps_over(layer, ext, taps, conv.at[:HALF], shifted)
     conv[HALF:, :] = late[...]
-    pack(layer, conv, gain, out)
+    pack(layer, conv, gain, packed)
+    send_all(packed, out, sems)
 
 
 def out_kernel(n, *refs):
     parts, rest = refs[:n], refs[n:]
-    x, wt, out, *rest = rest
-    copies = rest[0] if len(rest) == 6 else None
-    means, scale, acts, held, sems = rest[-5:]
-    fetch = pltpu.make_async_copy(x, held, sems.at[0])
+    x, source, out, means, scale, acts, held, wt, sems = rest
+    weights = pltpu.make_async_copy(source, wt, sems.at[1])
+    weights.start()
+    mine = x if len(x.shape) == 2 else x.at[lax.axis_index("x")]
+    fetch = pltpu.make_async_copy(mine, held, sems.at[0])
     fetch.start()
     pick = (lax.broadcasted_iota(jnp.int32, (16, 128), 0) < 3).astype(BF)
     total = jnp.zeros((TOK, 128), F32)
@@ -264,6 +276,7 @@
         return 0
 
     lax.fori_loop(0, TOK // 16, activate, 0, unroll=2)
+    weights.wait()
     branch = jnp.zeros((TOK, FEAT), F32)
     for k in range(NX):
         branch += lax.dot_general(
@@ -271,23 +284,33 @@
             preferred_element_type=F32,
         )
     fetch.wait()
-    out[...] = (held[...].astype(F32) + branch).astype(BF)
-    if copies is not None:
-        send_all(out, copies, sems)
-
-
-def call(body, out, ins, scratch, flops, place=pltpu.VMEM):
+    new = (held[...].astype(F32) + branch).astype(BF)
+    if len(out.shape) == 2:
+        out[...] = new
+    else:
+        held[...] = new
+        send_all(held, out, sems)
+
+
+def in_hbm(v):
+    return v if INTERPRET else pltpu.with_memory_space_constraint(v, pltpu.HBM)
+
+
+def call(body, out, ins, scratch, flops, place=pltpu.VMEM, loose=(), far=()):
+    def spot(i):
+        return pltpu.HBM if i in far else pl.ANY if i in loose else pltpu.VMEM
+
     spec = pl.BlockSpec(memory_space=place)
     return pl.pallas_call(
         body,
         out_shape=out,
-        in_specs=[pl.BlockSpec(memory_space=pltpu.VMEM)] * len(ins),
-        out_specs=(spec,) * len(out) if isinstance(out, tuple) else spec,
+        in_specs=[pl.BlockSpec(memory_space=spot(i)) for i in range(len(ins))],
+        out_specs=spec,
         scratch_shapes=scratch,
         cost_estimate=pl.CostEstimate(flops=flops, transcendentals=0, bytes_accessed=1 << 20),
         compiler_params=pltpu.CompilerParams(vmem_limit_bytes=14 << 20),
         interpret=INTERPRET,
-    )(*ins)
+    )(*(in_hbm(v) if i in far else v for i, v in enumerate(ins)))
 
 
 def normalise(layer, parts, gain):
@@ -296,23 +319,62 @@
 
     return call(
         body,
-        jax.ShapeDtypeStruct((NX, parts[0].shape[-2], FEAT), BF),
+        pltpu.HBM((NX, parts[0].shape[-2], FEAT), BF),
         [*parts, gain],
-        [pltpu.VMEM((parts[0].shape[-2], 128), F32)],
+        [
+            pltpu.VMEM((parts[0].shape[-2], 128), F32),
+            pltpu.VMEM((NX, parts[0].shape[-2], FEAT), BF),
+            pltpu.SemaphoreType.DMA(()),
+        ],
         8 * NX * TOK * FEAT,
+        pltpu.HBM,
     )
 
 
 def mix(xs, mine, other):
+    weights = pltpu.VMEM((NZ, NY, 2, 16, CH), BF)
     return call(
         mix_kernel,
-        (
-            jax.ShapeDtypeStruct((xs.shape[1], CH), BF),
-            jax.ShapeDtypeStruct((NX, 2, NY, 2, 16, CH), BF),
-        ),
+        jax.ShapeDtypeStruct((xs.shape[1], CH), BF),
         [xs, mine, other],
-        [pltpu.VMEM((NZ, NY, 2, 16, CH), BF), pltpu.VMEM((NZ, NY, 2, 16, CH), BF)],
+        [weights, weights, pltpu.VMEM(xs.shape, BF), pltpu.SemaphoreType.DMA(())],
         4 * NX * TOK * FEAT * CH,
+        far=(0,),
+    )
+
+
+def arrange_kernel(mine, other, wt, sems):
+    def fill(halves):
+        copies = []
+        for k in range(NX):
+            for c, w in enumerate(halves):
+                part = w.at[2 * k : 2 * k + 2, :, 32:, :]
+                copies.append(
+                    pltpu.make_async_copy(part, wt.at[k, :, :, c], sems.at[2 * k + c])
+                )
+        for one in copies:
+            one.start()
+        for one in copies:
+            one.wait()
+
+    @pl.when(core_here() == 0)
+    def _():
+        fill((mine, other))
+
+    @pl.when(core_here() == 1)
+    def _():
+        fill((other, mine))
+
+
+def arrange(mine, other):
+    return call(
+        arrange_kernel,
+        pltpu.HBM((NX, 2, NY, 2, 16, CH), BF),
+        [mine, other],
+        [pltpu.SemaphoreType.DMA((2 * NX,))],
+        1 << 26,
+        pltpu.HBM,
+        (0, 1),
     )
 
 
@@ -352,14 +414,17 @@
 
     return call(
         body,
-        jax.ShapeDtypeStruct((PACK, CH), BF),
+        pltpu.HBM((NX, PACK, CH), BF),
         [before, glu, late, taps, gain],
         [
             pltpu.VMEM((TAPS + HALF, CH), F32),
             pltpu.VMEM((8, SPAN, CH), F32),
             pltpu.VMEM((TOK, CH), F32),
+            pltpu.VMEM((PACK, CH), BF),
+            pltpu.SemaphoreType.DMA((NX,)),
         ],
         2 * HALF * CH * TAPS,
+        pltpu.HBM,
     )
 
 
@@ -383,17 +448,18 @@
 
     shape = jax.ShapeDtypeStruct((TOK, FEAT), BF)
     copies = pltpu.HBM((NX, TOK, FEAT), BF)
-    inside, anywhere = pl.BlockSpec(memory_space=pltpu.VMEM), pl.BlockSpec(memory_space=pl.ANY)
+    inside, far = pl.BlockSpec(memory_space=pltpu.VMEM), pl.BlockSpec(memory_space=pltpu.HBM)
     return pl.pallas_call(
         body,
-        out_shape=(shape, copies) if to_all else shape,
-        in_specs=[inside] * len(parts) + [anywhere, inside],
-        out_specs=(inside, pl.BlockSpec(memory_space=pltpu.HBM)) if to_all else inside,
+        out_shape=copies if to_all else shape,
+        in_specs=[inside] * len(parts) + [far, far],
+        out_specs=far if to_all else inside,
         scratch_shapes=[
             pltpu.VMEM((NX, TOK, 128), F32),
             pltpu.VMEM((TOK, 128), F32),
             pltpu.VMEM((NX, TOK, CH), BF),
             pltpu.VMEM((TOK, FEAT), BF),
+            pltpu.VMEM(wt.shape, BF),
             pltpu.SemaphoreType.DMA((NX,)),
         ],
         cost_estimate=pl.CostEstimate(
@@ -401,7 +467,7 @@
         ),
         compiler_params=pltpu.CompilerParams(vmem_limit_bytes=14 << 20),
         interpret=INTERPRET,
-    )(*parts, x, wt)
+    )(*parts, in_hbm(x), in_hbm(wt))
 
 
 def shards(stream, norm_gain, w_value, w_gate, conv_taps, channel_gain, w_out):
@@ -414,27 +480,31 @@
     chain = [(i, i + 1) for i in range(count - 1)]
     extended = jnp.concatenate([lax.ppermute(x[TOK - TAPS :], "sp", chain), x])
     once = lines(blocks)
-    parts = from_all_x(after(extended, blocks))
+    extended = after(extended, blocks)
+    parts = [extended, along_x(extended, 1), along_x(extended, 2)]
+    parts.append(along_x(extended, 3))
     ready = spread(0, once)
     gathered = plane(ready)
     ready = spread(1, once)
     normed = normalise(0, parts, gain)
     other = swap_cores(gathered)
     following = plane(after(ready, gathered))
-    glu, wt = mix(normed, gathered, other)
+    glu = mix(normed, gathered, other)
     packed = conv_whole(0, glu, conv_taps, channel_gain)
     parts = from_all_x(packed)
-    x, copies = project(parts, x, wt, True)
-
-    parts = [lax.all_to_all(copies, "x", split_axis=0, concat_axis=0, tiled=True)]
+    wt = arrange(after(gathered, packed), other)
+    copies = project(parts, x, wt, True)
+
+    xs = exchange_x(copies)
     other = swap_cores(following)
-    normed = normalise(1, parts, gain)
-    glu, wt = mix(normed, following, other)
+    normed = normalise(1, xs, gain)
+    glu = mix(normed, following, other)
     before = lax.ppermute(glu[TOK - TAPS :], "sp", chain)
     late = conv_late(1, glu, conv_taps)
-    packed = convolve(1, before, glu, late, conv_taps, channel_gain)
-    parts = from_all_x(packed)
-    x = project(parts, x, wt, False)
+    copies = convolve(1, before, glu, late, conv_taps, channel_gain)
+    parts = exchange_x(copies)
+    wt = arrange(after(following, copies), other)
+    x = project(parts, xs[0], wt, False)
     return x
 
 

time: 196 us -> 221 us (1.13)
  the two profiles are of different devices: /device:TPU:64 before, /device:TPU:66 now
where the time goes in v4:
time: 221 us; the launch traced here: 220 us
  waiting for transfers between devices  61 us (28%)
  Pallas kernels  60.9 us (28%)
  starting transfers between devices  57.3 us (26%)
  blocking collectives  35.9 us (16%)
  local copies, waits for them, and re-layouts  3.42 us (2%)
    pallas_call x11, Pallas kernels, call(): pl.pallas_call(body, out_shape=out, in_specs=[pl.BlockSpec(memory_space=s...  55.7 us
    all_to_all x2, waiting for transfers between devices, plane(): lax.all_to_all(copies, 'sp', split_axis=0, concat_axis=0, tiled=True, axi...  40.1 us
    all_to_all x2, starting transfers between devices, plane(): lax.all_to_all(copies, 'sp', split_axis=0, concat_axis=0, tiled=True, axi...  19.2 us
    ppermute x6, starting transfers between devices, along_x(): return lax.ppermute(v, 'x', [(i, (i + step) % NX) for i in range(NX)])  19 us
    all_to_all x1, blocking collectives, to_group(): lax.all_to_all(copies, 'sp', split_axis=0, concat_axis=0, tiled=True, axi...  18.8 us
    all_to_all x1, blocking collectives, exchange_x(): lax.all_to_all(copies, 'x', split_axis=0, concat_axis=0, tiled=True)  17.1 us
    ppermute x6, waiting for transfers between devices, along_x(): return lax.ppermute(v, 'x', [(i, (i + step) % NX) for i in range(NX)])  16.3 us
    ppermute x1, starting transfers between devices, to_column_owner(): return lax.ppermute(v, ('sp', 'x'), pairs)  6.05 us
  transfers between devices with their start and end apart: 14, of which 7 were waited for; matrix products, arithmetic and copies ran while one was open for 1% of the time, Pallas kernels for 23%

profile of v4, /device:TPU:66, one launch (start us, length us, event | category | flops | bytes accessed | tf_op | source)
XLA Modules:
  0.0 219.8 jit_solution(1031185944609674394)
XLA Ops:
  0.0 6.0 %collective-permute-start.1 = (bf16[2,16,256]{2,1,0:T(8,128)(2,1)}, bf16[2,16,256]{2,1,0:T(8,128)(2,1)S(1)}, u32[]{:S(2)}, u32[]{:S(2)}) collective-permute-start(bf16[2,16,256]{2,1,0:T(8,128)(2,1)} %bitcast.1), channel_id=1, source_target_pairs={{0,0},{1,128},{2,256},{3,384},{4,4},{5,20},{6,36},{7,52},{8,8},{9,... | collective-permute-start | bytes 49160 | tf_op jit(solution)/shard_map/ppermute | solution.py:70
  8.0 18.8 %all_to_all.25.refs_0_ = bf16[8,2,48,256]{3,2,1,0:T(8,128)(2,1)S(1)} all-to-all(bf16[8,2,48,256]{3,2,1,0:T(8,128)(2,1)S(1)} %broadcast_in_dim.3), channel_id=1, replica_groups={{0,8,16,24,32,40,48,56},{64,72,80,88,96,104,112,120},{128,136,144,152,1..., dimensions={0} | all-to-all | bytes 786432 | tf_op jit(solution)/shard_map/all_to_all | solution.py:35
  28.0 14.1 %all-to-all-start.1 = ((bf16[8,8,48,256]{3,2,1,0:T(8,128)(2,1)}), bf16[8,8,48,256]{3,2,1,0:T(8,128)(2,1)S(1)}, u32[]{:S(2)}, u32[]{:S(2)}) async-start(bf16[8,8,48,256]{3,2,1,0:T(8,128)(2,1)} %shard_map.74), calls=%async_computation.1 | async-start | bytes 3145728 | tf_op jit(solution)/shard_map/all_to_all | solution.py:45
  43.7 21.5 %all-to-all-done.1.mine = bf16[8,8,48,256]{3,2,1,0:T(8,128)(2,1)S(1)} async-done(((bf16[8,8,48,256]{3,2,1,0:T(8,128)(2,1)}), bf16[8,8,48,256]{3,2,1,0:T(8,128)(2,1)S(1)}, u32[]{:S(2)}, u32[]{:S(2)}) %all-to-all-start.1) | async-done | bytes 1572896 | tf_op jit(solution)/shard_map/all_to_all | solution.py:45
  65.1 5.0 %all-to-all-start.3 = ((bf16[8,8,48,256]{3,2,1,0:T(8,128)(2,1)}), bf16[8,8,48,256]{3,2,1,0:T(8,128)(2,1)S(1)}, u32[]{:S(2)}, u32[]{:S(2)}) async-start(bf16[8,8,48,256]{3,2,1,0:T(8,128)(2,1)} %copy-done.1), calls=%async_computation.3 | async-start | bytes 3145728 | tf_op jit(solution)/shard_map/all_to_all | solution.py:45
  74.5 18.6 %all-to-all-done.3.mine = bf16[8,8,48,256]{3,2,1,0:T(8,128)(2,1)S(1)} async-done(((bf16[8,8,48,256]{3,2,1,0:T(8,128)(2,1)}), bf16[8,8,48,256]{3,2,1,0:T(8,128)(2,1)S(1)}, u32[]{:S(2)}, u32[]{:S(2)}) %all-to-all-start.3) | async-done | bytes 1572896 | tf_op jit(solution)/shard_map/all_to_all | solution.py:45
  98.0 4.5 %collective-permute-start.3 = (bf16[384,512]{1,0:T(8,128)(2,1)S(1)}, bf16[384,512]{1,0:T(8,128)(2,1)}, u32[]{:S(2)}, u32[]{:S(2)}) collective-permute-start(bf16[384,512]{1,0:T(8,128)(2,1)S(1)} %pad_maximum_fusion.refs_0_), channel_id=1, source_target_pairs={{0,2},{1,3},{2,0},{3,1},{4,6},{5,7},{6,4},{7,5},{8,10},{9,11},{10,... | collective-permute-start | bytes 1179656 | tf_op jit(solution)/shard_map/ppermute | solution.py:74
  105.2 4.9 %collective-permute-done.2.refs_1_ = bf16[384,512]{1,0:T(8,128)(2,1)} collective-permute-done((bf16[384,512]{1,0:T(8,128)(2,1)S(1)}, bf16[384,512]{1,0:T(8,128)(2,1)}, u32[]{:S(2)}, u32[]{:S(2)}) %collective-permute-start.2) | collective-permute-done | bytes 393248 | tf_op jit(solution)/shard_map/ppermute | solution.py:74
  110.1 3.5 %collective-permute-done.3.refs_2_ = bf16[384,512]{1,0:T(8,128)(2,1)} collective-permute-done((bf16[384,512]{1,0:T(8,128)(2,1)S(1)}, bf16[384,512]{1,0:T(8,128)(2,1)}, u32[]{:S(2)}, u32[]{:S(2)}) %collective-permute-start.3) | collective-permute-done | bytes 393248 | tf_op jit(solution)/shard_map/ppermute | solution.py:74
  113.6 7.9 %collective-permute-done.4.refs_3_ = bf16[384,512]{1,0:T(8,128)(2,1)} collective-permute-done((bf16[384,512]{1,0:T(8,128)(2,1)S(1)}, bf16[384,512]{1,0:T(8,128)(2,1)}, u32[]{:S(2)}, u32[]{:S(2)}) %collective-permute-start.4) | collective-permute-done | bytes 393248 | tf_op jit(solution)/shard_map/ppermute | solution.py:74
  121.5 3.4 %shard_map.73.source = bf16[4,384,512]{2,1,0:T(8,128)(2,1)} custom-call(bf16[384,512]{1,0:T(8,128)(2,1)S(1)} %pad_maximum_fusion.refs_0_, bf16[384,512]{1,0:T(8,128)(2,1)} %collective-permute-done.2.refs_1_, bf16[384,512]{1,0:T(8,128)(2,1)} %collective-permute-done.3.refs_2_, bf16[384,512]{1,0:T(8,128)(2,1)} %collective-permute-done.4.refs_3_, ...), custom_call_target="tpu_custom_call" | custom-call | flops 4194304 | bytes 1048576 | tf_op jit(solution)/shard_map/pallas_call | solution.py:304
  124.9 3.8 %shard_map.75.refs_0_ = bf16[384,256]{1,0:T(8,128)(2,1)S(1)} custom-call(bf16[4,384,512]{2,1,0:T(8,128)(2,1)} %shard_map.73.source, bf16[8,8,48,256]{3,2,1,0:T(8,128)(2,1)S(1)} %all-to-all-done.1.mine, bf16[8,8,48,256]{3,2,1,0:T(8,128)(2,1)} %collective-permute-done.5.other), custom_call_target="tpu_custom_call" | custom-call | flops 536870912 | bytes 1048576 | tf_op jit(solution)/shard_map/pallas_call | solution.py:304
  128.8 3.4 %shard_map.76.refs_0_ = bf16[272,256]{1,0:T(8,128)(2,1)S(1)} custom-call(bf16[384,256]{1,0:T(8,128)(2,1)S(1)} %shard_map.75.refs_0_, f32[2,128,256]{2,1,0:T(8,128)S(1)} %copy-done.2, f32[2,256]{1,0:T(2,128)S(1)} %copy-done.3), custom_call_target="tpu_custom_call" | custom-call | flops 16777216 | bytes 1048576 | tf_op jit(solution)/shard_map/pallas_call | solution.py:304
  132.2 2.5 %collective-permute-start.6 = (bf16[272,256]{1,0:T(8,128)(2,1)S(1)}, bf16[272,256]{1,0:T(8,128)(2,1)S(1)}, u32[]{:S(2)}, u32[]{:S(2)}) collective-permute-start(bf16[272,256]{1,0:T(8,128)(2,1)S(1)} %shard_map.76.refs_0_), channel_id=1, source_target_pairs={{0,1},{1,2},{2,3},{3,0},{4,5},{5,6},{6,7},{7,4},{8,9},{9,10},{10,1... | collective-permute-start | bytes 417800 | tf_op jit(solution)/shard_map/ppermute | solution.py:74
  134.7 4.2 %collective-permute-start.7 = (bf16[272,256]{1,0:T(8,128)(2,1)S(1)}, bf16[272,256]{1,0:T(8,128)(2,1)S(1)}, u32[]{:S(2)}, u32[]{:S(2)}) collective-permute-start(bf16[272,256]{1,0:T(8,128)(2,1)S(1)} %shard_map.76.refs_0_), channel_id=1, source_target_pairs={{0,2},{1,3},{2,0},{3,1},{4,6},{5,7},{6,4},{7,5},{8,10},{9,11},{10,... | collective-permute-start | bytes 417800 | tf_op jit(solution)/shard_map/ppermute | solution.py:74
  138.9 3.9 %collective-permute-start.8 = (bf16[272,256]{1,0:T(8,128)(2,1)S(1)}, bf16[272,256]{1,0:T(8,128)(2,1)S(1)}, u32[]{:S(2)}, u32[]{:S(2)}) collective-permute-start(bf16[272,256]{1,0:T(8,128)(2,1)S(1)} %shard_map.76.refs_0_), channel_id=1, source_target_pairs={{0,3},{1,0},{2,1},{3,2},{4,7},{5,4},{6,5},{7,6},{8,11},{9,8},{10,9... | collective-permute-start | bytes 417800 | tf_op jit(solution)/shard_map/ppermute | solution.py:74
  142.9 17.1 %shard_map.77.refs_5_ = bf16[4,2,8,2,16,256]{5,4,3,2,1,0:T(8,128)(2,1)} custom-call(bf16[8,8,48,256]{3,2,1,0:T(8,128)(2,1)S(1)} %all-to-all-done.1.mine, bf16[8,8,48,256]{3,2,1,0:T(8,128)(2,1)} %collective-permute-done.5.other), custom_call_target="tpu_custom_call" | custom-call | flops 67108864 | bytes 1048576 | tf_op jit(solution)/shard_map/pallas_call | solution.py:304
  160.0 2.8 %shard_map.78 = bf16[4,256,512]{2,1,0:T(8,128)(2,1)} custom-call(bf16[272,256]{1,0:T(8,128)(2,1)S(1)} %shard_map.76.refs_0_, bf16[272,256]{1,0:T(8,128)(2,1)S(1)} %collective-permute-done.6.refs_1_, bf16[272,256]{1,0:T(8,128)(2,1)S(1)} %collective-permute-done.7.refs_2_, bf16[272,256]{1,0:T(8,128)(2,1)S(1)} %collective-permute-done.8.refs_3_, ...), custom_call_target="tpu_custom_call" | custom-call | flops 268435456 | bytes 1048576 | tf_op jit(solution)/shard_map/pallas_call | solution.py:452
  162.7 17.1 %all_to_all.26.refs_0_.refs_1_ = bf16[4,256,512]{2,1,0:T(8,128)(2,1)S(1)} all-to-all(bf16[4,256,512]{2,1,0:T(8,128)(2,1)} %shard_map.78), channel_id=1, replica_groups=mesh['sp'=128,'tp'=4] {'tp'}, dimensions={0} | all-to-all | bytes 2097152 | tf_op jit(solution)/shard_map/all_to_all | solution.py:82
  181.5 3.4 %shard_map.81.refs_0_.refs_1_ = bf16[256,256]{1,0:T(8,128)(2,1)S(1)} custom-call(bf16[4,256,512]{2,1,0:T(8,128)(2,1)} %shard_map.79.source, bf16[8,8,48,256]{3,2,1,0:T(8,128)(2,1)S(1)} %all-to-all-done.3.mine, bf16[8,8,48,256]{3,2,1,0:T(8,128)(2,1)} %collective-permute-done.9.other), custom_call_target="tpu_custom_call" | custom-call | flops 536870912 | bytes 1048576 | tf_op jit(solution)/shard_map/pallas_call | solution.py:304
  188.4 4.2 %collective-permute-done.10.refs_0_ = bf16[128,256]{1,0:T(8,128)(2,1)S(1)} collective-permute-done((bf16[128,256]{1,0:T(8,128)(2,1)S(1)}, bf16[128,256]{1,0:T(8,128)(2,1)S(1)}, u32[]{:S(2)}, u32[]{:S(2)}) %collective-permute-start.10) | collective-permute-done | bytes 65568 | tf_op jit(solution)/shard_map/ppermute | solution.py:502
  192.6 2.8 %shard_map.83 = bf16[4,272,256]{2,1,0:T(8,128)(2,1)} custom-call(bf16[128,256]{1,0:T(8,128)(2,1)S(1)} %collective-permute-done.10.refs_0_, bf16[256,256]{1,0:T(8,128)(2,1)S(1)} %shard_map.81.refs_0_.refs_1_, f32[128,256]{1,0:T(8,128)S(1)} %shard_map.82.refs_2_, f32[2,128,256]{2,1,0:T(8,128)S(1)} %copy-done.2, f32[2,256]{1,0:T(2,128)S(1)} %copy-done.3), custom_call_target="tpu_custom_call" | custom-call | flops 8388608 | bytes 1048576 | tf_op jit(solution)/shard_map/pallas_call | solution.py:304
  195.4 4.9 %all-to-all-start.4 = ((bf16[4,272,256]{2,1,0:T(8,128)(2,1)}), bf16[4,272,256]{2,1,0:T(8,128)(2,1)S(1)}, u32[]{:S(2)}, u32[]{:S(2)}) async-start(bf16[4,272,256]{2,1,0:T(8,128)(2,1)} %shard_map.83), calls=%async_computation.4 | async-start | bytes 1114112 | tf_op jit(solution)/shard_map/all_to_all | solution.py:82
  200.3 17.1 %shard_map.84.refs_2_ = bf16[4,2,8,2,16,256]{5,4,3,2,1,0:T(8,128)(2,1)} custom-call(bf16[8,8,48,256]{3,2,1,0:T(8,128)(2,1)S(1)} %all-to-all-done.3.mine, bf16[8,8,48,256]{3,2,1,0:T(8,128)(2,1)} %collective-permute-done.9.other), custom_call_target="tpu_custom_call" | custom-call | flops 67108864 | bytes 1048576 | tf_op jit(solution)/shard_map/pallas_call | solution.py:304
  (37 shorter events, 24.2 us)
Async XLA Ops:
  0.0 8.0 %collective-permute-start.1 = (bf16[2,16,256]{2,1,0:T(8,128)(2,1)}, bf16[2,16,256]{2,1,0:T(8,128)(2,1)S(1)}, u32[]{:S(2)}, u32[]{:S(2)}) collective-permute-start(bf16[2,16,256]{2,1,0:T(8,128)(2,1)} %bitcast.1), channel_id=1, source_target_pairs={{0,0},{1,128},{2,256},{3,384},{4,4},{5,20},{6,36},{7,52},{8,8},{9,... | collective-permute-start | bytes 49160 | tf_op jit(solution)/shard_map/ppermute | solution.py:70
  28.0 37.1 %all-to-all-start.1 = ((bf16[8,8,48,256]{3,2,1,0:T(8,128)(2,1)}), bf16[8,8,48,256]{3,2,1,0:T(8,128)(2,1)S(1)}, u32[]{:S(2)}, u32[]{:S(2)}) async-start(bf16[8,8,48,256]{3,2,1,0:T(8,128)(2,1)} %shard_map.74), calls=%async_computation.1 | async-start | bytes 3145728 | tf_op jit(solution)/shard_map/all_to_all | solution.py:45
  42.5 1.2 copy-start.1
  43.7 28.4 %copy-start.4 = (bf16[256,512]{1,0:T(8,128)(2,1)S(1)}, bf16[256,512]{1,0:T(8,128)(2,1)}, u32[]{:S(2)}) copy-start(bf16[256,512]{1,0:T(8,128)(2,1)} %refs_4_.2) | copy-start | bytes 786436
  65.1 28.0 %all-to-all-start.3 = ((bf16[8,8,48,256]{3,2,1,0:T(8,128)(2,1)}), bf16[8,8,48,256]{3,2,1,0:T(8,128)(2,1)S(1)}, u32[]{:S(2)}, u32[]{:S(2)}) async-start(bf16[8,8,48,256]{3,2,1,0:T(8,128)(2,1)} %copy-done.1), calls=%async_computation.3 | async-start | bytes 3145728 | tf_op jit(solution)/shard_map/all_to_all | solution.py:45
  70.2 54.7 %collective-permute-start.5 = (bf16[8,8,48,256]{3,2,1,0:T(8,128)(2,1)S(1)}, bf16[8,8,48,256]{3,2,1,0:T(8,128)(2,1)}, u32[]{:S(2)}, u32[]{:S(2)}) collective-permute-start(bf16[8,8,48,256]{3,2,1,0:T(8,128)(2,1)S(1)} %all-to-all-done.1.mine), channel_id=1, source_target_pairs={{0,4},{4,0},{8,12},{12,8},{16,20},{20,16},{24,28},{28,24},{32,36},... | collective-permute-start | bytes 4718600 | tf_op jit(solution)/shard_map/ppermute | solution.py:57
  72.1 23.0 %collective-permute-start = (bf16[128,512]{1,0:T(8,128)(2,1)S(1)}, bf16[128,512]{1,0:T(8,128)(2,1)}, u32[]{:S(2)}, u32[]{:S(2)}) collective-permute-start(bf16[128,512]{1,0:T(8,128)(2,1)S(1)} %slice.6), channel_id=1, source_target_pairs={{0,4},{4,8},{8,12},{12,16},{16,20},{20,24},{24,28},{28,32},{32,36}... | collective-permute-start | bytes 393224 | tf_op jit(solution)/shard_map/ppermute | solution.py:481
  93.2 88.3 %collective-permute-start.9 = (bf16[8,8,48,256]{3,2,1,0:T(8,128)(2,1)S(1)}, bf16[8,8,48,256]{3,2,1,0:T(8,128)(2,1)}, u32[]{:S(2)}, u32[]{:S(2)}) collective-permute-start(bf16[8,8,48,256]{3,2,1,0:T(8,128)(2,1)S(1)} %all-to-all-done.3.mine), channel_id=1, source_target_pairs={{0,4},{4,0},{8,12},{12,8},{16,20},{20,16},{24,28},{28,24},{32,36},... | collective-permute-start | bytes 4718600 | tf_op jit(solution)/shard_map/ppermute | solution.py:57
  96.1 14.0 %collective-permute-start.2 = (bf16[384,512]{1,0:T(8,128)(2,1)S(1)}, bf16[384,512]{1,0:T(8,128)(2,1)}, u32[]{:S(2)}, u32[]{:S(2)}) collective-permute-start(bf16[384,512]{1,0:T(8,128)(2,1)S(1)} %pad_maximum_fusion.refs_0_), channel_id=1, source_target_pairs={{0,1},{1,2},{2,3},{3,0},{4,5},{5,6},{6,7},{7,4},{8,9},{9,10},{10,1... | collective-permute-start | bytes 1179656 | tf_op jit(solution)/shard_map/ppermute | solution.py:74
  98.0 15.5 %collective-permute-start.3 = (bf16[384,512]{1,0:T(8,128)(2,1)S(1)}, bf16[384,512]{1,0:T(8,128)(2,1)}, u32[]{:S(2)}, u32[]{:S(2)}) collective-permute-start(bf16[384,512]{1,0:T(8,128)(2,1)S(1)} %pad_maximum_fusion.refs_0_), channel_id=1, source_target_pairs={{0,2},{1,3},{2,0},{3,1},{4,6},{5,7},{6,4},{7,5},{8,10},{9,11},{10,... | collective-permute-start | bytes 1179656 | tf_op jit(solution)/shard_map/ppermute | solution.py:74
  102.5 19.0 %collective-permute-start.4 = (bf16[384,512]{1,0:T(8,128)(2,1)S(1)}, bf16[384,512]{1,0:T(8,128)(2,1)}, u32[]{:S(2)}, u32[]{:S(2)}) collective-permute-start(bf16[384,512]{1,0:T(8,128)(2,1)S(1)} %pad_maximum_fusion.refs_0_), channel_id=1, source_target_pairs={{0,3},{1,0},{2,1},{3,2},{4,7},{5,4},{6,5},{7,6},{8,11},{9,8},{10,9... | collective-permute-start | bytes 1179656 | tf_op jit(solution)/shard_map/ppermute | solution.py:74
  124.9 3.9 %copy-start.2 = (f32[2,128,256]{2,1,0:T(8,128)S(1)}, f32[2,128,256]{2,1,0:T(8,128)}, u32[]{:S(2)}) copy-start(f32[2,128,256]{2,1,0:T(8,128)} %refs_3_.1) | copy-start | bytes 786436
  124.9 3.9 %copy-start.3 = (f32[2,256]{1,0:T(2,128)S(1)}, f32[2,256]{1,0:T(2,128)}, u32[]{:S(2)}) copy-start(f32[2,256]{1,0:T(2,128)} %refs_4_.3) | copy-start | bytes 6148
  132.2 27.8 %collective-permute-start.6 = (bf16[272,256]{1,0:T(8,128)(2,1)S(1)}, bf16[272,256]{1,0:T(8,128)(2,1)S(1)}, u32[]{:S(2)}, u32[]{:S(2)}) collective-permute-start(bf16[272,256]{1,0:T(8,128)(2,1)S(1)} %shard_map.76.refs_0_), channel_id=1, source_target_pairs={{0,1},{1,2},{2,3},{3,0},{4,5},{5,6},{6,7},{7,4},{8,9},{9,10},{10,1... | collective-permute-start | bytes 417800 | tf_op jit(solution)/shard_map/ppermute | solution.py:74
  134.7 25.2 %collective-permute-start.7 = (bf16[272,256]{1,0:T(8,128)(2,1)S(1)}, bf16[272,256]{1,0:T(8,128)(2,1)S(1)}, u32[]{:S(2)}, u32[]{:S(2)}) collective-permute-start(bf16[272,256]{1,0:T(8,128)(2,1)S(1)} %shard_map.76.refs_0_), channel_id=1, source_target_pairs={{0,2},{1,3},{2,0},{3,1},{4,6},{5,7},{6,4},{7,5},{8,10},{9,11},{10,... | collective-permute-start | bytes 417800 | tf_op jit(solution)/shard_map/ppermute | solution.py:74
  138.9 21.0 %collective-permute-start.8 = (bf16[272,256]{1,0:T(8,128)(2,1)S(1)}, bf16[272,256]{1,0:T(8,128)(2,1)S(1)}, u32[]{:S(2)}, u32[]{:S(2)}) collective-permute-start(bf16[272,256]{1,0:T(8,128)(2,1)S(1)} %shard_map.76.refs_0_), channel_id=1, source_target_pairs={{0,3},{1,0},{2,1},{3,2},{4,7},{5,4},{6,5},{7,6},{8,11},{9,8},{10,9... | collective-permute-start | bytes 417800 | tf_op jit(solution)/shard_map/ppermute | solution.py:74
  179.8 5.0 %copy-start = (bf16[4,256,512]{2,1,0:T(8,128)(2,1)}, bf16[4,256,512]{2,1,0:T(8,128)(2,1)S(1)}, u32[]{:S(2)}) copy-start(bf16[4,256,512]{2,1,0:T(8,128)(2,1)S(1)} %all_to_all.26.refs_0_.refs_1_) | copy-start | bytes 3145732
  184.9 7.7 %collective-permute-start.10 = (bf16[128,256]{1,0:T(8,128)(2,1)S(1)}, bf16[128,256]{1,0:T(8,128)(2,1)S(1)}, u32[]{:S(2)}, u32[]{:S(2)}) collective-permute-start(bf16[128,256]{1,0:T(8,128)(2,1)S(1)} %slice.8), channel_id=1, source_target_pairs={{0,4},{4,8},{8,12},{12,16},{16,20},{20,24},{24,28},{28,32},{32,36}... | collective-permute-start | bytes 196616 | tf_op jit(solution)/shard_map/ppermute | solution.py:502
  195.4 22.0 %all-to-all-start.4 = ((bf16[4,272,256]{2,1,0:T(8,128)(2,1)}), bf16[4,272,256]{2,1,0:T(8,128)(2,1)S(1)}, u32[]{:S(2)}, u32[]{:S(2)}) async-start(bf16[4,272,256]{2,1,0:T(8,128)(2,1)} %shard_map.83), calls=%async_computation.4 | async-start | bytes 1114112 | tf_op jit(solution)/shard_map/all_to_all | solution.py:82

commit v5 on v4

--- a/solution.py
+++ b/solution.py
@@ -93,7 +93,7 @@
 
 
 def norm_kernel(layer, n, *refs):
-    parts, (gain, out, scale, xs, sem) = refs[:n], refs[n:]
+    parts, (gain, xs, scale) = refs[:n], refs[n:]
 
     def squares(i, _):
         rows = pl.ds(pl.multiple_of(i * 16, 16), 16)
@@ -120,15 +120,9 @@
         return 0
 
     lax.fori_loop(0, steps, apply, 0, unroll=2)
-    done = pltpu.make_async_copy(xs, out, sem)
-    done.start()
-    done.wait()
-
-
-def mix_kernel(source, mine, other, glu, vs, gs, xs, sem):
-    fetch = pltpu.make_async_copy(source, xs, sem)
-    fetch.start()
-
+
+
+def mix_kernel(xs, mine, other, glu, vs, gs):
     def fill(zy, yz):
         for z in range(NZ):
             for c, w in enumerate((zy.at[z], yz.at[:, z])):
@@ -143,7 +137,6 @@
     def _():
         fill(other, mine)
 
-    fetch.wait()
     value = jnp.zeros(glu.shape, F32)
     gate = jnp.zeros(glu.shape, F32)
     for k in range(NX):
@@ -296,21 +289,18 @@
     return v if INTERPRET else pltpu.with_memory_space_constraint(v, pltpu.HBM)
 
 
-def call(body, out, ins, scratch, flops, place=pltpu.VMEM, loose=(), far=()):
-    def spot(i):
-        return pltpu.HBM if i in far else pl.ANY if i in loose else pltpu.VMEM
-
+def call(body, out, ins, scratch, flops, place=pltpu.VMEM):
     spec = pl.BlockSpec(memory_space=place)
     return pl.pallas_call(
         body,
         out_shape=out,
-        in_specs=[pl.BlockSpec(memory_space=spot(i)) for i in range(len(ins))],
+        in_specs=[pl.BlockSpec(memory_space=pltpu.VMEM)] * len(ins),
         out_specs=spec,
         scratch_shapes=scratch,
         cost_estimate=pl.CostEstimate(flops=flops, transcendentals=0, bytes_accessed=1 << 20),
         compiler_params=pltpu.CompilerParams(vmem_limit_bytes=14 << 20),
         interpret=INTERPRET,
-    )(*(in_hbm(v) if i in far else v for i, v in enumerate(ins)))
+    )(*ins)
 
 
 def normalise(layer, parts, gain):
@@ -319,15 +309,10 @@
 
     return call(
         body,
-        pltpu.HBM((NX, parts[0].shape[-2], FEAT), BF),
+        jax.ShapeDtypeStruct((NX, parts[0].shape[-2], FEAT), BF),
         [*parts, gain],
-        [
-            pltpu.VMEM((parts[0].shape[-2], 128), F32),
-            pltpu.VMEM((NX, parts[0].shape[-2], FEAT), BF),
-            pltpu.SemaphoreType.DMA(()),
-        ],
+        [pltpu.VMEM((parts[0].shape[-2], 128), F32)],
         8 * NX * TOK * FEAT,
-        pltpu.HBM,
     )
 
 
@@ -337,25 +322,16 @@
         mix_kernel,
         jax.ShapeDtypeStruct((xs.shape[1], CH), BF),
         [xs, mine, other],
-        [weights, weights, pltpu.VMEM(xs.shape, BF), pltpu.SemaphoreType.DMA(())],
+        [weights, weights],
         4 * NX * TOK * FEAT * CH,
-        far=(0,),
-    )
-
-
-def arrange_kernel(mine, other, wt, sems):
+    )
+
+
+def arrange_kernel(mine, other, out, wt, sem):
     def fill(halves):
-        copies = []
         for k in range(NX):
             for c, w in enumerate(halves):
-                part = w.at[2 * k : 2 * k + 2, :, 32:, :]
-                copies.append(
-                    pltpu.make_async_copy(part, wt.at[k, :, :, c], sems.at[2 * k + c])
-                )
-        for one in copies:
-            one.start()
-        for one in copies:
-            one.wait()
+                wt[k, :, :, c] = w[2 * k : 2 * k + 2, :, 32:, :]
 
     @pl.when(core_here() == 0)
     def _():
@@ -365,16 +341,20 @@
     def _():
         fill((other, mine))
 
+    done = pltpu.make_async_copy(wt, out, sem)
+    done.start()
+    done.wait()
+
 
 def arrange(mine, other):
+    shape = (NX, 2, NY, 2, 16, CH)
     return call(
         arrange_kernel,
-        pltpu.HBM((NX, 2, NY, 2, 16, CH), BF),
+        pltpu.HBM(shape, BF),
         [mine, other],
-        [pltpu.SemaphoreType.DMA((2 * NX,))],
+        [pltpu.VMEM(shape, BF), pltpu.SemaphoreType.DMA(())],
         1 << 26,
         pltpu.HBM,
-        (0, 1),
     )
 
 

time: 221 us -> 195 us (0.88)
  the two profiles are of different devices: /device:TPU:66 before, /device:TPU:1 now
where the time goes in v5:
time: 195 us; the launch traced here: 193 us
  waiting for transfers between devices  60.1 us (31%)
  starting transfers between devices  52.6 us (27%)
  blocking collectives  48.9 us (25%)
  Pallas kernels  27.2 us (14%)
  local copies, waits for them, and re-layouts  3.41 us (2%)
    all_to_all x2, waiting for transfers between devices, plane(): lax.all_to_all(copies, 'sp', split_axis=0, concat_axis=0, tiled=True, axi...  37.3 us
    all_to_all x1, blocking collectives, to_group(): lax.all_to_all(copies, 'sp', split_axis=0, concat_axis=0, tiled=True, axi...  32.1 us
    pallas_call x11, Pallas kernels, call(): pl.pallas_call(body, out_shape=out, in_specs=[pl.BlockSpec(memory_space=p...  22 us
    ppermute x6, starting transfers between devices, along_x(): return lax.ppermute(v, 'x', [(i, (i + step) % NX) for i in range(NX)])  19.4 us
    all_to_all x1, blocking collectives, exchange_x(): lax.all_to_all(copies, 'x', split_axis=0, concat_axis=0, tiled=True)  16.8 us
    ppermute x6, waiting for transfers between devices, along_x(): return lax.ppermute(v, 'x', [(i, (i + step) % NX) for i in range(NX)])  16 us
    ppermute x2, starting transfers between devices, swap_cores(): return lax.ppermute(v, 'sp', [(i, i ^ 1) for i in range(count)])  14.8 us
    all_to_all x2, starting transfers between devices, plane(): lax.all_to_all(copies, 'sp', split_axis=0, concat_axis=0, tiled=True, axi...  8.03 us
  transfers between devices with their start and end apart: 14, of which 7 were waited for; matrix products, arithmetic and copies ran while one was open for 2% of the time, Pallas kernels for 10%

profile of v5, /device:TPU:1, one launch (start us, length us, event | category | flops | bytes accessed | tf_op | source)
XLA Modules:
  0.0 193.5 jit_solution(7224694693246226875)
XLA Ops:
  2.8 32.1 %all_to_all.25.refs_0_ = bf16[8,2,48,256]{3,2,1,0:T(8,128)(2,1)S(1)} all-to-all(bf16[8,2,48,256]{3,2,1,0:T(8,128)(2,1)S(1)} %broadcast_in_dim.3), channel_id=1, replica_groups={{0,8,16,24,32,40,48,56},{64,72,80,88,96,104,112,120},{128,136,144,152,1..., dimensions={0} | all-to-all | bytes 786432 | tf_op jit(solution)/shard_map/all_to_all | solution.py:35
  36.1 4.5 %all-to-all-start.1 = ((bf16[8,8,48,256]{3,2,1,0:T(8,128)(2,1)}), bf16[8,8,48,256]{3,2,1,0:T(8,128)(2,1)S(1)}, u32[]{:S(2)}, u32[]{:S(2)}) async-start(bf16[8,8,48,256]{3,2,1,0:T(8,128)(2,1)} %shard_map.74), calls=%async_computation.1 | async-start | bytes 3145728 | tf_op jit(solution)/shard_map/all_to_all | solution.py:45
  42.1 22.2 %all-to-all-done.1.mine = bf16[8,8,48,256]{3,2,1,0:T(8,128)(2,1)S(1)} async-done(((bf16[8,8,48,256]{3,2,1,0:T(8,128)(2,1)}), bf16[8,8,48,256]{3,2,1,0:T(8,128)(2,1)S(1)}, u32[]{:S(2)}, u32[]{:S(2)}) %all-to-all-start.1) | async-done | bytes 1572896 | tf_op jit(solution)/shard_map/all_to_all | solution.py:45
  64.3 3.6 %all-to-all-start.3 = ((bf16[8,8,48,256]{3,2,1,0:T(8,128)(2,1)}), bf16[8,8,48,256]{3,2,1,0:T(8,128)(2,1)S(1)}, u32[]{:S(2)}, u32[]{:S(2)}) async-start(bf16[8,8,48,256]{3,2,1,0:T(8,128)(2,1)} %copy-done.1), calls=%async_computation.3 | async-start | bytes 3145728 | tf_op jit(solution)/shard_map/all_to_all | solution.py:45
  67.9 6.1 %collective-permute-start.5 = (bf16[8,8,48,256]{3,2,1,0:T(8,128)(2,1)S(1)}, bf16[8,8,48,256]{3,2,1,0:T(8,128)(2,1)}, u32[]{:S(2)}, u32[]{:S(2)}) collective-permute-start(bf16[8,8,48,256]{3,2,1,0:T(8,128)(2,1)S(1)} %all-to-all-done.1.mine), channel_id=1, source_target_pairs={{0,4},{4,0},{8,12},{12,8},{16,20},{20,16},{24,28},{28,24},{32,36},... | collective-permute-start | bytes 4718600 | tf_op jit(solution)/shard_map/ppermute | solution.py:57
  76.1 15.1 %all-to-all-done.3.mine = bf16[8,8,48,256]{3,2,1,0:T(8,128)(2,1)S(1)} async-done(((bf16[8,8,48,256]{3,2,1,0:T(8,128)(2,1)}), bf16[8,8,48,256]{3,2,1,0:T(8,128)(2,1)S(1)}, u32[]{:S(2)}, u32[]{:S(2)}) %all-to-all-start.3) | async-done | bytes 1572896 | tf_op jit(solution)/shard_map/all_to_all | solution.py:45
  91.2 8.6 %collective-permute-start.9 = (bf16[8,8,48,256]{3,2,1,0:T(8,128)(2,1)S(1)}, bf16[8,8,48,256]{3,2,1,0:T(8,128)(2,1)}, u32[]{:S(2)}, u32[]{:S(2)}) collective-permute-start(bf16[8,8,48,256]{3,2,1,0:T(8,128)(2,1)S(1)} %all-to-all-done.3.mine), channel_id=1, source_target_pairs={{0,4},{4,0},{8,12},{12,8},{16,20},{20,16},{24,28},{28,24},{32,36},... | collective-permute-start | bytes 4718600 | tf_op jit(solution)/shard_map/ppermute | solution.py:57
  100.9 3.2 %collective-permute-start.2 = (bf16[384,512]{1,0:T(8,128)(2,1)S(1)}, bf16[384,512]{1,0:T(8,128)(2,1)}, u32[]{:S(2)}, u32[]{:S(2)}) collective-permute-start(bf16[384,512]{1,0:T(8,128)(2,1)S(1)} %pad_maximum_fusion.refs_0_), channel_id=1, source_target_pairs={{0,1},{1,2},{2,3},{3,0},{4,5},{5,6},{6,7},{7,4},{8,9},{9,10},{10,1... | collective-permute-start | bytes 1179656 | tf_op jit(solution)/shard_map/ppermute | solution.py:74
  106.0 4.3 %collective-permute-start.4 = (bf16[384,512]{1,0:T(8,128)(2,1)S(1)}, bf16[384,512]{1,0:T(8,128)(2,1)}, u32[]{:S(2)}, u32[]{:S(2)}) collective-permute-start(bf16[384,512]{1,0:T(8,128)(2,1)S(1)} %pad_maximum_fusion.refs_0_), channel_id=1, source_target_pairs={{0,3},{1,0},{2,1},{3,2},{4,7},{5,4},{6,5},{7,6},{8,11},{9,8},{10,9... | collective-permute-start | bytes 1179656 | tf_op jit(solution)/shard_map/ppermute | solution.py:74
  111.1 12.1 %collective-permute-done.2.refs_1_ = bf16[384,512]{1,0:T(8,128)(2,1)} collective-permute-done((bf16[384,512]{1,0:T(8,128)(2,1)S(1)}, bf16[384,512]{1,0:T(8,128)(2,1)}, u32[]{:S(2)}, u32[]{:S(2)}) %collective-permute-start.2) | collective-permute-done | bytes 393248 | tf_op jit(solution)/shard_map/ppermute | solution.py:74
  127.7 2.6 %shard_map.75.refs_0_ = bf16[384,256]{1,0:T(8,128)(2,1)S(1)} custom-call(bf16[4,384,512]{2,1,0:T(8,128)(2,1)S(1)} %shard_map.73.xs, bf16[8,8,48,256]{3,2,1,0:T(8,128)(2,1)S(1)} %all-to-all-done.1.mine, bf16[8,8,48,256]{3,2,1,0:T(8,128)(2,1)} %collective-permute-done.5.other), custom_call_target="tpu_custom_call" | custom-call | flops 536870912 | bytes 1048576 | tf_op jit(solution)/shard_map/pallas_call | solution.py:294
  130.3 3.4 %shard_map.76.refs_0_ = bf16[272,256]{1,0:T(8,128)(2,1)S(1)} custom-call(bf16[384,256]{1,0:T(8,128)(2,1)S(1)} %shard_map.75.refs_0_, f32[2,128,256]{2,1,0:T(8,128)S(1)} %copy-done.2, f32[2,256]{1,0:T(2,128)S(1)} %copy-done.3), custom_call_target="tpu_custom_call" | custom-call | flops 16777216 | bytes 1048576 | tf_op jit(solution)/shard_map/pallas_call | solution.py:294
  133.7 3.6 %collective-permute-start.6 = (bf16[272,256]{1,0:T(8,128)(2,1)S(1)}, bf16[272,256]{1,0:T(8,128)(2,1)S(1)}, u32[]{:S(2)}, u32[]{:S(2)}) collective-permute-start(bf16[272,256]{1,0:T(8,128)(2,1)S(1)} %shard_map.76.refs_0_), channel_id=1, source_target_pairs={{0,1},{1,2},{2,3},{3,0},{4,5},{5,6},{6,7},{7,4},{8,9},{9,10},{10,1... | collective-permute-start | bytes 417800 | tf_op jit(solution)/shard_map/ppermute | solution.py:74
  137.3 4.5 %collective-permute-start.7 = (bf16[272,256]{1,0:T(8,128)(2,1)S(1)}, bf16[272,256]{1,0:T(8,128)(2,1)S(1)}, u32[]{:S(2)}, u32[]{:S(2)}) collective-permute-start(bf16[272,256]{1,0:T(8,128)(2,1)S(1)} %shard_map.76.refs_0_), channel_id=1, source_target_pairs={{0,2},{1,3},{2,0},{3,1},{4,6},{5,7},{6,4},{7,5},{8,10},{9,11},{10,... | collective-permute-start | bytes 417800 | tf_op jit(solution)/shard_map/ppermute | solution.py:74
  143.7 2.5 %shard_map.77.refs_5_ = bf16[4,2,8,2,16,256]{5,4,3,2,1,0:T(8,128)(2,1)} custom-call(bf16[8,8,48,256]{3,2,1,0:T(8,128)(2,1)S(1)} %all-to-all-done.1.mine, bf16[8,8,48,256]{3,2,1,0:T(8,128)(2,1)} %collective-permute-done.5.other), custom_call_target="tpu_custom_call" | custom-call | flops 67108864 | bytes 1048576 | tf_op jit(solution)/shard_map/pallas_call | solution.py:294
  147.8 2.7 %shard_map.78 = bf16[4,256,512]{2,1,0:T(8,128)(2,1)} custom-call(bf16[272,256]{1,0:T(8,128)(2,1)S(1)} %shard_map.76.refs_0_, bf16[272,256]{1,0:T(8,128)(2,1)S(1)} %collective-permute-done.6.refs_1_, bf16[272,256]{1,0:T(8,128)(2,1)S(1)} %collective-permute-done.7.refs_2_, bf16[272,256]{1,0:T(8,128)(2,1)S(1)} %collective-permute-done.8.refs_3_, ...), custom_call_target="tpu_custom_call" | custom-call | flops 268435456 | bytes 1048576 | tf_op jit(solution)/shard_map/pallas_call | solution.py:432
  150.6 16.8 %all_to_all.26.refs_0_.refs_1_ = bf16[4,256,512]{2,1,0:T(8,128)(2,1)S(1)} all-to-all(bf16[4,256,512]{2,1,0:T(8,128)(2,1)} %shard_map.78), channel_id=1, replica_groups=mesh['sp'=128,'tp'=4] {'tp'}, dimensions={0} | all-to-all | bytes 2097152 | tf_op jit(solution)/shard_map/all_to_all | solution.py:82
  168.1 2.3 %shard_map.81.refs_0_.refs_1_ = bf16[256,256]{1,0:T(8,128)(2,1)S(1)} custom-call(bf16[4,256,512]{2,1,0:T(8,128)(2,1)S(1)} %shard_map.79.xs, bf16[8,8,48,256]{3,2,1,0:T(8,128)(2,1)S(1)} %all-to-all-done.3.mine, bf16[8,8,48,256]{3,2,1,0:T(8,128)(2,1)} %collective-permute-done.9.other), custom_call_target="tpu_custom_call" | custom-call | flops 536870912 | bytes 1048576 | tf_op jit(solution)/shard_map/pallas_call | solution.py:294
  170.4 3.4 %collective-permute-start.10 = (bf16[128,256]{1,0:T(8,128)(2,1)S(1)}, bf16[128,256]{1,0:T(8,128)(2,1)S(1)}, u32[]{:S(2)}, u32[]{:S(2)}) collective-permute-start(bf16[128,256]{1,0:T(8,128)(2,1)S(1)} %slice.8), channel_id=1, source_target_pairs={{0,4},{4,8},{8,12},{12,16},{16,20},{20,24},{24,28},{28,32},{32,36}... | collective-permute-start | bytes 196616 | tf_op jit(solution)/shard_map/ppermute | solution.py:482
  175.4 2.8 %shard_map.83 = bf16[4,272,256]{2,1,0:T(8,128)(2,1)} custom-call(bf16[128,256]{1,0:T(8,128)(2,1)S(1)} %collective-permute-done.10.refs_0_, bf16[256,256]{1,0:T(8,128)(2,1)S(1)} %shard_map.81.refs_0_.refs_1_, f32[128,256]{1,0:T(8,128)S(1)} %shard_map.82.refs_2_, f32[2,128,256]{2,1,0:T(8,128)S(1)} %copy-done.2, f32[2,256]{1,0:T(2,128)S(1)} %copy-done.3), custom_call_target="tpu_custom_call" | custom-call | flops 8388608 | bytes 1048576 | tf_op jit(solution)/shard_map/pallas_call | solution.py:294
  178.2 3.5 %all-to-all-start.4 = ((bf16[4,272,256]{2,1,0:T(8,128)(2,1)}), bf16[4,272,256]{2,1,0:T(8,128)(2,1)S(1)}, u32[]{:S(2)}, u32[]{:S(2)}) async-start(bf16[4,272,256]{2,1,0:T(8,128)(2,1)} %shard_map.83), calls=%async_computation.4 | async-start | bytes 1114112 | tf_op jit(solution)/shard_map/all_to_all | solution.py:82
  181.7 2.5 %shard_map.84.refs_2_ = bf16[4,2,8,2,16,256]{5,4,3,2,1,0:T(8,128)(2,1)} custom-call(bf16[8,8,48,256]{3,2,1,0:T(8,128)(2,1)S(1)} %all-to-all-done.3.mine, bf16[8,8,48,256]{3,2,1,0:T(8,128)(2,1)} %collective-permute-done.9.other), custom_call_target="tpu_custom_call" | custom-call | flops 67108864 | bytes 1048576 | tf_op jit(solution)/shard_map/pallas_call | solution.py:294
  184.2 6.8 %all-to-all-done.4.refs_0_ = bf16[4,272,256]{2,1,0:T(8,128)(2,1)S(1)} async-done(((bf16[4,272,256]{2,1,0:T(8,128)(2,1)}), bf16[4,272,256]{2,1,0:T(8,128)(2,1)S(1)}, u32[]{:S(2)}, u32[]{:S(2)}) %all-to-all-start.4) | async-done | bytes 557088 | tf_op jit(solution)/shard_map/all_to_all | solution.py:82
  191.0 2.5 %shard_map.85 = bf16[256,512]{1,0:T(8,128)(2,1)} custom-call(bf16[4,272,256]{2,1,0:T(8,128)(2,1)S(1)} %all-to-all-done.4.refs_0_, bf16[4,256,512]{2,1,0:T(8,128)(2,1)} %copy-done, bf16[4,2,8,2,16,256]{5,4,3,2,1,0:T(8,128)(2,1)} %shard_map.84.refs_2_), custom_call_target="tpu_custom_call" | custom-call | flops 268435456 | bytes 1048576 | tf_op jit(solution)/shard_map/pallas_call | solution.py:432
  (37 shorter events, 21.7 us)
Async XLA Ops:
  0.0 2.8 %collective-permute-start.1 = (bf16[2,16,256]{2,1,0:T(8,128)(2,1)}, bf16[2,16,256]{2,1,0:T(8,128)(2,1)S(1)}, u32[]{:S(2)}, u32[]{:S(2)}) collective-permute-start(bf16[2,16,256]{2,1,0:T(8,128)(2,1)} %bitcast.1), channel_id=1, source_target_pairs={{0,0},{1,128},{2,256},{3,384},{4,4},{5,20},{6,36},{7,52},{8,8},{9,... | collective-permute-start | bytes 49160 | tf_op jit(solution)/shard_map/ppermute | solution.py:70
  36.1 28.2 %all-to-all-start.1 = ((bf16[8,8,48,256]{3,2,1,0:T(8,128)(2,1)}), bf16[8,8,48,256]{3,2,1,0:T(8,128)(2,1)S(1)}, u32[]{:S(2)}, u32[]{:S(2)}) async-start(bf16[8,8,48,256]{3,2,1,0:T(8,128)(2,1)} %shard_map.74), calls=%async_computation.1 | async-start | bytes 3145728 | tf_op jit(solution)/shard_map/all_to_all | solution.py:45
  40.9 1.2 copy-start.1
  42.1 31.9 %copy-start.4 = (bf16[256,512]{1,0:T(8,128)(2,1)S(1)}, bf16[256,512]{1,0:T(8,128)(2,1)}, u32[]{:S(2)}) copy-start(bf16[256,512]{1,0:T(8,128)(2,1)} %refs_4_.2) | copy-start | bytes 786436
  64.3 26.9 %all-to-all-start.3 = ((bf16[8,8,48,256]{3,2,1,0:T(8,128)(2,1)}), bf16[8,8,48,256]{3,2,1,0:T(8,128)(2,1)S(1)}, u32[]{:S(2)}, u32[]{:S(2)}) async-start(bf16[8,8,48,256]{3,2,1,0:T(8,128)(2,1)} %copy-done.1), calls=%async_computation.3 | async-start | bytes 3145728 | tf_op jit(solution)/shard_map/all_to_all | solution.py:45
  67.9 59.8 %collective-permute-start.5 = (bf16[8,8,48,256]{3,2,1,0:T(8,128)(2,1)S(1)}, bf16[8,8,48,256]{3,2,1,0:T(8,128)(2,1)}, u32[]{:S(2)}, u32[]{:S(2)}) collective-permute-start(bf16[8,8,48,256]{3,2,1,0:T(8,128)(2,1)S(1)} %all-to-all-done.1.mine), channel_id=1, source_target_pairs={{0,4},{4,0},{8,12},{12,8},{16,20},{20,16},{24,28},{28,24},{32,36},... | collective-permute-start | bytes 4718600 | tf_op jit(solution)/shard_map/ppermute | solution.py:57
  74.0 25.8 %collective-permute-start = (bf16[128,512]{1,0:T(8,128)(2,1)S(1)}, bf16[128,512]{1,0:T(8,128)(2,1)}, u32[]{:S(2)}, u32[]{:S(2)}) collective-permute-start(bf16[128,512]{1,0:T(8,128)(2,1)S(1)} %slice.6), channel_id=1, source_target_pairs={{0,4},{4,8},{8,12},{12,16},{16,20},{20,24},{24,28},{28,32},{32,36}... | collective-permute-start | bytes 393224 | tf_op jit(solution)/shard_map/ppermute | solution.py:461
  91.2 76.9 %collective-permute-start.9 = (bf16[8,8,48,256]{3,2,1,0:T(8,128)(2,1)S(1)}, bf16[8,8,48,256]{3,2,1,0:T(8,128)(2,1)}, u32[]{:S(2)}, u32[]{:S(2)}) collective-permute-start(bf16[8,8,48,256]{3,2,1,0:T(8,128)(2,1)S(1)} %all-to-all-done.3.mine), channel_id=1, source_target_pairs={{0,4},{4,0},{8,12},{12,8},{16,20},{20,16},{24,28},{28,24},{32,36},... | collective-permute-start | bytes 4718600 | tf_op jit(solution)/shard_map/ppermute | solution.py:57
  100.9 22.3 %collective-permute-start.2 = (bf16[384,512]{1,0:T(8,128)(2,1)S(1)}, bf16[384,512]{1,0:T(8,128)(2,1)}, u32[]{:S(2)}, u32[]{:S(2)}) collective-permute-start(bf16[384,512]{1,0:T(8,128)(2,1)S(1)} %pad_maximum_fusion.refs_0_), channel_id=1, source_target_pairs={{0,1},{1,2},{2,3},{3,0},{4,5},{5,6},{6,7},{7,4},{8,9},{9,10},{10,1... | collective-permute-start | bytes 1179656 | tf_op jit(solution)/shard_map/ppermute | solution.py:74
  104.1 19.1 %collective-permute-start.3 = (bf16[384,512]{1,0:T(8,128)(2,1)S(1)}, bf16[384,512]{1,0:T(8,128)(2,1)}, u32[]{:S(2)}, u32[]{:S(2)}) collective-permute-start(bf16[384,512]{1,0:T(8,128)(2,1)S(1)} %pad_maximum_fusion.refs_0_), channel_id=1, source_target_pairs={{0,2},{1,3},{2,0},{3,1},{4,6},{5,7},{6,4},{7,5},{8,10},{9,11},{10,... | collective-permute-start | bytes 1179656 | tf_op jit(solution)/shard_map/ppermute | solution.py:74
  106.0 19.4 %collective-permute-start.4 = (bf16[384,512]{1,0:T(8,128)(2,1)S(1)}, bf16[384,512]{1,0:T(8,128)(2,1)}, u32[]{:S(2)}, u32[]{:S(2)}) collective-permute-start(bf16[384,512]{1,0:T(8,128)(2,1)S(1)} %pad_maximum_fusion.refs_0_), channel_id=1, source_target_pairs={{0,3},{1,0},{2,1},{3,2},{4,7},{5,4},{6,5},{7,6},{8,11},{9,8},{10,9... | collective-permute-start | bytes 1179656 | tf_op jit(solution)/shard_map/ppermute | solution.py:74
  127.7 2.6 %copy-start.2 = (f32[2,128,256]{2,1,0:T(8,128)S(1)}, f32[2,128,256]{2,1,0:T(8,128)}, u32[]{:S(2)}) copy-start(f32[2,128,256]{2,1,0:T(8,128)} %refs_3_.1) | copy-start | bytes 786436
  127.7 2.6 %copy-start.3 = (f32[2,256]{1,0:T(2,128)S(1)}, f32[2,256]{1,0:T(2,128)}, u32[]{:S(2)}) copy-start(f32[2,256]{1,0:T(2,128)} %refs_4_.3) | copy-start | bytes 6148
  133.7 12.4 %collective-permute-start.6 = (bf16[272,256]{1,0:T(8,128)(2,1)S(1)}, bf16[272,256]{1,0:T(8,128)(2,1)S(1)}, u32[]{:S(2)}, u32[]{:S(2)}) collective-permute-start(bf16[272,256]{1,0:T(8,128)(2,1)S(1)} %shard_map.76.refs_0_), channel_id=1, source_target_pairs={{0,1},{1,2},{2,3},{3,0},{4,5},{5,6},{6,7},{7,4},{8,9},{9,10},{10,1... | collective-permute-start | bytes 417800 | tf_op jit(solution)/shard_map/ppermute | solution.py:74
  137.3 9.1 %collective-permute-start.7 = (bf16[272,256]{1,0:T(8,128)(2,1)S(1)}, bf16[272,256]{1,0:T(8,128)(2,1)S(1)}, u32[]{:S(2)}, u32[]{:S(2)}) collective-permute-start(bf16[272,256]{1,0:T(8,128)(2,1)S(1)} %shard_map.76.refs_0_), channel_id=1, source_target_pairs={{0,2},{1,3},{2,0},{3,1},{4,6},{5,7},{6,4},{7,5},{8,10},{9,11},{10,... | collective-permute-start | bytes 417800 | tf_op jit(solution)/shard_map/ppermute | solution.py:74
  141.7 6.1 %collective-permute-start.8 = (bf16[272,256]{1,0:T(8,128)(2,1)S(1)}, bf16[272,256]{1,0:T(8,128)(2,1)S(1)}, u32[]{:S(2)}, u32[]{:S(2)}) collective-permute-start(bf16[272,256]{1,0:T(8,128)(2,1)S(1)} %shard_map.76.refs_0_), channel_id=1, source_target_pairs={{0,3},{1,0},{2,1},{3,2},{4,7},{5,4},{6,5},{7,6},{8,11},{9,8},{10,9... | collective-permute-start | bytes 417800 | tf_op jit(solution)/shard_map/ppermute | solution.py:74
  167.4 3.0 %copy-start = (bf16[4,256,512]{2,1,0:T(8,128)(2,1)}, bf16[4,256,512]{2,1,0:T(8,128)(2,1)S(1)}, u32[]{:S(2)}) copy-start(bf16[4,256,512]{2,1,0:T(8,128)(2,1)S(1)} %all_to_all.26.refs_0_.refs_1_) | copy-start | bytes 3145732
  170.4 5.0 %collective-permute-start.10 = (bf16[128,256]{1,0:T(8,128)(2,1)S(1)}, bf16[128,256]{1,0:T(8,128)(2,1)S(1)}, u32[]{:S(2)}, u32[]{:S(2)}) collective-permute-start(bf16[128,256]{1,0:T(8,128)(2,1)S(1)} %slice.8), channel_id=1, source_target_pairs={{0,4},{4,8},{8,12},{12,16},{16,20},{20,24},{24,28},{28,32},{32,36}... | collective-permute-start | bytes 196616 | tf_op jit(solution)/shard_map/ppermute | solution.py:482
  178.2 12.8 %all-to-all-start.4 = ((bf16[4,272,256]{2,1,0:T(8,128)(2,1)}), bf16[4,272,256]{2,1,0:T(8,128)(2,1)S(1)}, u32[]{:S(2)}, u32[]{:S(2)}) async-start(bf16[4,272,256]{2,1,0:T(8,128)(2,1)} %shard_map.83), calls=%async_computation.4 | async-start | bytes 1114112 | tf_op jit(solution)/shard_map/all_to_all | solution.py:82

commit v6 on v5

--- a/solution.py
+++ b/solution.py
@@ -93,7 +93,10 @@
 
 
 def norm_kernel(layer, n, *refs):
-    parts, (gain, xs, scale) = refs[:n], refs[n:]
+    parts, (gain, xs, scale, *spare) = refs[:n], refs[n:]
+    out = xs
+    if spare:
+        xs = spare[0]
 
     def squares(i, _):
         rows = pl.ds(pl.multiple_of(i * 16, 16), 16)
@@ -120,22 +123,37 @@
         return 0
 
     lax.fori_loop(0, steps, apply, 0, unroll=2)
-
-
-def mix_kernel(xs, mine, other, glu, vs, gs):
-    def fill(zy, yz):
+    if spare:
+        done = pltpu.make_async_copy(xs, out, spare[1])
+        done.start()
+        done.wait()
+
+
+def mix_kernel(xs, mine, source, glu, vs, gs, other, sems, *spare):
+    copies = [pltpu.make_async_copy(source, other, sems.at[0])]
+    if spare:
+        copies.append(pltpu.make_async_copy(xs, spare[0], sems.at[1]))
+        xs = spare[0]
+    for one in copies:
+        one.start()
+
+    def from_even(w):
         for z in range(NZ):
-            for c, w in enumerate((zy.at[z], yz.at[:, z])):
-                vs[z, :, c] = w[:, :16, :]
-                gs[z, :, c] = w[:, 16:32, :]
-
-    @pl.when(core_here() == 0)
-    def _():
-        fill(mine, other)
-
-    @pl.when(core_here() == 1)
-    def _():
-        fill(other, mine)
+            vs[z, :, 0] = w[z, :, :16, :]
+            gs[z, :, 0] = w[z, :, 16:32, :]
+
+    def from_odd(w):
+        for z in range(NZ):
+            vs[z, :, 1] = w[:, z, :16, :]
+            gs[z, :, 1] = w[:, z, 16:32, :]
+
+    even = core_here() == 0
+    pl.when(even)(lambda: from_even(mine))
+    pl.when(jnp.logical_not(even))(lambda: from_odd(mine))
+    for one in copies:
+        one.wait()
+    pl.when(even)(lambda: from_odd(other))
+    pl.when(jnp.logical_not(even))(lambda: from_even(other))
 
     value = jnp.zeros(glu.shape, F32)
     gate = jnp.zeros(glu.shape, F32)
@@ -303,28 +321,40 @@
     )(*ins)
 
 
-def normalise(layer, parts, gain):
+def normalise(layer, parts, gain, far):
     def body(*refs):
         norm_kernel(layer, len(parts), *refs)
 
+    shape = (NX, parts[0].shape[-2], FEAT)
+    scratch = [pltpu.VMEM((shape[1], 128), F32)]
+    if far:
+        scratch += [pltpu.VMEM(shape, BF), pltpu.SemaphoreType.DMA(())]
     return call(
         body,
-        jax.ShapeDtypeStruct((NX, parts[0].shape[-2], FEAT), BF),
+        pltpu.HBM(shape, BF) if far else jax.ShapeDtypeStruct(shape, BF),
         [*parts, gain],
-        [pltpu.VMEM((parts[0].shape[-2], 128), F32)],
+        scratch,
         8 * NX * TOK * FEAT,
-    )
-
-
-def mix(xs, mine, other):
+        pltpu.HBM if far else pltpu.VMEM,
+    )
+
+
+def mix(xs, mine, other, far):
     weights = pltpu.VMEM((NZ, NY, 2, 16, CH), BF)
-    return call(
+    scratch = [weights, weights, pltpu.VMEM(other.shape, BF), pltpu.SemaphoreType.DMA((2,))]
+    spots = [pltpu.HBM if far else pltpu.VMEM, pltpu.VMEM, pltpu.HBM]
+    return pl.pallas_call(
         mix_kernel,
-        jax.ShapeDtypeStruct((xs.shape[1], CH), BF),
-        [xs, mine, other],
-        [weights, weights],
-        4 * NX * TOK * FEAT * CH,
-    )
+        out_shape=jax.ShapeDtypeStruct((xs.shape[1], CH), BF),
+        in_specs=[pl.BlockSpec(memory_space=spot) for spot in spots],
+        out_specs=pl.BlockSpec(memory_space=pltpu.VMEM),
+        scratch_shapes=scratch + ([pltpu.VMEM(xs.shape, BF)] if far else []),
+        cost_estimate=pl.CostEstimate(
+            flops=4 * NX * TOK * FEAT * CH, transcendentals=0, bytes_accessed=1 << 20
+        ),
+        compiler_params=pltpu.CompilerParams(vmem_limit_bytes=14 << 20),
+        interpret=INTERPRET,
+    )(in_hbm(xs) if far else xs, mine, in_hbm(other))
 
 
 def arrange_kernel(mine, other, out, wt, sem):
@@ -414,7 +444,7 @@
 
     return call(
         body,
-        jax.ShapeDtypeStruct((NZ, NZ, 48, CH), BF),
+        pltpu.HBM((NZ, NZ, 48, CH), BF),
         [once],
         [pltpu.SemaphoreType.DMA((NZ,))],
         1 << 26,
@@ -458,18 +488,19 @@
     x = stream
     count = lax.axis_size("sp")
     chain = [(i, i + 1) for i in range(count - 1)]
-    extended = jnp.concatenate([lax.ppermute(x[TOK - TAPS :], "sp", chain), x])
+    extended = jnp.concatenate([lax.ppermute(x, "sp", chain)[TOK - TAPS :], x])
     once = lines(blocks)
     extended = after(extended, blocks)
-    parts = [extended, along_x(extended, 1), along_x(extended, 2)]
+    parts = [extended, along_x(extended, 2)]
+    parts[1:1] = [along_x(extended, 1)]
     parts.append(along_x(extended, 3))
     ready = spread(0, once)
     gathered = plane(ready)
     ready = spread(1, once)
-    normed = normalise(0, parts, gain)
+    normed = normalise(0, parts, gain, True)
     other = swap_cores(gathered)
     following = plane(after(ready, gathered))
-    glu = mix(normed, gathered, other)
+    glu = mix(normed, gathered, other, True)
     packed = conv_whole(0, glu, conv_taps, channel_gain)
     parts = from_all_x(packed)
     wt = arrange(after(gathered, packed), other)
@@ -477,8 +508,8 @@
 
     xs = exchange_x(copies)
     other = swap_cores(following)
-    normed = normalise(1, xs, gain)
-    glu = mix(normed, following, other)
+    normed = normalise(1, xs, gain, False)
+    glu = mix(normed, following, other, False)
     before = lax.ppermute(glu[TOK - TAPS :], "sp", chain)
     late = conv_late(1, glu, conv_taps)
     copies = convolve(1, before, glu, late, conv_taps, channel_gain)

time: 195 us -> 198 us (1.015)
  Pallas kernels: 27.2 us -> 29.7 us
    pallas_call x0 -> x2, Pallas kernels: none -> 5.23 us  [mix(): pl.pallas_call(mix_kernel, out_shape=jax.ShapeDtypeStruct((xs.shape[1], C...]
    pallas_call x11 -> x9, Pallas kernels: 22 us -> 19.2 us  [call(): pl.pallas_call(body, out_shape=out, in_specs=[pl.BlockSpec(memory_space=p...]
  transfers between devices with their start and end apart: 14 -> 14, of which waited for: 7 -> 8; matrix products, arithmetic and copies ran while one was open for 2% -> 2% of each run, Pallas kernels for 10% -> 11%
where the time goes in v6:
time: 198 us; the launch traced here: 197 us
  waiting for transfers between devices  61.2 us (31%)
  starting transfers between devices  53 us (27%)
  blocking collectives  48.3 us (24%)
  Pallas kernels  29.7 us (15%)
  local copies, waits for them, and re-layouts  3.16 us (2%)
    all_to_all x2, waiting for transfers between devices, plane(): lax.all_to_all(copies, 'sp', split_axis=0, concat_axis=0, tiled=True, axi...  37.6 us
    all_to_all x1, blocking collectives, to_group(): lax.all_to_all(copies, 'sp', split_axis=0, concat_axis=0, tiled=True, axi...  32.1 us
    ppermute x6, starting transfers between devices, along_x(): return lax.ppermute(v, 'x', [(i, (i + step) % NX) for i in range(NX)])  19.4 us
    pallas_call x9, Pallas kernels, call(): pl.pallas_call(body, out_shape=out, in_specs=[pl.BlockSpec(memory_space=p...  19.2 us
    all_to_all x1, blocking collectives, exchange_x(): lax.all_to_all(copies, 'x', split_axis=0, concat_axis=0, tiled=True)  16.2 us
    ppermute x2, starting transfers between devices, swap_cores(): return lax.ppermute(v, 'sp', [(i, i ^ 1) for i in range(count)])  16.1 us
    ppermute x6, waiting for transfers between devices, along_x(): return lax.ppermute(v, 'x', [(i, (i + step) % NX) for i in range(NX)])  15.7 us
    all_to_all x2, starting transfers between devices, plane(): lax.all_to_all(copies, 'sp', split_axis=0, concat_axis=0, tiled=True, axi...  8.03 us
  transfers between devices with their start and end apart: 14, of which 8 were waited for; matrix products, arithmetic and copies ran while one was open for 2% of the time, Pallas kernels for 11%

profile of v6, /device:TPU:1, one launch (start us, length us, event | category | flops | bytes accessed | tf_op | source)
XLA Modules:
  0.0 196.6 jit_solution(9608177367717921838)
XLA Ops:
  2.8 32.1 %all_to_all.25.refs_0_ = bf16[8,2,48,256]{3,2,1,0:T(8,128)(2,1)S(1)} all-to-all(bf16[8,2,48,256]{3,2,1,0:T(8,128)(2,1)S(1)} %broadcast_in_dim.3), channel_id=1, replica_groups={{0,8,16,24,32,40,48,56},{64,72,80,88,96,104,112,120},{128,136,144,152,1..., dimensions={0} | all-to-all | bytes 786432 | tf_op jit(solution)/shard_map/all_to_all | solution.py:35
  36.1 4.5 %all-to-all-start.1 = ((bf16[8,8,48,256]{3,2,1,0:T(8,128)(2,1)}), bf16[8,8,48,256]{3,2,1,0:T(8,128)(2,1)S(1)}, u32[]{:S(2)}, u32[]{:S(2)}) async-start(bf16[8,8,48,256]{3,2,1,0:T(8,128)(2,1)} %shard_map.74), calls=%async_computation.1 | async-start | bytes 3145728 | tf_op jit(solution)/shard_map/all_to_all | solution.py:45
  41.8 22.5 %all-to-all-done.1.mine = bf16[8,8,48,256]{3,2,1,0:T(8,128)(2,1)S(1)} async-done(((bf16[8,8,48,256]{3,2,1,0:T(8,128)(2,1)}), bf16[8,8,48,256]{3,2,1,0:T(8,128)(2,1)S(1)}, u32[]{:S(2)}, u32[]{:S(2)}) %all-to-all-start.1) | async-done | bytes 1572896 | tf_op jit(solution)/shard_map/all_to_all | solution.py:45
  64.3 3.6 %all-to-all-start.3 = ((bf16[8,8,48,256]{3,2,1,0:T(8,128)(2,1)}), bf16[8,8,48,256]{3,2,1,0:T(8,128)(2,1)S(1)}, u32[]{:S(2)}, u32[]{:S(2)}) async-start(bf16[8,8,48,256]{3,2,1,0:T(8,128)(2,1)} %shard_map.80), calls=%async_computation.3 | async-start | bytes 3145728 | tf_op jit(solution)/shard_map/all_to_all | solution.py:45
  67.9 6.1 %collective-permute-start.5 = (bf16[8,8,48,256]{3,2,1,0:T(8,128)(2,1)S(1)}, bf16[8,8,48,256]{3,2,1,0:T(8,128)(2,1)}, u32[]{:S(2)}, u32[]{:S(2)}) collective-permute-start(bf16[8,8,48,256]{3,2,1,0:T(8,128)(2,1)S(1)} %all-to-all-done.1.mine), channel_id=1, source_target_pairs={{0,4},{4,0},{8,12},{12,8},{16,20},{20,16},{24,28},{28,24},{32,36},... | collective-permute-start | bytes 4718600 | tf_op jit(solution)/shard_map/ppermute | solution.py:57
  76.1 15.2 %all-to-all-done.3.mine = bf16[8,8,48,256]{3,2,1,0:T(8,128)(2,1)S(1)} async-done(((bf16[8,8,48,256]{3,2,1,0:T(8,128)(2,1)}), bf16[8,8,48,256]{3,2,1,0:T(8,128)(2,1)S(1)}, u32[]{:S(2)}, u32[]{:S(2)}) %all-to-all-start.3) | async-done | bytes 1572896 | tf_op jit(solution)/shard_map/all_to_all | solution.py:45
  91.3 10.0 %collective-permute-start.9 = (bf16[8,8,48,256]{3,2,1,0:T(8,128)(2,1)S(1)}, bf16[8,8,48,256]{3,2,1,0:T(8,128)(2,1)}, u32[]{:S(2)}, u32[]{:S(2)}) collective-permute-start(bf16[8,8,48,256]{3,2,1,0:T(8,128)(2,1)S(1)} %all-to-all-done.3.mine), channel_id=1, source_target_pairs={{0,4},{4,0},{8,12},{12,8},{16,20},{20,16},{24,28},{28,24},{32,36},... | collective-permute-start | bytes 4718600 | tf_op jit(solution)/shard_map/ppermute | solution.py:57
  103.2 3.2 %collective-permute-start.2 = (bf16[384,512]{1,0:T(8,128)(2,1)S(1)}, bf16[384,512]{1,0:T(8,128)(2,1)}, u32[]{:S(2)}, u32[]{:S(2)}) collective-permute-start(bf16[384,512]{1,0:T(8,128)(2,1)S(1)} %pad_maximum_fusion.refs_0_), channel_id=1, source_target_pairs={{0,1},{1,2},{2,3},{3,0},{4,5},{5,6},{6,7},{7,4},{8,9},{9,10},{10,1... | collective-permute-start | bytes 1179656 | tf_op jit(solution)/shard_map/ppermute | solution.py:74
  108.3 4.3 %collective-permute-start.4 = (bf16[384,512]{1,0:T(8,128)(2,1)S(1)}, bf16[384,512]{1,0:T(8,128)(2,1)}, u32[]{:S(2)}, u32[]{:S(2)}) collective-permute-start(bf16[384,512]{1,0:T(8,128)(2,1)S(1)} %pad_maximum_fusion.refs_0_), channel_id=1, source_target_pairs={{0,3},{1,0},{2,1},{3,2},{4,7},{5,4},{6,5},{7,6},{8,11},{9,8},{10,9... | collective-permute-start | bytes 1179656 | tf_op jit(solution)/shard_map/ppermute | solution.py:74
  113.4 12.1 %collective-permute-done.2.refs_1_ = bf16[384,512]{1,0:T(8,128)(2,1)} collective-permute-done((bf16[384,512]{1,0:T(8,128)(2,1)S(1)}, bf16[384,512]{1,0:T(8,128)(2,1)}, u32[]{:S(2)}, u32[]{:S(2)}) %collective-permute-start.2) | collective-permute-done | bytes 393248 | tf_op jit(solution)/shard_map/ppermute | solution.py:74
  127.8 3.4 %shard_map.73.xs = bf16[4,384,512]{2,1,0:T(8,128)(2,1)} custom-call(bf16[384,512]{1,0:T(8,128)(2,1)S(1)} %pad_maximum_fusion.refs_0_, bf16[384,512]{1,0:T(8,128)(2,1)} %collective-permute-done.2.refs_1_, bf16[384,512]{1,0:T(8,128)(2,1)} %collective-permute-done.3.refs_2_, bf16[384,512]{1,0:T(8,128)(2,1)} %collective-permute-done.4.refs_3_, ...), custom_call_target="tpu_custom_call" | custom-call | flops 4194304 | bytes 1048576 | tf_op jit(solution)/shard_map/pallas_call | solution.py:312
  131.2 3.0 %shard_map.75.refs_0_ = bf16[384,256]{1,0:T(8,128)(2,1)S(1)} custom-call(bf16[4,384,512]{2,1,0:T(8,128)(2,1)} %shard_map.73.xs, bf16[8,8,48,256]{3,2,1,0:T(8,128)(2,1)S(1)} %all-to-all-done.1.mine, bf16[8,8,48,256]{3,2,1,0:T(8,128)(2,1)} %collective-permute-done.5.source.other), custom_call_target="tpu_custom_call" | custom-call | flops 536870912 | bytes 1048576 | tf_op jit(solution)/shard_map/pallas_call | solution.py:346
  134.2 3.4 %shard_map.76.refs_0_ = bf16[272,256]{1,0:T(8,128)(2,1)S(1)} custom-call(bf16[384,256]{1,0:T(8,128)(2,1)S(1)} %shard_map.75.refs_0_, f32[2,128,256]{2,1,0:T(8,128)S(1)} %copy-done.1, f32[2,256]{1,0:T(2,128)S(1)} %copy-done.2), custom_call_target="tpu_custom_call" | custom-call | flops 16777216 | bytes 1048576 | tf_op jit(solution)/shard_map/pallas_call | solution.py:312
  137.6 3.5 %collective-permute-start.6 = (bf16[272,256]{1,0:T(8,128)(2,1)S(1)}, bf16[272,256]{1,0:T(8,128)(2,1)S(1)}, u32[]{:S(2)}, u32[]{:S(2)}) collective-permute-start(bf16[272,256]{1,0:T(8,128)(2,1)S(1)} %shard_map.76.refs_0_), channel_id=1, source_target_pairs={{0,1},{1,2},{2,3},{3,0},{4,5},{5,6},{6,7},{7,4},{8,9},{9,10},{10,1... | collective-permute-start | bytes 417800 | tf_op jit(solution)/shard_map/ppermute | solution.py:74
  141.2 4.5 %collective-permute-start.7 = (bf16[272,256]{1,0:T(8,128)(2,1)S(1)}, bf16[272,256]{1,0:T(8,128)(2,1)S(1)}, u32[]{:S(2)}, u32[]{:S(2)}) collective-permute-start(bf16[272,256]{1,0:T(8,128)(2,1)S(1)} %shard_map.76.refs_0_), channel_id=1, source_target_pairs={{0,2},{1,3},{2,0},{3,1},{4,6},{5,7},{6,4},{7,5},{8,10},{9,11},{10,... | collective-permute-start | bytes 417800 | tf_op jit(solution)/shard_map/ppermute | solution.py:74
  147.6 2.5 %shard_map.77.refs_5_ = bf16[4,2,8,2,16,256]{5,4,3,2,1,0:T(8,128)(2,1)} custom-call(bf16[8,8,48,256]{3,2,1,0:T(8,128)(2,1)S(1)} %all-to-all-done.1.mine, bf16[8,8,48,256]{3,2,1,0:T(8,128)(2,1)} %collective-permute-done.5.source.other), custom_call_target="tpu_custom_call" | custom-call | flops 67108864 | bytes 1048576 | tf_op jit(solution)/shard_map/pallas_call | solution.py:312
  151.5 2.8 %shard_map.78 = bf16[4,256,512]{2,1,0:T(8,128)(2,1)} custom-call(bf16[272,256]{1,0:T(8,128)(2,1)S(1)} %shard_map.76.refs_0_, bf16[272,256]{1,0:T(8,128)(2,1)S(1)} %collective-permute-done.6.refs_1_, bf16[272,256]{1,0:T(8,128)(2,1)S(1)} %collective-permute-done.7.refs_2_, bf16[272,256]{1,0:T(8,128)(2,1)S(1)} %collective-permute-done.8.refs_3_, ...), custom_call_target="tpu_custom_call" | custom-call | flops 268435456 | bytes 1048576 | tf_op jit(solution)/shard_map/pallas_call | solution.py:462
  154.2 16.2 %all_to_all.26.refs_0_.refs_1_ = bf16[4,256,512]{2,1,0:T(8,128)(2,1)S(1)} all-to-all(bf16[4,256,512]{2,1,0:T(8,128)(2,1)} %shard_map.78), channel_id=1, replica_groups=mesh['sp'=128,'tp'=4] {'tp'}, dimensions={0} | all-to-all | bytes 2097152 | tf_op jit(solution)/shard_map/all_to_all | solution.py:82
  173.4 2.6 %collective-permute-start.10 = (bf16[128,256]{1,0:T(8,128)(2,1)S(1)}, bf16[128,256]{1,0:T(8,128)(2,1)S(1)}, u32[]{:S(2)}, u32[]{:S(2)}) collective-permute-start(bf16[128,256]{1,0:T(8,128)(2,1)S(1)} %slice.9), channel_id=1, source_target_pairs={{0,4},{4,8},{8,12},{12,16},{16,20},{20,24},{24,28},{28,32},{32,36}... | collective-permute-start | bytes 196616 | tf_op jit(solution)/shard_map/ppermute | solution.py:513
  178.8 2.8 %shard_map.83 = bf16[4,272,256]{2,1,0:T(8,128)(2,1)} custom-call(bf16[128,256]{1,0:T(8,128)(2,1)S(1)} %collective-permute-done.10.refs_0_, bf16[256,256]{1,0:T(8,128)(2,1)S(1)} %shard_map.81.refs_0_.refs_1_, f32[128,256]{1,0:T(8,128)S(1)} %shard_map.82.refs_2_, f32[2,128,256]{2,1,0:T(8,128)S(1)} %copy-done.1, f32[2,256]{1,0:T(2,128)S(1)} %copy-done.2), custom_call_target="tpu_custom_call" | custom-call | flops 8388608 | bytes 1048576 | tf_op jit(solution)/shard_map/pallas_call | solution.py:312
  181.6 3.5 %all-to-all-start.4 = ((bf16[4,272,256]{2,1,0:T(8,128)(2,1)}), bf16[4,272,256]{2,1,0:T(8,128)(2,1)S(1)}, u32[]{:S(2)}, u32[]{:S(2)}) async-start(bf16[4,272,256]{2,1,0:T(8,128)(2,1)} %shard_map.83), calls=%async_computation.4 | async-start | bytes 1114112 | tf_op jit(solution)/shard_map/all_to_all | solution.py:82
  185.1 2.5 %shard_map.84.refs_2_ = bf16[4,2,8,2,16,256]{5,4,3,2,1,0:T(8,128)(2,1)} custom-call(bf16[8,8,48,256]{3,2,1,0:T(8,128)(2,1)S(1)} %all-to-all-done.3.mine, bf16[8,8,48,256]{3,2,1,0:T(8,128)(2,1)} %collective-permute-done.9.source.other), custom_call_target="tpu_custom_call" | custom-call | flops 67108864 | bytes 1048576 | tf_op jit(solution)/shard_map/pallas_call | solution.py:312
  187.5 6.6 %all-to-all-done.4.refs_0_ = bf16[4,272,256]{2,1,0:T(8,128)(2,1)S(1)} async-done(((bf16[4,272,256]{2,1,0:T(8,128)(2,1)}), bf16[4,272,256]{2,1,0:T(8,128)(2,1)S(1)}, u32[]{:S(2)}, u32[]{:S(2)}) %all-to-all-start.4) | async-done | bytes 557088 | tf_op jit(solution)/shard_map/all_to_all | solution.py:82
  194.1 2.5 %shard_map.85 = bf16[256,512]{1,0:T(8,128)(2,1)} custom-call(bf16[4,272,256]{2,1,0:T(8,128)(2,1)S(1)} %all-to-all-done.4.refs_0_, bf16[4,256,512]{2,1,0:T(8,128)(2,1)} %copy-done, bf16[4,2,8,2,16,256]{5,4,3,2,1,0:T(8,128)(2,1)} %shard_map.84.refs_2_), custom_call_target="tpu_custom_call" | custom-call | flops 268435456 | bytes 1048576 | tf_op jit(solution)/shard_map/pallas_call | solution.py:462
  (35 shorter events, 23.2 us)
Async XLA Ops:
  0.0 2.8 %collective-permute-start.1 = (bf16[2,16,256]{2,1,0:T(8,128)(2,1)}, bf16[2,16,256]{2,1,0:T(8,128)(2,1)S(1)}, u32[]{:S(2)}, u32[]{:S(2)}) collective-permute-start(bf16[2,16,256]{2,1,0:T(8,128)(2,1)} %bitcast.1), channel_id=1, source_target_pairs={{0,0},{1,128},{2,256},{3,384},{4,4},{5,20},{6,36},{7,52},{8,8},{9,... | collective-permute-start | bytes 49160 | tf_op jit(solution)/shard_map/ppermute | solution.py:70
  36.1 28.2 %all-to-all-start.1 = ((bf16[8,8,48,256]{3,2,1,0:T(8,128)(2,1)}), bf16[8,8,48,256]{3,2,1,0:T(8,128)(2,1)S(1)}, u32[]{:S(2)}, u32[]{:S(2)}) async-start(bf16[8,8,48,256]{3,2,1,0:T(8,128)(2,1)} %shard_map.74), calls=%async_computation.1 | async-start | bytes 3145728 | tf_op jit(solution)/shard_map/all_to_all | solution.py:45
  41.8 32.2 %copy-start.3 = (bf16[256,512]{1,0:T(8,128)(2,1)S(1)}, bf16[256,512]{1,0:T(8,128)(2,1)}, u32[]{:S(2)}) copy-start(bf16[256,512]{1,0:T(8,128)(2,1)} %refs_4_.2) | copy-start | bytes 786436
  64.3 27.0 %all-to-all-start.3 = ((bf16[8,8,48,256]{3,2,1,0:T(8,128)(2,1)}), bf16[8,8,48,256]{3,2,1,0:T(8,128)(2,1)S(1)}, u32[]{:S(2)}, u32[]{:S(2)}) async-start(bf16[8,8,48,256]{3,2,1,0:T(8,128)(2,1)} %shard_map.80), calls=%async_computation.3 | async-start | bytes 3145728 | tf_op jit(solution)/shard_map/all_to_all | solution.py:45
  67.9 63.3 %collective-permute-start.5 = (bf16[8,8,48,256]{3,2,1,0:T(8,128)(2,1)S(1)}, bf16[8,8,48,256]{3,2,1,0:T(8,128)(2,1)}, u32[]{:S(2)}, u32[]{:S(2)}) collective-permute-start(bf16[8,8,48,256]{3,2,1,0:T(8,128)(2,1)S(1)} %all-to-all-done.1.mine), channel_id=1, source_target_pairs={{0,4},{4,0},{8,12},{12,8},{16,20},{20,16},{24,28},{28,24},{32,36},... | collective-permute-start | bytes 4718600 | tf_op jit(solution)/shard_map/ppermute | solution.py:57
  74.0 27.3 %collective-permute-start = (bf16[256,512]{1,0:T(8,128)(2,1)S(1)}, bf16[256,512]{1,0:T(8,128)(2,1)}, u32[]{:S(2)}, u32[]{:S(2)}) collective-permute-start(bf16[256,512]{1,0:T(8,128)(2,1)S(1)} %copy-done.3), channel_id=1, source_target_pairs={{0,4},{4,8},{8,12},{12,16},{16,20},{20,24},{24,28},{28,32},{32,36}... | collective-permute-start | bytes 786440 | tf_op jit(solution)/shard_map/ppermute | solution.py:491
  91.3 79.8 %collective-permute-start.9 = (bf16[8,8,48,256]{3,2,1,0:T(8,128)(2,1)S(1)}, bf16[8,8,48,256]{3,2,1,0:T(8,128)(2,1)}, u32[]{:S(2)}, u32[]{:S(2)}) collective-permute-start(bf16[8,8,48,256]{3,2,1,0:T(8,128)(2,1)S(1)} %all-to-all-done.3.mine), channel_id=1, source_target_pairs={{0,4},{4,0},{8,12},{12,8},{16,20},{20,16},{24,28},{28,24},{32,36},... | collective-permute-start | bytes 4718600 | tf_op jit(solution)/shard_map/ppermute | solution.py:57
  103.2 22.3 %collective-permute-start.2 = (bf16[384,512]{1,0:T(8,128)(2,1)S(1)}, bf16[384,512]{1,0:T(8,128)(2,1)}, u32[]{:S(2)}, u32[]{:S(2)}) collective-permute-start(bf16[384,512]{1,0:T(8,128)(2,1)S(1)} %pad_maximum_fusion.refs_0_), channel_id=1, source_target_pairs={{0,1},{1,2},{2,3},{3,0},{4,5},{5,6},{6,7},{7,4},{8,9},{9,10},{10,1... | collective-permute-start | bytes 1179656 | tf_op jit(solution)/shard_map/ppermute | solution.py:74
  106.4 19.1 %collective-permute-start.3 = (bf16[384,512]{1,0:T(8,128)(2,1)S(1)}, bf16[384,512]{1,0:T(8,128)(2,1)}, u32[]{:S(2)}, u32[]{:S(2)}) collective-permute-start(bf16[384,512]{1,0:T(8,128)(2,1)S(1)} %pad_maximum_fusion.refs_0_), channel_id=1, source_target_pairs={{0,2},{1,3},{2,0},{3,1},{4,6},{5,7},{6,4},{7,5},{8,10},{9,11},{10,... | collective-permute-start | bytes 1179656 | tf_op jit(solution)/shard_map/ppermute | solution.py:74
  108.3 19.4 %collective-permute-start.4 = (bf16[384,512]{1,0:T(8,128)(2,1)S(1)}, bf16[384,512]{1,0:T(8,128)(2,1)}, u32[]{:S(2)}, u32[]{:S(2)}) collective-permute-start(bf16[384,512]{1,0:T(8,128)(2,1)S(1)} %pad_maximum_fusion.refs_0_), channel_id=1, source_target_pairs={{0,3},{1,0},{2,1},{3,2},{4,7},{5,4},{6,5},{7,6},{8,11},{9,8},{10,9... | collective-permute-start | bytes 1179656 | tf_op jit(solution)/shard_map/ppermute | solution.py:74
  131.2 3.1 %copy-start.1 = (f32[2,128,256]{2,1,0:T(8,128)S(1)}, f32[2,128,256]{2,1,0:T(8,128)}, u32[]{:S(2)}) copy-start(f32[2,128,256]{2,1,0:T(8,128)} %refs_3_.1) | copy-start | bytes 786436
  131.2 3.0 %copy-start.2 = (f32[2,256]{1,0:T(2,128)S(1)}, f32[2,256]{1,0:T(2,128)}, u32[]{:S(2)}) copy-start(f32[2,256]{1,0:T(2,128)} %refs_4_.3) | copy-start | bytes 6148
  137.6 12.5 %collective-permute-start.6 = (bf16[272,256]{1,0:T(8,128)(2,1)S(1)}, bf16[272,256]{1,0:T(8,128)(2,1)S(1)}, u32[]{:S(2)}, u32[]{:S(2)}) collective-permute-start(bf16[272,256]{1,0:T(8,128)(2,1)S(1)} %shard_map.76.refs_0_), channel_id=1, source_target_pairs={{0,1},{1,2},{2,3},{3,0},{4,5},{5,6},{6,7},{7,4},{8,9},{9,10},{10,1... | collective-permute-start | bytes 417800 | tf_op jit(solution)/shard_map/ppermute | solution.py:74
  141.2 9.1 %collective-permute-start.7 = (bf16[272,256]{1,0:T(8,128)(2,1)S(1)}, bf16[272,256]{1,0:T(8,128)(2,1)S(1)}, u32[]{:S(2)}, u32[]{:S(2)}) collective-permute-start(bf16[272,256]{1,0:T(8,128)(2,1)S(1)} %shard_map.76.refs_0_), channel_id=1, source_target_pairs={{0,2},{1,3},{2,0},{3,1},{4,6},{5,7},{6,4},{7,5},{8,10},{9,11},{10,... | collective-permute-start | bytes 417800 | tf_op jit(solution)/shard_map/ppermute | solution.py:74
  145.7 5.8 %collective-permute-start.8 = (bf16[272,256]{1,0:T(8,128)(2,1)S(1)}, bf16[272,256]{1,0:T(8,128)(2,1)S(1)}, u32[]{:S(2)}, u32[]{:S(2)}) collective-permute-start(bf16[272,256]{1,0:T(8,128)(2,1)S(1)} %shard_map.76.refs_0_), channel_id=1, source_target_pairs={{0,3},{1,0},{2,1},{3,2},{4,7},{5,4},{6,5},{7,6},{8,11},{9,8},{10,9... | collective-permute-start | bytes 417800 | tf_op jit(solution)/shard_map/ppermute | solution.py:74
  170.5 2.9 %copy-start = (bf16[4,256,512]{2,1,0:T(8,128)(2,1)}, bf16[4,256,512]{2,1,0:T(8,128)(2,1)S(1)}, u32[]{:S(2)}) copy-start(bf16[4,256,512]{2,1,0:T(8,128)(2,1)S(1)} %all_to_all.26.refs_0_.refs_1_) | copy-start | bytes 3145732
  173.4 5.4 %collective-permute-start.10 = (bf16[128,256]{1,0:T(8,128)(2,1)S(1)}, bf16[128,256]{1,0:T(8,128)(2,1)S(1)}, u32[]{:S(2)}, u32[]{:S(2)}) collective-permute-start(bf16[128,256]{1,0:T(8,128)(2,1)S(1)} %slice.9), channel_id=1, source_target_pairs={{0,4},{4,8},{8,12},{12,16},{16,20},{20,24},{24,28},{28,32},{32,36}... | collective-permute-start | bytes 196616 | tf_op jit(solution)/shard_map/ppermute | solution.py:513
  181.6 12.5 %all-to-all-start.4 = ((bf16[4,272,256]{2,1,0:T(8,128)(2,1)}), bf16[4,272,256]{2,1,0:T(8,128)(2,1)S(1)}, u32[]{:S(2)}, u32[]{:S(2)}) async-start(bf16[4,272,256]{2,1,0:T(8,128)(2,1)} %shard_map.83), calls=%async_computation.4 | async-start | bytes 1114112 | tf_op jit(solution)/shard_map/all_to_all | solution.py:82

commit v7 on v6

--- a/solution.py
+++ b/solution.py
@@ -75,7 +75,8 @@
 
 
 def from_all_x(v):
-    return [v] + [along_x(v, step) for step in range(1, NX)]
+    two = along_x(v, 2)
+    return [v, along_x(v, 1), two, along_x(v, 3)]
 
 
 def exchange_x(copies):
@@ -129,13 +130,14 @@
         done.wait()
 
 
-def mix_kernel(xs, mine, source, glu, vs, gs, other, sems, *spare):
+def mix_kernel(held, gain, mine, source, glu, vs, gs, other, sems, xs, *spare):
     copies = [pltpu.make_async_copy(source, other, sems.at[0])]
-    if spare:
-        copies.append(pltpu.make_async_copy(xs, spare[0], sems.at[1]))
-        xs = spare[0]
+    if not spare:
+        copies.append(pltpu.make_async_copy(held, xs, sems.at[1]))
     for one in copies:
         one.start()
+    if spare:
+        norm_kernel(1, 1, held, gain, xs, spare[0])
 
     def from_even(w):
         for z in range(NZ):
@@ -321,40 +323,40 @@
     )(*ins)
 
 
-def normalise(layer, parts, gain, far):
+def normalise(layer, parts, gain):
     def body(*refs):
         norm_kernel(layer, len(parts), *refs)
 
     shape = (NX, parts[0].shape[-2], FEAT)
-    scratch = [pltpu.VMEM((shape[1], 128), F32)]
-    if far:
-        scratch += [pltpu.VMEM(shape, BF), pltpu.SemaphoreType.DMA(())]
     return call(
         body,
-        pltpu.HBM(shape, BF) if far else jax.ShapeDtypeStruct(shape, BF),
+        pltpu.HBM(shape, BF),
         [*parts, gain],
-        scratch,
+        [pltpu.VMEM((shape[1], 128), F32), pltpu.VMEM(shape, BF), pltpu.SemaphoreType.DMA(())],
         8 * NX * TOK * FEAT,
-        pltpu.HBM if far else pltpu.VMEM,
-    )
-
-
-def mix(xs, mine, other, far):
+        pltpu.HBM,
+    )
+
+
+def mix(xs, gain, mine, other, far):
     weights = pltpu.VMEM((NZ, NY, 2, 16, CH), BF)
     scratch = [weights, weights, pltpu.VMEM(other.shape, BF), pltpu.SemaphoreType.DMA((2,))]
-    spots = [pltpu.HBM if far else pltpu.VMEM, pltpu.VMEM, pltpu.HBM]
+    scratch.append(pltpu.VMEM(xs.shape, BF))
+    if not far:
+        scratch.append(pltpu.VMEM((TOK, 128), F32))
+    spots = [pltpu.HBM if far else pltpu.VMEM, pltpu.VMEM, pltpu.VMEM, pltpu.HBM]
     return pl.pallas_call(
         mix_kernel,
         out_shape=jax.ShapeDtypeStruct((xs.shape[1], CH), BF),
         in_specs=[pl.BlockSpec(memory_space=spot) for spot in spots],
         out_specs=pl.BlockSpec(memory_space=pltpu.VMEM),
-        scratch_shapes=scratch + ([pltpu.VMEM(xs.shape, BF)] if far else []),
+        scratch_shapes=scratch,
         cost_estimate=pl.CostEstimate(
             flops=4 * NX * TOK * FEAT * CH, transcendentals=0, bytes_accessed=1 << 20
         ),
         compiler_params=pltpu.CompilerParams(vmem_limit_bytes=14 << 20),
         interpret=INTERPRET,
-    )(in_hbm(xs) if far else xs, mine, in_hbm(other))
+    )(in_hbm(xs) if far else xs, gain, mine, in_hbm(other))
 
 
 def arrange_kernel(mine, other, out, wt, sem):
@@ -497,10 +499,10 @@
     ready = spread(0, once)
     gathered = plane(ready)
     ready = spread(1, once)
-    normed = normalise(0, parts, gain, True)
+    normed = normalise(0, parts, gain)
     other = swap_cores(gathered)
     following = plane(after(ready, gathered))
-    glu = mix(normed, gathered, other, True)
+    glu = mix(normed, gain, gathered, other, True)
     packed = conv_whole(0, glu, conv_taps, channel_gain)
     parts = from_all_x(packed)
     wt = arrange(after(gathered, packed), other)
@@ -508,8 +510,7 @@
 
     xs = exchange_x(copies)
     other = swap_cores(following)
-    normed = normalise(1, xs, gain, False)
-    glu = mix(normed, following, other, False)
+    glu = mix(xs[0], gain, following, other, False)
     before = lax.ppermute(glu[TOK - TAPS :], "sp", chain)
     late = conv_late(1, glu, conv_taps)
     copies = convolve(1, before, glu, late, conv_taps, channel_gain)

time: 198 us -> 197 us (level)
    pallas_call x9 -> x8, Pallas kernels: 19.2 us -> 18.5 us  [call(): pl.pallas_call(body, out_shape=out, in_specs=[pl.BlockSpec(memory_space=p...]
  transfers between devices with their start and end apart: 14 -> 14, of which waited for: 8 -> 8; matrix products, arithmetic and copies ran while one was open for 2% -> 2% of each run, Pallas kernels for 11% -> 10%
where the time goes in v7:
time: 197 us; the launch traced here: 196 us
  waiting for transfers between devices  61.2 us (31%)
  starting transfers between devices  53 us (27%)
  blocking collectives  48.3 us (25%)
  Pallas kernels  29.4 us (15%)
  local copies, waits for them, and re-layouts  3.16 us (2%)
    all_to_all x2, waiting for transfers between devices, plane(): lax.all_to_all(copies, 'sp', split_axis=0, concat_axis=0, tiled=True, axi...  37.6 us
    all_to_all x1, blocking collectives, to_group(): lax.all_to_all(copies, 'sp', split_axis=0, concat_axis=0, tiled=True, axi...  32.1 us
    ppermute x6, starting transfers between devices, along_x(): return lax.ppermute(v, 'x', [(i, (i + step) % NX) for i in range(NX)])  19.4 us
    pallas_call x8, Pallas kernels, call(): pl.pallas_call(body, out_shape=out, in_specs=[pl.BlockSpec(memory_space=p...  18.5 us
    all_to_all x1, blocking collectives, exchange_x(): lax.all_to_all(copies, 'x', split_axis=0, concat_axis=0, tiled=True)  16.2 us
    ppermute x2, starting transfers between devices, swap_cores(): return lax.ppermute(v, 'sp', [(i, i ^ 1) for i in range(count)])  16.1 us
    ppermute x6, waiting for transfers between devices, along_x(): return lax.ppermute(v, 'x', [(i, (i + step) % NX) for i in range(NX)])  15.7 us
    all_to_all x2, starting transfers between devices, plane(): lax.all_to_all(copies, 'sp', split_axis=0, concat_axis=0, tiled=True, axi...  8.03 us
  transfers between devices with their start and end apart: 14, of which 8 were waited for; matrix products, arithmetic and copies ran while one was open for 2% of the time, Pallas kernels for 10%

profile of v7, /device:TPU:1, one launch (start us, length us, event | category | flops | bytes accessed | tf_op | source)
XLA Modules:
  0.0 196.2 jit_solution(10499470023598882930)
XLA Ops:
  2.8 32.1 %all_to_all.25.refs_0_ = bf16[8,2,48,256]{3,2,1,0:T(8,128)(2,1)S(1)} all-to-all(bf16[8,2,48,256]{3,2,1,0:T(8,128)(2,1)S(1)} %broadcast_in_dim.3), channel_id=1, replica_groups={{0,8,16,24,32,40,48,56},{64,72,80,88,96,104,112,120},{128,136,144,152,1..., dimensions={0} | all-to-all | bytes 786432 | tf_op jit(solution)/shard_map/all_to_all | solution.py:35
  36.1 4.5 %all-to-all-start.1 = ((bf16[8,8,48,256]{3,2,1,0:T(8,128)(2,1)}), bf16[8,8,48,256]{3,2,1,0:T(8,128)(2,1)S(1)}, u32[]{:S(2)}, u32[]{:S(2)}) async-start(bf16[8,8,48,256]{3,2,1,0:T(8,128)(2,1)} %shard_map.74), calls=%async_computation.1 | async-start | bytes 3145728 | tf_op jit(solution)/shard_map/all_to_all | solution.py:45
  41.8 22.5 %all-to-all-done.1.mine = bf16[8,8,48,256]{3,2,1,0:T(8,128)(2,1)S(1)} async-done(((bf16[8,8,48,256]{3,2,1,0:T(8,128)(2,1)}), bf16[8,8,48,256]{3,2,1,0:T(8,128)(2,1)S(1)}, u32[]{:S(2)}, u32[]{:S(2)}) %all-to-all-start.1) | async-done | bytes 1572896 | tf_op jit(solution)/shard_map/all_to_all | solution.py:45
  64.3 3.6 %all-to-all-start.3 = ((bf16[8,8,48,256]{3,2,1,0:T(8,128)(2,1)}), bf16[8,8,48,256]{3,2,1,0:T(8,128)(2,1)S(1)}, u32[]{:S(2)}, u32[]{:S(2)}) async-start(bf16[8,8,48,256]{3,2,1,0:T(8,128)(2,1)} %shard_map.79), calls=%async_computation.3 | async-start | bytes 3145728 | tf_op jit(solution)/shard_map/all_to_all | solution.py:45
  67.9 6.1 %collective-permute-start.5 = (bf16[8,8,48,256]{3,2,1,0:T(8,128)(2,1)S(1)}, bf16[8,8,48,256]{3,2,1,0:T(8,128)(2,1)}, u32[]{:S(2)}, u32[]{:S(2)}) collective-permute-start(bf16[8,8,48,256]{3,2,1,0:T(8,128)(2,1)S(1)} %all-to-all-done.1.mine), channel_id=1, source_target_pairs={{0,4},{4,0},{8,12},{12,8},{16,20},{20,16},{24,28},{28,24},{32,36},... | collective-permute-start | bytes 4718600 | tf_op jit(solution)/shard_map/ppermute | solution.py:57
  76.1 15.2 %all-to-all-done.3.mine = bf16[8,8,48,256]{3,2,1,0:T(8,128)(2,1)S(1)} async-done(((bf16[8,8,48,256]{3,2,1,0:T(8,128)(2,1)}), bf16[8,8,48,256]{3,2,1,0:T(8,128)(2,1)S(1)}, u32[]{:S(2)}, u32[]{:S(2)}) %all-to-all-start.3) | async-done | bytes 1572896 | tf_op jit(solution)/shard_map/all_to_all | solution.py:45
  91.3 10.0 %collective-permute-start.9 = (bf16[8,8,48,256]{3,2,1,0:T(8,128)(2,1)S(1)}, bf16[8,8,48,256]{3,2,1,0:T(8,128)(2,1)}, u32[]{:S(2)}, u32[]{:S(2)}) collective-permute-start(bf16[8,8,48,256]{3,2,1,0:T(8,128)(2,1)S(1)} %all-to-all-done.3.mine), channel_id=1, source_target_pairs={{0,4},{4,0},{8,12},{12,8},{16,20},{20,16},{24,28},{28,24},{32,36},... | collective-permute-start | bytes 4718600 | tf_op jit(solution)/shard_map/ppermute | solution.py:57
  103.2 3.2 %collective-permute-start.2 = (bf16[384,512]{1,0:T(8,128)(2,1)S(1)}, bf16[384,512]{1,0:T(8,128)(2,1)}, u32[]{:S(2)}, u32[]{:S(2)}) collective-permute-start(bf16[384,512]{1,0:T(8,128)(2,1)S(1)} %pad_maximum_fusion.refs_0_), channel_id=1, source_target_pairs={{0,1},{1,2},{2,3},{3,0},{4,5},{5,6},{6,7},{7,4},{8,9},{9,10},{10,1... | collective-permute-start | bytes 1179656 | tf_op jit(solution)/shard_map/ppermute | solution.py:74
  108.3 4.3 %collective-permute-start.4 = (bf16[384,512]{1,0:T(8,128)(2,1)S(1)}, bf16[384,512]{1,0:T(8,128)(2,1)}, u32[]{:S(2)}, u32[]{:S(2)}) collective-permute-start(bf16[384,512]{1,0:T(8,128)(2,1)S(1)} %pad_maximum_fusion.refs_0_), channel_id=1, source_target_pairs={{0,3},{1,0},{2,1},{3,2},{4,7},{5,4},{6,5},{7,6},{8,11},{9,8},{10,9... | collective-permute-start | bytes 1179656 | tf_op jit(solution)/shard_map/ppermute | solution.py:74
  113.4 12.1 %collective-permute-done.2.refs_1_ = bf16[384,512]{1,0:T(8,128)(2,1)} collective-permute-done((bf16[384,512]{1,0:T(8,128)(2,1)S(1)}, bf16[384,512]{1,0:T(8,128)(2,1)}, u32[]{:S(2)}, u32[]{:S(2)}) %collective-permute-start.2) | collective-permute-done | bytes 393248 | tf_op jit(solution)/shard_map/ppermute | solution.py:74
  127.8 3.4 %shard_map.73.held = bf16[4,384,512]{2,1,0:T(8,128)(2,1)} custom-call(bf16[384,512]{1,0:T(8,128)(2,1)S(1)} %pad_maximum_fusion.refs_0_, bf16[384,512]{1,0:T(8,128)(2,1)} %collective-permute-done.2.refs_1_, bf16[384,512]{1,0:T(8,128)(2,1)} %collective-permute-done.3.refs_2_, bf16[384,512]{1,0:T(8,128)(2,1)} %collective-permute-done.4.refs_3_, ...), custom_call_target="tpu_custom_call" | custom-call | flops 4194304 | bytes 1048576 | tf_op jit(solution)/shard_map/pallas_call | solution.py:314
  131.2 3.0 %shard_map.75.refs_0_ = bf16[384,256]{1,0:T(8,128)(2,1)S(1)} custom-call(bf16[4,384,512]{2,1,0:T(8,128)(2,1)} %shard_map.73.held, f32[8,1,512]{2,1,0:T(1,128)S(1)} %reshape.3.refs_4_.gain, bf16[8,8,48,256]{3,2,1,0:T(8,128)(2,1)S(1)} %all-to-all-done.1.mine, bf16[8,8,48,256]{3,2,1,0:T(8,128)(2,1)} %collective-permute-done.5.source.other), custom_call_target="tpu_custom_call" | custom-call | flops 536870912 | bytes 1048576 | tf_op jit(solution)/shard_map/pallas_call | solution.py:348
  134.2 3.4 %shard_map.76.refs_0_ = bf16[272,256]{1,0:T(8,128)(2,1)S(1)} custom-call(bf16[384,256]{1,0:T(8,128)(2,1)S(1)} %shard_map.75.refs_0_, f32[2,128,256]{2,1,0:T(8,128)S(1)} %copy-done.1, f32[2,256]{1,0:T(2,128)S(1)} %copy-done.2), custom_call_target="tpu_custom_call" | custom-call | flops 16777216 | bytes 1048576 | tf_op jit(solution)/shard_map/pallas_call | solution.py:314
  137.6 3.5 %collective-permute-start.6 = (bf16[272,256]{1,0:T(8,128)(2,1)S(1)}, bf16[272,256]{1,0:T(8,128)(2,1)S(1)}, u32[]{:S(2)}, u32[]{:S(2)}) collective-permute-start(bf16[272,256]{1,0:T(8,128)(2,1)S(1)} %shard_map.76.refs_0_), channel_id=1, source_target_pairs={{0,1},{1,2},{2,3},{3,0},{4,5},{5,6},{6,7},{7,4},{8,9},{9,10},{10,1... | collective-permute-start | bytes 417800 | tf_op jit(solution)/shard_map/ppermute | solution.py:74
  141.2 4.5 %collective-permute-start.7 = (bf16[272,256]{1,0:T(8,128)(2,1)S(1)}, bf16[272,256]{1,0:T(8,128)(2,1)S(1)}, u32[]{:S(2)}, u32[]{:S(2)}) collective-permute-start(bf16[272,256]{1,0:T(8,128)(2,1)S(1)} %shard_map.76.refs_0_), channel_id=1, source_target_pairs={{0,2},{1,3},{2,0},{3,1},{4,6},{5,7},{6,4},{7,5},{8,10},{9,11},{10,... | collective-permute-start | bytes 417800 | tf_op jit(solution)/shard_map/ppermute | solution.py:74
  147.6 2.5 %shard_map.77.refs_5_ = bf16[4,2,8,2,16,256]{5,4,3,2,1,0:T(8,128)(2,1)} custom-call(bf16[8,8,48,256]{3,2,1,0:T(8,128)(2,1)S(1)} %all-to-all-done.1.mine, bf16[8,8,48,256]{3,2,1,0:T(8,128)(2,1)} %collective-permute-done.5.source.other), custom_call_target="tpu_custom_call" | custom-call | flops 67108864 | bytes 1048576 | tf_op jit(solution)/shard_map/pallas_call | solution.py:314
  151.5 2.8 %shard_map.78 = bf16[4,256,512]{2,1,0:T(8,128)(2,1)} custom-call(bf16[272,256]{1,0:T(8,128)(2,1)S(1)} %shard_map.76.refs_0_, bf16[272,256]{1,0:T(8,128)(2,1)S(1)} %collective-permute-done.6.refs_1_, bf16[272,256]{1,0:T(8,128)(2,1)S(1)} %collective-permute-done.7.refs_2_, bf16[272,256]{1,0:T(8,128)(2,1)S(1)} %collective-permute-done.8.refs_3_, ...), custom_call_target="tpu_custom_call" | custom-call | flops 268435456 | bytes 1048576 | tf_op jit(solution)/shard_map/pallas_call | solution.py:464
  154.2 16.2 %all_to_all.26.held.refs_1_ = bf16[4,256,512]{2,1,0:T(8,128)(2,1)S(1)} all-to-all(bf16[4,256,512]{2,1,0:T(8,128)(2,1)} %shard_map.78), channel_id=1, replica_groups=mesh['sp'=128,'tp'=4] {'tp'}, dimensions={0} | all-to-all | bytes 2097152 | tf_op jit(solution)/shard_map/all_to_all | solution.py:83
  170.5 2.6 %shard_map.80.refs_0_.refs_1_ = bf16[256,256]{1,0:T(8,128)(2,1)S(1)} custom-call(bf16[4,256,512]{2,1,0:T(8,128)(2,1)S(1)} %all_to_all.26.held.refs_1_, f32[8,1,512]{2,1,0:T(1,128)S(1)} %reshape.3.refs_4_.gain, bf16[8,8,48,256]{3,2,1,0:T(8,128)(2,1)S(1)} %all-to-all-done.3.mine, bf16[8,8,48,256]{3,2,1,0:T(8,128)(2,1)} %collective-permute-done.9.source.other), custom_call_target="tpu_custom_call" | custom-call | flops 536870912 | bytes 1048576 | tf_op jit(solution)/shard_map/pallas_call | solution.py:348
  173.1 2.6 %collective-permute-start.10 = (bf16[128,256]{1,0:T(8,128)(2,1)S(1)}, bf16[128,256]{1,0:T(8,128)(2,1)S(1)}, u32[]{:S(2)}, u32[]{:S(2)}) collective-permute-start(bf16[128,256]{1,0:T(8,128)(2,1)S(1)} %slice.9), channel_id=1, source_target_pairs={{0,4},{4,8},{8,12},{12,16},{16,20},{20,24},{24,28},{28,32},{32,36}... | collective-permute-start | bytes 196616 | tf_op jit(solution)/shard_map/ppermute | solution.py:514
  178.5 2.8 %shard_map.82 = bf16[4,272,256]{2,1,0:T(8,128)(2,1)} custom-call(bf16[128,256]{1,0:T(8,128)(2,1)S(1)} %collective-permute-done.10.refs_0_, bf16[256,256]{1,0:T(8,128)(2,1)S(1)} %shard_map.80.refs_0_.refs_1_, f32[128,256]{1,0:T(8,128)S(1)} %shard_map.81.refs_2_, f32[2,128,256]{2,1,0:T(8,128)S(1)} %copy-done.1, f32[2,256]{1,0:T(2,128)S(1)} %copy-done.2), custom_call_target="tpu_custom_call" | custom-call | flops 8388608 | bytes 1048576 | tf_op jit(solution)/shard_map/pallas_call | solution.py:314
  181.2 3.5 %all-to-all-start.4 = ((bf16[4,272,256]{2,1,0:T(8,128)(2,1)}), bf16[4,272,256]{2,1,0:T(8,128)(2,1)S(1)}, u32[]{:S(2)}, u32[]{:S(2)}) async-start(bf16[4,272,256]{2,1,0:T(8,128)(2,1)} %shard_map.82), calls=%async_computation.4 | async-start | bytes 1114112 | tf_op jit(solution)/shard_map/all_to_all | solution.py:83
  187.2 6.6 %all-to-all-done.4.refs_0_ = bf16[4,272,256]{2,1,0:T(8,128)(2,1)S(1)} async-done(((bf16[4,272,256]{2,1,0:T(8,128)(2,1)}), bf16[4,272,256]{2,1,0:T(8,128)(2,1)S(1)}, u32[]{:S(2)}, u32[]{:S(2)}) %all-to-all-start.4) | async-done | bytes 557088 | tf_op jit(solution)/shard_map/all_to_all | solution.py:83
  193.8 2.5 %shard_map.84 = bf16[256,512]{1,0:T(8,128)(2,1)} custom-call(bf16[4,272,256]{2,1,0:T(8,128)(2,1)S(1)} %all-to-all-done.4.refs_0_, bf16[4,256,512]{2,1,0:T(8,128)(2,1)} %copy-done, bf16[4,2,8,2,16,256]{5,4,3,2,1,0:T(8,128)(2,1)} %shard_map.83.refs_2_), custom_call_target="tpu_custom_call" | custom-call | flops 268435456 | bytes 1048576 | tf_op jit(solution)/shard_map/pallas_call | solution.py:464
  (34 shorter events, 22.8 us)
Async XLA Ops:
  0.0 2.8 %collective-permute-start.1 = (bf16[2,16,256]{2,1,0:T(8,128)(2,1)}, bf16[2,16,256]{2,1,0:T(8,128)(2,1)S(1)}, u32[]{:S(2)}, u32[]{:S(2)}) collective-permute-start(bf16[2,16,256]{2,1,0:T(8,128)(2,1)} %bitcast.1), channel_id=1, source_target_pairs={{0,0},{1,128},{2,256},{3,384},{4,4},{5,20},{6,36},{7,52},{8,8},{9,... | collective-permute-start | bytes 49160 | tf_op jit(solution)/shard_map/ppermute | solution.py:70
  36.1 28.2 %all-to-all-start.1 = ((bf16[8,8,48,256]{3,2,1,0:T(8,128)(2,1)}), bf16[8,8,48,256]{3,2,1,0:T(8,128)(2,1)S(1)}, u32[]{:S(2)}, u32[]{:S(2)}) async-start(bf16[8,8,48,256]{3,2,1,0:T(8,128)(2,1)} %shard_map.74), calls=%async_computation.1 | async-start | bytes 3145728 | tf_op jit(solution)/shard_map/all_to_all | solution.py:45
  41.8 32.2 %copy-start.3 = (bf16[256,512]{1,0:T(8,128)(2,1)S(1)}, bf16[256,512]{1,0:T(8,128)(2,1)}, u32[]{:S(2)}) copy-start(bf16[256,512]{1,0:T(8,128)(2,1)} %refs_4_.2) | copy-start | bytes 786436
  64.3 27.0 %all-to-all-start.3 = ((bf16[8,8,48,256]{3,2,1,0:T(8,128)(2,1)}), bf16[8,8,48,256]{3,2,1,0:T(8,128)(2,1)S(1)}, u32[]{:S(2)}, u32[]{:S(2)}) async-start(bf16[8,8,48,256]{3,2,1,0:T(8,128)(2,1)} %shard_map.79), calls=%async_computation.3 | async-start | bytes 3145728 | tf_op jit(solution)/shard_map/all_to_all | solution.py:45
  67.9 63.3 %collective-permute-start.5 = (bf16[8,8,48,256]{3,2,1,0:T(8,128)(2,1)S(1)}, bf16[8,8,48,256]{3,2,1,0:T(8,128)(2,1)}, u32[]{:S(2)}, u32[]{:S(2)}) collective-permute-start(bf16[8,8,48,256]{3,2,1,0:T(8,128)(2,1)S(1)} %all-to-all-done.1.mine), channel_id=1, source_target_pairs={{0,4},{4,0},{8,12},{12,8},{16,20},{20,16},{24,28},{28,24},{32,36},... | collective-permute-start | bytes 4718600 | tf_op jit(solution)/shard_map/ppermute | solution.py:57
  74.0 27.3 %collective-permute-start = (bf16[256,512]{1,0:T(8,128)(2,1)S(1)}, bf16[256,512]{1,0:T(8,128)(2,1)}, u32[]{:S(2)}, u32[]{:S(2)}) collective-permute-start(bf16[256,512]{1,0:T(8,128)(2,1)S(1)} %copy-done.3), channel_id=1, source_target_pairs={{0,4},{4,8},{8,12},{12,16},{16,20},{20,24},{24,28},{28,32},{32,36}... | collective-permute-start | bytes 786440 | tf_op jit(solution)/shard_map/ppermute | solution.py:493
  91.3 79.1 %collective-permute-start.9 = (bf16[8,8,48,256]{3,2,1,0:T(8,128)(2,1)S(1)}, bf16[8,8,48,256]{3,2,1,0:T(8,128)(2,1)}, u32[]{:S(2)}, u32[]{:S(2)}) collective-permute-start(bf16[8,8,48,256]{3,2,1,0:T(8,128)(2,1)S(1)} %all-to-all-done.3.mine), channel_id=1, source_target_pairs={{0,4},{4,0},{8,12},{12,8},{16,20},{20,16},{24,28},{28,24},{32,36},... | collective-permute-start | bytes 4718600 | tf_op jit(solution)/shard_map/ppermute | solution.py:57
  103.2 22.3 %collective-permute-start.2 = (bf16[384,512]{1,0:T(8,128)(2,1)S(1)}, bf16[384,512]{1,0:T(8,128)(2,1)}, u32[]{:S(2)}, u32[]{:S(2)}) collective-permute-start(bf16[384,512]{1,0:T(8,128)(2,1)S(1)} %pad_maximum_fusion.refs_0_), channel_id=1, source_target_pairs={{0,1},{1,2},{2,3},{3,0},{4,5},{5,6},{6,7},{7,4},{8,9},{9,10},{10,1... | collective-permute-start | bytes 1179656 | tf_op jit(solution)/shard_map/ppermute | solution.py:74
  106.4 19.1 %collective-permute-start.3 = (bf16[384,512]{1,0:T(8,128)(2,1)S(1)}, bf16[384,512]{1,0:T(8,128)(2,1)}, u32[]{:S(2)}, u32[]{:S(2)}) collective-permute-start(bf16[384,512]{1,0:T(8,128)(2,1)S(1)} %pad_maximum_fusion.refs_0_), channel_id=1, source_target_pairs={{0,2},{1,3},{2,0},{3,1},{4,6},{5,7},{6,4},{7,5},{8,10},{9,11},{10,... | collective-permute-start | bytes 1179656 | tf_op jit(solution)/shard_map/ppermute | solution.py:74
  108.3 19.4 %collective-permute-start.4 = (bf16[384,512]{1,0:T(8,128)(2,1)S(1)}, bf16[384,512]{1,0:T(8,128)(2,1)}, u32[]{:S(2)}, u32[]{:S(2)}) collective-permute-start(bf16[384,512]{1,0:T(8,128)(2,1)S(1)} %pad_maximum_fusion.refs_0_), channel_id=1, source_target_pairs={{0,3},{1,0},{2,1},{3,2},{4,7},{5,4},{6,5},{7,6},{8,11},{9,8},{10,9... | collective-permute-start | bytes 1179656 | tf_op jit(solution)/shard_map/ppermute | solution.py:74
  131.2 3.1 %copy-start.1 = (f32[2,128,256]{2,1,0:T(8,128)S(1)}, f32[2,128,256]{2,1,0:T(8,128)}, u32[]{:S(2)}) copy-start(f32[2,128,256]{2,1,0:T(8,128)} %refs_3_.1) | copy-start | bytes 786436
  131.2 3.0 %copy-start.2 = (f32[2,256]{1,0:T(2,128)S(1)}, f32[2,256]{1,0:T(2,128)}, u32[]{:S(2)}) copy-start(f32[2,256]{1,0:T(2,128)} %refs_4_.3) | copy-start | bytes 6148
  137.6 12.5 %collective-permute-start.6 = (bf16[272,256]{1,0:T(8,128)(2,1)S(1)}, bf16[272,256]{1,0:T(8,128)(2,1)S(1)}, u32[]{:S(2)}, u32[]{:S(2)}) collective-permute-start(bf16[272,256]{1,0:T(8,128)(2,1)S(1)} %shard_map.76.refs_0_), channel_id=1, source_target_pairs={{0,1},{1,2},{2,3},{3,0},{4,5},{5,6},{6,7},{7,4},{8,9},{9,10},{10,1... | collective-permute-start | bytes 417800 | tf_op jit(solution)/shard_map/ppermute | solution.py:74
  141.2 9.1 %collective-permute-start.7 = (bf16[272,256]{1,0:T(8,128)(2,1)S(1)}, bf16[272,256]{1,0:T(8,128)(2,1)S(1)}, u32[]{:S(2)}, u32[]{:S(2)}) collective-permute-start(bf16[272,256]{1,0:T(8,128)(2,1)S(1)} %shard_map.76.refs_0_), channel_id=1, source_target_pairs={{0,2},{1,3},{2,0},{3,1},{4,6},{5,7},{6,4},{7,5},{8,10},{9,11},{10,... | collective-permute-start | bytes 417800 | tf_op jit(solution)/shard_map/ppermute | solution.py:74
  145.7 5.8 %collective-permute-start.8 = (bf16[272,256]{1,0:T(8,128)(2,1)S(1)}, bf16[272,256]{1,0:T(8,128)(2,1)S(1)}, u32[]{:S(2)}, u32[]{:S(2)}) collective-permute-start(bf16[272,256]{1,0:T(8,128)(2,1)S(1)} %shard_map.76.refs_0_), channel_id=1, source_target_pairs={{0,3},{1,0},{2,1},{3,2},{4,7},{5,4},{6,5},{7,6},{8,11},{9,8},{10,9... | collective-permute-start | bytes 417800 | tf_op jit(solution)/shard_map/ppermute | solution.py:74
  170.5 2.6 %copy-start = (bf16[4,256,512]{2,1,0:T(8,128)(2,1)}, bf16[4,256,512]{2,1,0:T(8,128)(2,1)S(1)}, u32[]{:S(2)}) copy-start(bf16[4,256,512]{2,1,0:T(8,128)(2,1)S(1)} %all_to_all.26.held.refs_1_) | copy-start | bytes 3145732
  173.1 5.4 %collective-permute-start.10 = (bf16[128,256]{1,0:T(8,128)(2,1)S(1)}, bf16[128,256]{1,0:T(8,128)(2,1)S(1)}, u32[]{:S(2)}, u32[]{:S(2)}) collective-permute-start(bf16[128,256]{1,0:T(8,128)(2,1)S(1)} %slice.9), channel_id=1, source_target_pairs={{0,4},{4,8},{8,12},{12,16},{16,20},{20,24},{24,28},{28,32},{32,36}... | collective-permute-start | bytes 196616 | tf_op jit(solution)/shard_map/ppermute | solution.py:514
  181.2 12.5 %all-to-all-start.4 = ((bf16[4,272,256]{2,1,0:T(8,128)(2,1)}), bf16[4,272,256]{2,1,0:T(8,128)(2,1)S(1)}, u32[]{:S(2)}, u32[]{:S(2)}) async-start(bf16[4,272,256]{2,1,0:T(8,128)(2,1)} %shard_map.82), calls=%async_computation.4 | async-start | bytes 1114112 | tf_op jit(solution)/shard_map/all_to_all | solution.py:83

commit v8 on v7

--- a/solution.py
+++ b/solution.py
@@ -65,8 +65,7 @@
         for y in range(NY):
             for c in range(2):
                 for x in range(NX):
-                    place = (x * nb + b, y) if c == 0 else (y, x * nb + b)
-                    pairs.append((at(z, y, c) * NX + x, at(*place, c) * NX + a))
+                    pairs.append((at(z, y, c) * NX + x, at(x * nb + b, y, c) * NX + a))
     return lax.ppermute(v, ("sp", "x"), pairs)
 
 
@@ -360,18 +359,19 @@
 
 
 def arrange_kernel(mine, other, out, wt, sem):
-    def fill(halves):
-        for k in range(NX):
-            for c, w in enumerate(halves):
-                wt[k, :, :, c] = w[2 * k : 2 * k + 2, :, 32:, :]
+    def fill(zy, yz):
+        for z in range(NZ):
+            k, i = divmod(z, NZ // NX)
+            wt[k, i, :, 0] = zy[z, :, 32:, :]
+            wt[k, i, :, 1] = yz[:, z, 32:, :]
 
     @pl.when(core_here() == 0)
     def _():
-        fill((mine, other))
+        fill(mine, other)
 
     @pl.when(core_here() == 1)
     def _():
-        fill((other, mine))
+        fill(other, mine)
 
     done = pltpu.make_async_copy(wt, out, sem)
     done.start()

time: 197 us -> 197 us (level)
  starting transfers between devices: 53 us -> 55.6 us
  blocking collectives: 48.3 us -> 45.8 us
    all_to_all x1, blocking collectives: 32.1 us -> 29.6 us  [to_group(): lax.all_to_all(copies, 'sp', split_axis=0, concat_axis=0, tiled=True, axi...]
    all_to_all x2, starting transfers between devices: 8.03 us -> 10.4 us  [plane(): lax.all_to_all(copies, 'sp', split_axis=0, concat_axis=0, tiled=True, axi...]
where the time goes in v8:
time: 197 us; the launch traced here: 196 us
  waiting for transfers between devices  61.1 us (31%)
  starting transfers between devices  55.6 us (28%)
  blocking collectives  45.8 us (23%)
  Pallas kernels  29.4 us (15%)
  local copies, waits for them, and re-layouts  3.16 us (2%)
    all_to_all x2, waiting for transfers between devices, plane(): lax.all_to_all(copies, 'sp', split_axis=0, concat_axis=0, tiled=True, axi...  37.5 us
    all_to_all x1, blocking collectives, to_group(): lax.all_to_all(copies, 'sp', split_axis=0, concat_axis=0, tiled=True, axi...  29.6 us
    ppermute x6, starting transfers between devices, along_x(): return lax.ppermute(v, 'x', [(i, (i + step) % NX) for i in range(NX)])  19.3 us
    pallas_call x8, Pallas kernels, call(): pl.pallas_call(body, out_shape=out, in_specs=[pl.BlockSpec(memory_space=p...  18.5 us
    ppermute x2, starting transfers between devices, swap_cores(): return lax.ppermute(v, 'sp', [(i, i ^ 1) for i in range(count)])  16.3 us
    all_to_all x1, blocking collectives, exchange_x(): lax.all_to_all(copies, 'x', split_axis=0, concat_axis=0, tiled=True)  16.2 us
    ppermute x6, waiting for transfers between devices, along_x(): return lax.ppermute(v, 'x', [(i, (i + step) % NX) for i in range(NX)])  15.8 us
    all_to_all x2, starting transfers between devices, plane(): lax.all_to_all(copies, 'sp', split_axis=0, concat_axis=0, tiled=True, axi...  10.4 us
  transfers between devices with their start and end apart: 14, of which 8 were waited for; matrix products, arithmetic and copies ran while one was open for 2% of the time, Pallas kernels for 10%

profile of v8, /device:TPU:1, one launch (start us, length us, event | category | flops | bytes accessed | tf_op | source)
XLA Modules:
  0.0 196.2 jit_solution(5737463639915254738)
XLA Ops:
  2.8 29.6 %all_to_all.25.refs_0_ = bf16[8,2,48,256]{3,2,1,0:T(8,128)(2,1)S(1)} all-to-all(bf16[8,2,48,256]{3,2,1,0:T(8,128)(2,1)S(1)} %broadcast_in_dim.3), channel_id=1, replica_groups={{0,8,16,24,32,40,48,56},{64,72,80,88,96,104,112,120},{128,136,144,152,1..., dimensions={0} | all-to-all | bytes 786432 | tf_op jit(solution)/shard_map/all_to_all | solution.py:35
  33.6 6.8 %all-to-all-start.1 = ((bf16[8,8,48,256]{3,2,1,0:T(8,128)(2,1)}), bf16[8,8,48,256]{3,2,1,0:T(8,128)(2,1)S(1)}, u32[]{:S(2)}, u32[]{:S(2)}) async-start(bf16[8,8,48,256]{3,2,1,0:T(8,128)(2,1)} %shard_map.74), calls=%async_computation.1 | async-start | bytes 3145728 | tf_op jit(solution)/shard_map/all_to_all | solution.py:45
  41.7 22.5 %all-to-all-done.1.mine = bf16[8,8,48,256]{3,2,1,0:T(8,128)(2,1)S(1)} async-done(((bf16[8,8,48,256]{3,2,1,0:T(8,128)(2,1)}), bf16[8,8,48,256]{3,2,1,0:T(8,128)(2,1)S(1)}, u32[]{:S(2)}, u32[]{:S(2)}) %all-to-all-start.1) | async-done | bytes 1572896 | tf_op jit(solution)/shard_map/all_to_all | solution.py:45
  64.2 3.6 %all-to-all-start.3 = ((bf16[8,8,48,256]{3,2,1,0:T(8,128)(2,1)}), bf16[8,8,48,256]{3,2,1,0:T(8,128)(2,1)S(1)}, u32[]{:S(2)}, u32[]{:S(2)}) async-start(bf16[8,8,48,256]{3,2,1,0:T(8,128)(2,1)} %shard_map.79), calls=%async_computation.3 | async-start | bytes 3145728 | tf_op jit(solution)/shard_map/all_to_all | solution.py:45
  67.8 6.3 %collective-permute-start.5 = (bf16[8,8,48,256]{3,2,1,0:T(8,128)(2,1)S(1)}, bf16[8,8,48,256]{3,2,1,0:T(8,128)(2,1)}, u32[]{:S(2)}, u32[]{:S(2)}) collective-permute-start(bf16[8,8,48,256]{3,2,1,0:T(8,128)(2,1)S(1)} %all-to-all-done.1.mine), channel_id=1, source_target_pairs={{0,4},{4,0},{8,12},{12,8},{16,20},{20,16},{24,28},{28,24},{32,36},... | collective-permute-start | bytes 4718600 | tf_op jit(solution)/shard_map/ppermute | solution.py:57
  76.1 15.1 %all-to-all-done.3.mine = bf16[8,8,48,256]{3,2,1,0:T(8,128)(2,1)S(1)} async-done(((bf16[8,8,48,256]{3,2,1,0:T(8,128)(2,1)}), bf16[8,8,48,256]{3,2,1,0:T(8,128)(2,1)S(1)}, u32[]{:S(2)}, u32[]{:S(2)}) %all-to-all-start.3) | async-done | bytes 1572896 | tf_op jit(solution)/shard_map/all_to_all | solution.py:45
  91.2 10.1 %collective-permute-start.9 = (bf16[8,8,48,256]{3,2,1,0:T(8,128)(2,1)S(1)}, bf16[8,8,48,256]{3,2,1,0:T(8,128)(2,1)}, u32[]{:S(2)}, u32[]{:S(2)}) collective-permute-start(bf16[8,8,48,256]{3,2,1,0:T(8,128)(2,1)S(1)} %all-to-all-done.3.mine), channel_id=1, source_target_pairs={{0,4},{4,0},{8,12},{12,8},{16,20},{20,16},{24,28},{28,24},{32,36},... | collective-permute-start | bytes 4718600 | tf_op jit(solution)/shard_map/ppermute | solution.py:57
  103.2 3.1 %collective-permute-start.2 = (bf16[384,512]{1,0:T(8,128)(2,1)S(1)}, bf16[384,512]{1,0:T(8,128)(2,1)}, u32[]{:S(2)}, u32[]{:S(2)}) collective-permute-start(bf16[384,512]{1,0:T(8,128)(2,1)S(1)} %pad_maximum_fusion.refs_0_), channel_id=1, source_target_pairs={{0,1},{1,2},{2,3},{3,0},{4,5},{5,6},{6,7},{7,4},{8,9},{9,10},{10,1... | collective-permute-start | bytes 1179656 | tf_op jit(solution)/shard_map/ppermute | solution.py:73
  108.3 4.3 %collective-permute-start.4 = (bf16[384,512]{1,0:T(8,128)(2,1)S(1)}, bf16[384,512]{1,0:T(8,128)(2,1)}, u32[]{:S(2)}, u32[]{:S(2)}) collective-permute-start(bf16[384,512]{1,0:T(8,128)(2,1)S(1)} %pad_maximum_fusion.refs_0_), channel_id=1, source_target_pairs={{0,3},{1,0},{2,1},{3,2},{4,7},{5,4},{6,5},{7,6},{8,11},{9,8},{10,9... | collective-permute-start | bytes 1179656 | tf_op jit(solution)/shard_map/ppermute | solution.py:73
  113.3 12.2 %collective-permute-done.2.refs_1_ = bf16[384,512]{1,0:T(8,128)(2,1)} collective-permute-done((bf16[384,512]{1,0:T(8,128)(2,1)S(1)}, bf16[384,512]{1,0:T(8,128)(2,1)}, u32[]{:S(2)}, u32[]{:S(2)}) %collective-permute-start.2) | collective-permute-done | bytes 393248 | tf_op jit(solution)/shard_map/ppermute | solution.py:73
  127.8 3.4 %shard_map.73.held = bf16[4,384,512]{2,1,0:T(8,128)(2,1)} custom-call(bf16[384,512]{1,0:T(8,128)(2,1)S(1)} %pad_maximum_fusion.refs_0_, bf16[384,512]{1,0:T(8,128)(2,1)} %collective-permute-done.2.refs_1_, bf16[384,512]{1,0:T(8,128)(2,1)} %collective-permute-done.3.refs_2_, bf16[384,512]{1,0:T(8,128)(2,1)} %collective-permute-done.4.refs_3_, ...), custom_call_target="tpu_custom_call" | custom-call | flops 4194304 | bytes 1048576 | tf_op jit(solution)/shard_map/pallas_call | solution.py:313
  131.2 3.0 %shard_map.75.refs_0_ = bf16[384,256]{1,0:T(8,128)(2,1)S(1)} custom-call(bf16[4,384,512]{2,1,0:T(8,128)(2,1)} %shard_map.73.held, f32[8,1,512]{2,1,0:T(1,128)S(1)} %reshape.3.refs_4_.gain, bf16[8,8,48,256]{3,2,1,0:T(8,128)(2,1)S(1)} %all-to-all-done.1.mine, bf16[8,8,48,256]{3,2,1,0:T(8,128)(2,1)} %collective-permute-done.5.source.other), custom_call_target="tpu_custom_call" | custom-call | flops 536870912 | bytes 1048576 | tf_op jit(solution)/shard_map/pallas_call | solution.py:347
  134.2 3.4 %shard_map.76.refs_0_ = bf16[272,256]{1,0:T(8,128)(2,1)S(1)} custom-call(bf16[384,256]{1,0:T(8,128)(2,1)S(1)} %shard_map.75.refs_0_, f32[2,128,256]{2,1,0:T(8,128)S(1)} %copy-done.1, f32[2,256]{1,0:T(2,128)S(1)} %copy-done.2), custom_call_target="tpu_custom_call" | custom-call | flops 16777216 | bytes 1048576 | tf_op jit(solution)/shard_map/pallas_call | solution.py:313
  137.6 3.5 %collective-permute-start.6 = (bf16[272,256]{1,0:T(8,128)(2,1)S(1)}, bf16[272,256]{1,0:T(8,128)(2,1)S(1)}, u32[]{:S(2)}, u32[]{:S(2)}) collective-permute-start(bf16[272,256]{1,0:T(8,128)(2,1)S(1)} %shard_map.76.refs_0_), channel_id=1, source_target_pairs={{0,1},{1,2},{2,3},{3,0},{4,5},{5,6},{6,7},{7,4},{8,9},{9,10},{10,1... | collective-permute-start | bytes 417800 | tf_op jit(solution)/shard_map/ppermute | solution.py:73
  141.1 4.6 %collective-permute-start.7 = (bf16[272,256]{1,0:T(8,128)(2,1)S(1)}, bf16[272,256]{1,0:T(8,128)(2,1)S(1)}, u32[]{:S(2)}, u32[]{:S(2)}) collective-permute-start(bf16[272,256]{1,0:T(8,128)(2,1)S(1)} %shard_map.76.refs_0_), channel_id=1, source_target_pairs={{0,2},{1,3},{2,0},{3,1},{4,6},{5,7},{6,4},{7,5},{8,10},{9,11},{10,... | collective-permute-start | bytes 417800 | tf_op jit(solution)/shard_map/ppermute | solution.py:73
  147.6 2.5 %shard_map.77.refs_5_ = bf16[4,2,8,2,16,256]{5,4,3,2,1,0:T(8,128)(2,1)} custom-call(bf16[8,8,48,256]{3,2,1,0:T(8,128)(2,1)S(1)} %all-to-all-done.1.mine, bf16[8,8,48,256]{3,2,1,0:T(8,128)(2,1)} %collective-permute-done.5.source.other), custom_call_target="tpu_custom_call" | custom-call | flops 67108864 | bytes 1048576 | tf_op jit(solution)/shard_map/pallas_call | solution.py:313
  151.5 2.8 %shard_map.78 = bf16[4,256,512]{2,1,0:T(8,128)(2,1)} custom-call(bf16[272,256]{1,0:T(8,128)(2,1)S(1)} %shard_map.76.refs_0_, bf16[272,256]{1,0:T(8,128)(2,1)S(1)} %collective-permute-done.6.refs_1_, bf16[272,256]{1,0:T(8,128)(2,1)S(1)} %collective-permute-done.7.refs_2_, bf16[272,256]{1,0:T(8,128)(2,1)S(1)} %collective-permute-done.8.refs_3_, ...), custom_call_target="tpu_custom_call" | custom-call | flops 268435456 | bytes 1048576 | tf_op jit(solution)/shard_map/pallas_call | solution.py:464
  154.2 16.2 %all_to_all.26.held.refs_1_ = bf16[4,256,512]{2,1,0:T(8,128)(2,1)S(1)} all-to-all(bf16[4,256,512]{2,1,0:T(8,128)(2,1)} %shard_map.78), channel_id=1, replica_groups=mesh['sp'=128,'tp'=4] {'tp'}, dimensions={0} | all-to-all | bytes 2097152 | tf_op jit(solution)/shard_map/all_to_all | solution.py:82
  170.5 2.6 %shard_map.80.refs_0_.refs_1_ = bf16[256,256]{1,0:T(8,128)(2,1)S(1)} custom-call(bf16[4,256,512]{2,1,0:T(8,128)(2,1)S(1)} %all_to_all.26.held.refs_1_, f32[8,1,512]{2,1,0:T(1,128)S(1)} %reshape.3.refs_4_.gain, bf16[8,8,48,256]{3,2,1,0:T(8,128)(2,1)S(1)} %all-to-all-done.3.mine, bf16[8,8,48,256]{3,2,1,0:T(8,128)(2,1)} %collective-permute-done.9.source.other), custom_call_target="tpu_custom_call" | custom-call | flops 536870912 | bytes 1048576 | tf_op jit(solution)/shard_map/pallas_call | solution.py:347
  173.1 2.6 %collective-permute-start.10 = (bf16[128,256]{1,0:T(8,128)(2,1)S(1)}, bf16[128,256]{1,0:T(8,128)(2,1)S(1)}, u32[]{:S(2)}, u32[]{:S(2)}) collective-permute-start(bf16[128,256]{1,0:T(8,128)(2,1)S(1)} %slice.9), channel_id=1, source_target_pairs={{0,4},{4,8},{8,12},{12,16},{16,20},{20,24},{24,28},{28,32},{32,36}... | collective-permute-start | bytes 196616 | tf_op jit(solution)/shard_map/ppermute | solution.py:514
  178.5 2.8 %shard_map.82 = bf16[4,272,256]{2,1,0:T(8,128)(2,1)} custom-call(bf16[128,256]{1,0:T(8,128)(2,1)S(1)} %collective-permute-done.10.refs_0_, bf16[256,256]{1,0:T(8,128)(2,1)S(1)} %shard_map.80.refs_0_.refs_1_, f32[128,256]{1,0:T(8,128)S(1)} %shard_map.81.refs_2_, f32[2,128,256]{2,1,0:T(8,128)S(1)} %copy-done.1, f32[2,256]{1,0:T(2,128)S(1)} %copy-done.2), custom_call_target="tpu_custom_call" | custom-call | flops 8388608 | bytes 1048576 | tf_op jit(solution)/shard_map/pallas_call | solution.py:313
  181.2 3.5 %all-to-all-start.4 = ((bf16[4,272,256]{2,1,0:T(8,128)(2,1)}), bf16[4,272,256]{2,1,0:T(8,128)(2,1)S(1)}, u32[]{:S(2)}, u32[]{:S(2)}) async-start(bf16[4,272,256]{2,1,0:T(8,128)(2,1)} %shard_map.82), calls=%async_computation.4 | async-start | bytes 1114112 | tf_op jit(solution)/shard_map/all_to_all | solution.py:82
  187.2 6.6 %all-to-all-done.4.refs_0_ = bf16[4,272,256]{2,1,0:T(8,128)(2,1)S(1)} async-done(((bf16[4,272,256]{2,1,0:T(8,128)(2,1)}), bf16[4,272,256]{2,1,0:T(8,128)(2,1)S(1)}, u32[]{:S(2)}, u32[]{:S(2)}) %all-to-all-start.4) | async-done | bytes 557088 | tf_op jit(solution)/shard_map/all_to_all | solution.py:82
  193.8 2.5 %shard_map.84 = bf16[256,512]{1,0:T(8,128)(2,1)} custom-call(bf16[4,272,256]{2,1,0:T(8,128)(2,1)S(1)} %all-to-all-done.4.refs_0_, bf16[4,256,512]{2,1,0:T(8,128)(2,1)} %copy-done, bf16[4,2,8,2,16,256]{5,4,3,2,1,0:T(8,128)(2,1)} %shard_map.83.refs_2_), custom_call_target="tpu_custom_call" | custom-call | flops 268435456 | bytes 1048576 | tf_op jit(solution)/shard_map/pallas_call | solution.py:464
  (34 shorter events, 22.8 us)
Async XLA Ops:
  0.0 2.8 %collective-permute-start.1 = (bf16[2,16,256]{2,1,0:T(8,128)(2,1)}, bf16[2,16,256]{2,1,0:T(8,128)(2,1)S(1)}, u32[]{:S(2)}, u32[]{:S(2)}) collective-permute-start(bf16[2,16,256]{2,1,0:T(8,128)(2,1)} %bitcast.1), channel_id=1, source_target_pairs={{0,0},{1,128},{2,256},{3,384},{4,4},{5,132},{6,260},{7,388},{8,8},... | collective-permute-start | bytes 49160 | tf_op jit(solution)/shard_map/ppermute | solution.py:69
  33.6 30.6 %all-to-all-start.1 = ((bf16[8,8,48,256]{3,2,1,0:T(8,128)(2,1)}), bf16[8,8,48,256]{3,2,1,0:T(8,128)(2,1)S(1)}, u32[]{:S(2)}, u32[]{:S(2)}) async-start(bf16[8,8,48,256]{3,2,1,0:T(8,128)(2,1)} %shard_map.74), calls=%async_computation.1 | async-start | bytes 3145728 | tf_op jit(solution)/shard_map/all_to_all | solution.py:45
  41.7 32.3 %copy-start.3 = (bf16[256,512]{1,0:T(8,128)(2,1)S(1)}, bf16[256,512]{1,0:T(8,128)(2,1)}, u32[]{:S(2)}) copy-start(bf16[256,512]{1,0:T(8,128)(2,1)} %refs_4_.2) | copy-start | bytes 786436
  64.2 27.0 %all-to-all-start.3 = ((bf16[8,8,48,256]{3,2,1,0:T(8,128)(2,1)}), bf16[8,8,48,256]{3,2,1,0:T(8,128)(2,1)S(1)}, u32[]{:S(2)}, u32[]{:S(2)}) async-start(bf16[8,8,48,256]{3,2,1,0:T(8,128)(2,1)} %shard_map.79), calls=%async_computation.3 | async-start | bytes 3145728 | tf_op jit(solution)/shard_map/all_to_all | solution.py:45
  67.8 63.4 %collective-permute-start.5 = (bf16[8,8,48,256]{3,2,1,0:T(8,128)(2,1)S(1)}, bf16[8,8,48,256]{3,2,1,0:T(8,128)(2,1)}, u32[]{:S(2)}, u32[]{:S(2)}) collective-permute-start(bf16[8,8,48,256]{3,2,1,0:T(8,128)(2,1)S(1)} %all-to-all-done.1.mine), channel_id=1, source_target_pairs={{0,4},{4,0},{8,12},{12,8},{16,20},{20,16},{24,28},{28,24},{32,36},... | collective-permute-start | bytes 4718600 | tf_op jit(solution)/shard_map/ppermute | solution.py:57
  74.0 27.3 %collective-permute-start = (bf16[256,512]{1,0:T(8,128)(2,1)S(1)}, bf16[256,512]{1,0:T(8,128)(2,1)}, u32[]{:S(2)}, u32[]{:S(2)}) collective-permute-start(bf16[256,512]{1,0:T(8,128)(2,1)S(1)} %copy-done.3), channel_id=1, source_target_pairs={{0,4},{4,8},{8,12},{12,16},{16,20},{20,24},{24,28},{28,32},{32,36}... | collective-permute-start | bytes 786440 | tf_op jit(solution)/shard_map/ppermute | solution.py:493
  91.2 79.3 %collective-permute-start.9 = (bf16[8,8,48,256]{3,2,1,0:T(8,128)(2,1)S(1)}, bf16[8,8,48,256]{3,2,1,0:T(8,128)(2,1)}, u32[]{:S(2)}, u32[]{:S(2)}) collective-permute-start(bf16[8,8,48,256]{3,2,1,0:T(8,128)(2,1)S(1)} %all-to-all-done.3.mine), channel_id=1, source_target_pairs={{0,4},{4,0},{8,12},{12,8},{16,20},{20,16},{24,28},{28,24},{32,36},... | collective-permute-start | bytes 4718600 | tf_op jit(solution)/shard_map/ppermute | solution.py:57
  103.2 22.3 %collective-permute-start.2 = (bf16[384,512]{1,0:T(8,128)(2,1)S(1)}, bf16[384,512]{1,0:T(8,128)(2,1)}, u32[]{:S(2)}, u32[]{:S(2)}) collective-permute-start(bf16[384,512]{1,0:T(8,128)(2,1)S(1)} %pad_maximum_fusion.refs_0_), channel_id=1, source_target_pairs={{0,1},{1,2},{2,3},{3,0},{4,5},{5,6},{6,7},{7,4},{8,9},{9,10},{10,1... | collective-permute-start | bytes 1179656 | tf_op jit(solution)/shard_map/ppermute | solution.py:73
  106.4 19.1 %collective-permute-start.3 = (bf16[384,512]{1,0:T(8,128)(2,1)S(1)}, bf16[384,512]{1,0:T(8,128)(2,1)}, u32[]{:S(2)}, u32[]{:S(2)}) collective-permute-start(bf16[384,512]{1,0:T(8,128)(2,1)S(1)} %pad_maximum_fusion.refs_0_), channel_id=1, source_target_pairs={{0,2},{1,3},{2,0},{3,1},{4,6},{5,7},{6,4},{7,5},{8,10},{9,11},{10,... | collective-permute-start | bytes 1179656 | tf_op jit(solution)/shard_map/ppermute | solution.py:73
  108.3 19.5 %collective-permute-start.4 = (bf16[384,512]{1,0:T(8,128)(2,1)S(1)}, bf16[384,512]{1,0:T(8,128)(2,1)}, u32[]{:S(2)}, u32[]{:S(2)}) collective-permute-start(bf16[384,512]{1,0:T(8,128)(2,1)S(1)} %pad_maximum_fusion.refs_0_), channel_id=1, source_target_pairs={{0,3},{1,0},{2,1},{3,2},{4,7},{5,4},{6,5},{7,6},{8,11},{9,8},{10,9... | collective-permute-start | bytes 1179656 | tf_op jit(solution)/shard_map/ppermute | solution.py:73
  131.2 3.1 %copy-start.1 = (f32[2,128,256]{2,1,0:T(8,128)S(1)}, f32[2,128,256]{2,1,0:T(8,128)}, u32[]{:S(2)}) copy-start(f32[2,128,256]{2,1,0:T(8,128)} %refs_3_.1) | copy-start | bytes 786436
  131.2 3.0 %copy-start.2 = (f32[2,256]{1,0:T(2,128)S(1)}, f32[2,256]{1,0:T(2,128)}, u32[]{:S(2)}) copy-start(f32[2,256]{1,0:T(2,128)} %refs_4_.3) | copy-start | bytes 6148
  137.6 12.5 %collective-permute-start.6 = (bf16[272,256]{1,0:T(8,128)(2,1)S(1)}, bf16[272,256]{1,0:T(8,128)(2,1)S(1)}, u32[]{:S(2)}, u32[]{:S(2)}) collective-permute-start(bf16[272,256]{1,0:T(8,128)(2,1)S(1)} %shard_map.76.refs_0_), channel_id=1, source_target_pairs={{0,1},{1,2},{2,3},{3,0},{4,5},{5,6},{6,7},{7,4},{8,9},{9,10},{10,1... | collective-permute-start | bytes 417800 | tf_op jit(solution)/shard_map/ppermute | solution.py:73
  141.1 9.1 %collective-permute-start.7 = (bf16[272,256]{1,0:T(8,128)(2,1)S(1)}, bf16[272,256]{1,0:T(8,128)(2,1)S(1)}, u32[]{:S(2)}, u32[]{:S(2)}) collective-permute-start(bf16[272,256]{1,0:T(8,128)(2,1)S(1)} %shard_map.76.refs_0_), channel_id=1, source_target_pairs={{0,2},{1,3},{2,0},{3,1},{4,6},{5,7},{6,4},{7,5},{8,10},{9,11},{10,... | collective-permute-start | bytes 417800 | tf_op jit(solution)/shard_map/ppermute | solution.py:73
  145.7 5.8 %collective-permute-start.8 = (bf16[272,256]{1,0:T(8,128)(2,1)S(1)}, bf16[272,256]{1,0:T(8,128)(2,1)S(1)}, u32[]{:S(2)}, u32[]{:S(2)}) collective-permute-start(bf16[272,256]{1,0:T(8,128)(2,1)S(1)} %shard_map.76.refs_0_), channel_id=1, source_target_pairs={{0,3},{1,0},{2,1},{3,2},{4,7},{5,4},{6,5},{7,6},{8,11},{9,8},{10,9... | collective-permute-start | bytes 417800 | tf_op jit(solution)/shard_map/ppermute | solution.py:73
  170.5 2.6 %copy-start = (bf16[4,256,512]{2,1,0:T(8,128)(2,1)}, bf16[4,256,512]{2,1,0:T(8,128)(2,1)S(1)}, u32[]{:S(2)}) copy-start(bf16[4,256,512]{2,1,0:T(8,128)(2,1)S(1)} %all_to_all.26.held.refs_1_) | copy-start | bytes 3145732
  173.1 5.4 %collective-permute-start.10 = (bf16[128,256]{1,0:T(8,128)(2,1)S(1)}, bf16[128,256]{1,0:T(8,128)(2,1)S(1)}, u32[]{:S(2)}, u32[]{:S(2)}) collective-permute-start(bf16[128,256]{1,0:T(8,128)(2,1)S(1)} %slice.9), channel_id=1, source_target_pairs={{0,4},{4,8},{8,12},{12,16},{16,20},{20,24},{24,28},{28,32},{32,36}... | collective-permute-start | bytes 196616 | tf_op jit(solution)/shard_map/ppermute | solution.py:514
  181.2 12.5 %all-to-all-start.4 = ((bf16[4,272,256]{2,1,0:T(8,128)(2,1)}), bf16[4,272,256]{2,1,0:T(8,128)(2,1)S(1)}, u32[]{:S(2)}, u32[]{:S(2)}) async-start(bf16[4,272,256]{2,1,0:T(8,128)(2,1)} %shard_map.82), calls=%async_computation.4 | async-start | bytes 1114112 | tf_op jit(solution)/shard_map/all_to_all | solution.py:82

commit v9 on v8

--- a/solution.py
+++ b/solution.py
@@ -129,14 +129,19 @@
         done.wait()
 
 
-def mix_kernel(held, gain, mine, source, glu, vs, gs, other, sems, xs, *spare):
-    copies = [pltpu.make_async_copy(source, other, sems.at[0])]
-    if not spare:
-        copies.append(pltpu.make_async_copy(held, xs, sems.at[1]))
+def mix_kernel(n, *refs):
+    parts, rest = refs[:n], refs[n:]
+    gain, mine, other, glu, vs, gs, xs, *spare = rest
+    copies = []
+    if len(spare) == 2:
+        far, sems = spare
+        copies.append(pltpu.make_async_copy(other, far, sems.at[0]))
+        copies.append(pltpu.make_async_copy(parts[0], xs, sems.at[1]))
+        other = far
     for one in copies:
         one.start()
-    if spare:
-        norm_kernel(1, 1, held, gain, xs, spare[0])
+    if not copies:
+        norm_kernel(1, n, *parts, gain, xs, spare[0])
 
     def from_even(w):
         for z in range(NZ):
@@ -337,16 +342,22 @@
     )
 
 
-def mix(xs, gain, mine, other, far):
+def mix(parts, gain, mine, other, far):
+    def body(*refs):
+        mix_kernel(len(parts), *refs)
+
+    rows = parts[0].shape[-2]
     weights = pltpu.VMEM((NZ, NY, 2, 16, CH), BF)
-    scratch = [weights, weights, pltpu.VMEM(other.shape, BF), pltpu.SemaphoreType.DMA((2,))]
-    scratch.append(pltpu.VMEM(xs.shape, BF))
-    if not far:
+    scratch = [weights, weights, pltpu.VMEM((NX, rows, FEAT), BF)]
+    if far:
+        scratch += [pltpu.VMEM(other.shape, BF), pltpu.SemaphoreType.DMA((2,))]
+    else:
         scratch.append(pltpu.VMEM((TOK, 128), F32))
-    spots = [pltpu.HBM if far else pltpu.VMEM, pltpu.VMEM, pltpu.VMEM, pltpu.HBM]
+    place = pltpu.HBM if far else pltpu.VMEM
+    spots = [place] * len(parts) + [pltpu.VMEM, pltpu.VMEM, place]
     return pl.pallas_call(
-        mix_kernel,
-        out_shape=jax.ShapeDtypeStruct((xs.shape[1], CH), BF),
+        body,
+        out_shape=jax.ShapeDtypeStruct((rows, CH), BF),
         in_specs=[pl.BlockSpec(memory_space=spot) for spot in spots],
         out_specs=pl.BlockSpec(memory_space=pltpu.VMEM),
         scratch_shapes=scratch,
@@ -355,7 +366,7 @@
         ),
         compiler_params=pltpu.CompilerParams(vmem_limit_bytes=14 << 20),
         interpret=INTERPRET,
-    )(in_hbm(xs) if far else xs, gain, mine, in_hbm(other))
+    )(*([in_hbm(v) for v in parts] if far else parts), gain, mine, in_hbm(other) if far else other)
 
 
 def arrange_kernel(mine, other, out, wt, sem):
@@ -502,21 +513,21 @@
     normed = normalise(0, parts, gain)
     other = swap_cores(gathered)
     following = plane(after(ready, gathered))
-    glu = mix(normed, gain, gathered, other, True)
+    glu = mix([normed], gain, gathered, other, True)
     packed = conv_whole(0, glu, conv_taps, channel_gain)
     parts = from_all_x(packed)
     wt = arrange(after(gathered, packed), other)
-    copies = project(parts, x, wt, True)
-
-    xs = exchange_x(copies)
+    x = project(parts, x, wt, False)
+
+    xs = from_all_x(x)
     other = swap_cores(following)
-    glu = mix(xs[0], gain, following, other, False)
+    glu = mix(xs, gain, following, other, False)
     before = lax.ppermute(glu[TOK - TAPS :], "sp", chain)
     late = conv_late(1, glu, conv_taps)
+    wt = arrange(after(following, late), other)
     copies = convolve(1, before, glu, late, conv_taps, channel_gain)
     parts = exchange_x(copies)
-    wt = arrange(after(following, copies), other)
-    x = project(parts, xs[0], wt, False)
+    x = project(parts, x, wt, False)
     return x
 
 

time: 197 us -> 199 us (1.010)
  blocking collectives: 45.8 us -> 29.6 us
  waiting for transfers between devices: 61.1 us -> 72.4 us
  starting transfers between devices: 55.6 us -> 63.7 us
    all_to_all x1 -> x0, blocking collectives: 16.2 us -> none  [exchange_x(): lax.all_to_all(copies, 'x', split_axis=0, concat_axis=0, tiled=True)]
    ppermute x6 -> x9, starting transfers between devices: 19.3 us -> 27.5 us  [along_x(): return lax.ppermute(v, 'x', [(i, (i + step) % NX) for i in range(NX)])]
    ppermute x6 -> x9, waiting for transfers between devices: 15.8 us -> 22.9 us  [along_x(): return lax.ppermute(v, 'x', [(i, (i + step) % NX) for i in range(NX)])]
    ppermute x1, waiting for transfers between devices: 0.01 us -> 3.29 us  [shards(): extended = jnp.concatenate([lax.ppermute(x, 'sp', chain)[TOK - TAPS:], x])]
    ppermute x2, starting transfers between devices: 16.3 us -> 13.6 us  [swap_cores(): return lax.ppermute(v, 'sp', [(i, i ^ 1) for i in range(count)])]
    ppermute x1, starting transfers between devices: 2.55 us -> 5.23 us  [shards(): before = lax.ppermute(glu[TOK - TAPS:], 'sp', chain)]
    all_to_all x2, waiting for transfers between devices: 37.5 us -> 39.5 us  [plane(): lax.all_to_all(copies, 'sp', split_axis=0, concat_axis=0, tiled=True, axi...]
  transfers between devices with their start and end apart: 14 -> 17, of which waited for: 8 -> 10; matrix products, arithmetic and copies ran while one was open for 2% -> 2% of each run, Pallas kernels for 10% -> 10%
where the time goes in v9:
time: 199 us; the launch traced here: 198 us
  waiting for transfers between devices  72.4 us (36%)
  starting transfers between devices  63.7 us (32%)
  blocking collectives  29.6 us (15%)
  Pallas kernels  28.7 us (14%)
  local copies, waits for them, and re-layouts  2.25 us (1%)
    all_to_all x2, waiting for transfers between devices, plane(): lax.all_to_all(copies, 'sp', split_axis=0, concat_axis=0, tiled=True, axi...  39.5 us
    all_to_all x1, blocking collectives, to_group(): lax.all_to_all(copies, 'sp', split_axis=0, concat_axis=0, tiled=True, axi...  29.6 us
    ppermute x9, starting transfers between devices, along_x(): return lax.ppermute(v, 'x', [(i, (i + step) % NX) for i in range(NX)])  27.5 us
    ppermute x9, waiting for transfers between devices, along_x(): return lax.ppermute(v, 'x', [(i, (i + step) % NX) for i in range(NX)])  22.9 us
    pallas_call x8, Pallas kernels, call(): pl.pallas_call(body, out_shape=out, in_specs=[pl.BlockSpec(memory_space=p...  18.5 us
    ppermute x2, starting transfers between devices, swap_cores(): return lax.ppermute(v, 'sp', [(i, i ^ 1) for i in range(count)])  13.6 us
    all_to_all x2, starting transfers between devices, plane(): lax.all_to_all(copies, 'sp', split_axis=0, concat_axis=0, tiled=True, axi...  10.4 us
    all_to_all x1, waiting for transfers between devices, exchange_x(): lax.all_to_all(copies, 'x', split_axis=0, concat_axis=0, tiled=True)  6.64 us
  transfers between devices with their start and end apart: 17, of which 10 were waited for; matrix products, arithmetic and copies ran while one was open for 2% of the time, Pallas kernels for 10%

profile of v9, /device:TPU:1, one launch (start us, length us, event | category | flops | bytes accessed | tf_op | source)
XLA Modules:
  0.0 197.9 jit_solution(11742372566775023988)
XLA Ops:
  2.8 29.6 %all_to_all.20.refs_0_ = bf16[8,2,48,256]{3,2,1,0:T(8,128)(2,1)S(1)} all-to-all(bf16[8,2,48,256]{3,2,1,0:T(8,128)(2,1)S(1)} %broadcast_in_dim.3), channel_id=1, replica_groups={{0,8,16,24,32,40,48,56},{64,72,80,88,96,104,112,120},{128,136,144,152,1..., dimensions={0} | all-to-all | bytes 786432 | tf_op jit(solution)/shard_map/all_to_all | solution.py:35
  33.6 6.8 %all-to-all-start.1 = ((bf16[8,8,48,256]{3,2,1,0:T(8,128)(2,1)}), bf16[8,8,48,256]{3,2,1,0:T(8,128)(2,1)S(1)}, u32[]{:S(2)}, u32[]{:S(2)}) async-start(bf16[8,8,48,256]{3,2,1,0:T(8,128)(2,1)} %shard_map.74), calls=%async_computation.1 | async-start | bytes 3145728 | tf_op jit(solution)/shard_map/all_to_all | solution.py:45
  41.7 22.5 %all-to-all-done.1.refs_2_.mine = bf16[8,8,48,256]{3,2,1,0:T(8,128)(2,1)S(1)} async-done(((bf16[8,8,48,256]{3,2,1,0:T(8,128)(2,1)}), bf16[8,8,48,256]{3,2,1,0:T(8,128)(2,1)S(1)}, u32[]{:S(2)}, u32[]{:S(2)}) %all-to-all-start.1) | async-done | bytes 1572896 | tf_op jit(solution)/shard_map/all_to_all | solution.py:45
  64.2 3.6 %all-to-all-start.2 = ((bf16[8,8,48,256]{3,2,1,0:T(8,128)(2,1)}), bf16[8,8,48,256]{3,2,1,0:T(8,128)(2,1)S(1)}, u32[]{:S(2)}, u32[]{:S(2)}) async-start(bf16[8,8,48,256]{3,2,1,0:T(8,128)(2,1)} %shard_map.79), calls=%async_computation.2 | async-start | bytes 3145728 | tf_op jit(solution)/shard_map/all_to_all | solution.py:45
  67.8 6.3 %collective-permute-start.5 = (bf16[8,8,48,256]{3,2,1,0:T(8,128)(2,1)S(1)}, bf16[8,8,48,256]{3,2,1,0:T(8,128)(2,1)}, u32[]{:S(2)}, u32[]{:S(2)}) collective-permute-start(bf16[8,8,48,256]{3,2,1,0:T(8,128)(2,1)S(1)} %all-to-all-done.1.refs_2_.mine), channel_id=1, source_target_pairs={{0,4},{4,0},{8,12},{12,8},{16,20},{20,16},{24,28},{28,24},{32,36},... | collective-permute-start | bytes 4718600 | tf_op jit(solution)/shard_map/ppermute | solution.py:57
  74.0 17.1 %all-to-all-done.2.refs_5_.mine = bf16[8,8,48,256]{3,2,1,0:T(8,128)(2,1)S(1)} async-done(((bf16[8,8,48,256]{3,2,1,0:T(8,128)(2,1)}), bf16[8,8,48,256]{3,2,1,0:T(8,128)(2,1)S(1)}, u32[]{:S(2)}, u32[]{:S(2)}) %all-to-all-start.2) | async-done | bytes 1572896 | tf_op jit(solution)/shard_map/all_to_all | solution.py:45
  91.1 7.3 %collective-permute-start.12 = (bf16[8,8,48,256]{3,2,1,0:T(8,128)(2,1)S(1)}, bf16[8,8,48,256]{3,2,1,0:T(8,128)(2,1)}, u32[]{:S(2)}, u32[]{:S(2)}) collective-permute-start(bf16[8,8,48,256]{3,2,1,0:T(8,128)(2,1)S(1)} %all-to-all-done.2.refs_5_.mine), channel_id=1, source_target_pairs={{0,4},{4,0},{8,12},{12,8},{16,20},{20,16},{24,28},{28,24},{32,36},... | collective-permute-start | bytes 4718600 | tf_op jit(solution)/shard_map/ppermute | solution.py:57
  100.5 3.3 %collective-permute-done = bf16[256,512]{1,0:T(8,128)(2,1)S(1)} collective-permute-done((bf16[256,512]{1,0:T(8,128)(2,1)S(1)}, bf16[256,512]{1,0:T(8,128)(2,1)S(1)}, u32[]{:S(2)}, u32[]{:S(2)}) %collective-permute-start) | collective-permute-done | bytes 262176 | tf_op jit(solution)/shard_map/ppermute | solution.py:504
  104.8 3.1 %collective-permute-start.2 = (bf16[384,512]{1,0:T(8,128)(2,1)S(1)}, bf16[384,512]{1,0:T(8,128)(2,1)}, u32[]{:S(2)}, u32[]{:S(2)}) collective-permute-start(bf16[384,512]{1,0:T(8,128)(2,1)S(1)} %pad_maximum_fusion.refs_0_), channel_id=1, source_target_pairs={{0,1},{1,2},{2,3},{3,0},{4,5},{5,6},{6,7},{7,4},{8,9},{9,10},{10,1... | collective-permute-start | bytes 1179656 | tf_op jit(solution)/shard_map/ppermute | solution.py:73
  109.9 4.3 %collective-permute-start.4 = (bf16[384,512]{1,0:T(8,128)(2,1)S(1)}, bf16[384,512]{1,0:T(8,128)(2,1)}, u32[]{:S(2)}, u32[]{:S(2)}) collective-permute-start(bf16[384,512]{1,0:T(8,128)(2,1)S(1)} %pad_maximum_fusion.refs_0_), channel_id=1, source_target_pairs={{0,3},{1,0},{2,1},{3,2},{4,7},{5,4},{6,5},{7,6},{8,11},{9,8},{10,9... | collective-permute-start | bytes 1179656 | tf_op jit(solution)/shard_map/ppermute | solution.py:73
  115.0 11.0 %collective-permute-done.2.refs_1_ = bf16[384,512]{1,0:T(8,128)(2,1)} collective-permute-done((bf16[384,512]{1,0:T(8,128)(2,1)S(1)}, bf16[384,512]{1,0:T(8,128)(2,1)}, u32[]{:S(2)}, u32[]{:S(2)}) %collective-permute-start.2) | collective-permute-done | bytes 393248 | tf_op jit(solution)/shard_map/ppermute | solution.py:73
  126.0 2.8 %collective-permute-done.4.refs_3_ = bf16[384,512]{1,0:T(8,128)(2,1)} collective-permute-done((bf16[384,512]{1,0:T(8,128)(2,1)S(1)}, bf16[384,512]{1,0:T(8,128)(2,1)}, u32[]{:S(2)}, u32[]{:S(2)}) %collective-permute-start.4) | collective-permute-done | bytes 393248 | tf_op jit(solution)/shard_map/ppermute | solution.py:73
  128.8 3.4 %shard_map.73.refs_0_ = bf16[4,384,512]{2,1,0:T(8,128)(2,1)} custom-call(bf16[384,512]{1,0:T(8,128)(2,1)S(1)} %pad_maximum_fusion.refs_0_, bf16[384,512]{1,0:T(8,128)(2,1)} %collective-permute-done.2.refs_1_, bf16[384,512]{1,0:T(8,128)(2,1)} %collective-permute-done.3.refs_2_, bf16[384,512]{1,0:T(8,128)(2,1)} %collective-permute-done.4.refs_3_, ...), custom_call_target="tpu_custom_call" | custom-call | flops 4194304 | bytes 1048576 | tf_op jit(solution)/shard_map/pallas_call | solution.py:318
  132.2 3.0 %shard_map.75.refs_0_ = bf16[384,256]{1,0:T(8,128)(2,1)S(1)} custom-call(bf16[4,384,512]{2,1,0:T(8,128)(2,1)} %shard_map.73.refs_0_, f32[8,1,512]{2,1,0:T(1,128)S(1)} %reshape.3.refs_4_.refs_1_, bf16[8,8,48,256]{3,2,1,0:T(8,128)(2,1)S(1)} %all-to-all-done.1.refs_2_.mine, bf16[8,8,48,256]{3,2,1,0:T(8,128)(2,1)} %collective-permute-done.5.refs_3_.other), custom_call_target="tpu_custom_call" | custom-call | flops 536870912 | bytes 1048576 | tf_op jit(solution)/shard_map/pallas_call | solution.py:358
  135.2 3.4 %shard_map.76.refs_0_ = bf16[272,256]{1,0:T(8,128)(2,1)S(1)} custom-call(bf16[384,256]{1,0:T(8,128)(2,1)S(1)} %shard_map.75.refs_0_, f32[2,128,256]{2,1,0:T(8,128)S(1)} %copy-done, f32[2,256]{1,0:T(2,128)S(1)} %copy-done.2), custom_call_target="tpu_custom_call" | custom-call | flops 16777216 | bytes 1048576 | tf_op jit(solution)/shard_map/pallas_call | solution.py:318
  138.6 2.8 %collective-permute-start.6 = (bf16[272,256]{1,0:T(8,128)(2,1)S(1)}, bf16[272,256]{1,0:T(8,128)(2,1)S(1)}, u32[]{:S(2)}, u32[]{:S(2)}) collective-permute-start(bf16[272,256]{1,0:T(8,128)(2,1)S(1)} %shard_map.76.refs_0_), channel_id=1, source_target_pairs={{0,1},{1,2},{2,3},{3,0},{4,5},{5,6},{6,7},{7,4},{8,9},{9,10},{10,1... | collective-permute-start | bytes 417800 | tf_op jit(solution)/shard_map/ppermute | solution.py:73
  141.4 4.8 %collective-permute-start.7 = (bf16[272,256]{1,0:T(8,128)(2,1)S(1)}, bf16[272,256]{1,0:T(8,128)(2,1)S(1)}, u32[]{:S(2)}, u32[]{:S(2)}) collective-permute-start(bf16[272,256]{1,0:T(8,128)(2,1)S(1)} %shard_map.76.refs_0_), channel_id=1, source_target_pairs={{0,2},{1,3},{2,0},{3,1},{4,6},{5,7},{6,4},{7,5},{8,10},{9,11},{10,... | collective-permute-start | bytes 417800 | tf_op jit(solution)/shard_map/ppermute | solution.py:73
  156.8 4.1 %collective-permute-start.11 = (bf16[256,512]{1,0:T(8,128)(2,1)S(1)}, bf16[256,512]{1,0:T(8,128)(2,1)S(1)}, u32[]{:S(2)}, u32[]{:S(2)}) collective-permute-start(bf16[256,512]{1,0:T(8,128)(2,1)S(1)} %shard_map.78.refs_0_.refs_1_), channel_id=1, source_target_pairs={{0,3},{1,0},{2,1},{3,2},{4,7},{5,4},{6,5},{7,6},{8,11},{9,8},{10,9... | collective-permute-start | bytes 786440 | tf_op jit(solution)/shard_map/ppermute | solution.py:73
  163.6 6.4 %collective-permute-done.11.refs_3_ = bf16[256,512]{1,0:T(8,128)(2,1)S(1)} collective-permute-done((bf16[256,512]{1,0:T(8,128)(2,1)S(1)}, bf16[256,512]{1,0:T(8,128)(2,1)S(1)}, u32[]{:S(2)}, u32[]{:S(2)}) %collective-permute-start.11) | collective-permute-done | bytes 262176 | tf_op jit(solution)/shard_map/ppermute | solution.py:73
  170.2 3.0 %shard_map.80.refs_0_.refs_1_ = bf16[256,256]{1,0:T(8,128)(2,1)S(1)} custom-call(bf16[256,512]{1,0:T(8,128)(2,1)S(1)} %shard_map.78.refs_0_.refs_1_, bf16[256,512]{1,0:T(8,128)(2,1)S(1)} %collective-permute-done.9.refs_1_, bf16[256,512]{1,0:T(8,128)(2,1)S(1)} %collective-permute-done.10.refs_2_, bf16[256,512]{1,0:T(8,128)(2,1)S(1)} %collective-permute-done.11.refs_3_, ...), custom_call_target="tpu_custom_call" | custom-call | flops 536870912 | bytes 1048576 | tf_op jit(solution)/shard_map/pallas_call | solution.py:358
  173.2 5.2 %collective-permute-start.13 = (bf16[128,256]{1,0:T(8,128)(2,1)S(1)}, bf16[128,256]{1,0:T(8,128)(2,1)S(1)}, u32[]{:S(2)}, u32[]{:S(2)}) collective-permute-start(bf16[128,256]{1,0:T(8,128)(2,1)S(1)} %slice.9), channel_id=1, source_target_pairs={{0,4},{4,8},{8,12},{12,16},{16,20},{20,24},{24,28},{28,32},{32,36}... | collective-permute-start | bytes 196616 | tf_op jit(solution)/shard_map/ppermute | solution.py:525
  180.1 2.8 %shard_map.82 = bf16[4,272,256]{2,1,0:T(8,128)(2,1)} custom-call(bf16[128,256]{1,0:T(8,128)(2,1)S(1)} %collective-permute-done.13.refs_0_, bf16[256,256]{1,0:T(8,128)(2,1)S(1)} %shard_map.80.refs_0_.refs_1_, f32[128,256]{1,0:T(8,128)S(1)} %shard_map.81.refs_2_, f32[2,128,256]{2,1,0:T(8,128)S(1)} %copy-done, f32[2,256]{1,0:T(2,128)S(1)} %copy-done.2), custom_call_target="tpu_custom_call" | custom-call | flops 8388608 | bytes 1048576 | tf_op jit(solution)/shard_map/pallas_call | solution.py:318
  182.8 3.5 %all-to-all-start.3 = ((bf16[4,272,256]{2,1,0:T(8,128)(2,1)}), bf16[4,272,256]{2,1,0:T(8,128)(2,1)S(1)}, u32[]{:S(2)}, u32[]{:S(2)}) async-start(bf16[4,272,256]{2,1,0:T(8,128)(2,1)} %shard_map.82), calls=%async_computation.3 | async-start | bytes 1114112 | tf_op jit(solution)/shard_map/all_to_all | solution.py:82
  188.8 6.6 %all-to-all-done.3.refs_0_ = bf16[4,272,256]{2,1,0:T(8,128)(2,1)S(1)} async-done(((bf16[4,272,256]{2,1,0:T(8,128)(2,1)}), bf16[4,272,256]{2,1,0:T(8,128)(2,1)S(1)}, u32[]{:S(2)}, u32[]{:S(2)}) %all-to-all-start.3) | async-done | bytes 557088 | tf_op jit(solution)/shard_map/all_to_all | solution.py:82
  (39 shorter events, 31.0 us)
Async XLA Ops:
  0.0 2.8 %collective-permute-start.1 = (bf16[2,16,256]{2,1,0:T(8,128)(2,1)}, bf16[2,16,256]{2,1,0:T(8,128)(2,1)S(1)}, u32[]{:S(2)}, u32[]{:S(2)}) collective-permute-start(bf16[2,16,256]{2,1,0:T(8,128)(2,1)} %bitcast.1), channel_id=1, source_target_pairs={{0,0},{1,128},{2,256},{3,384},{4,4},{5,132},{6,260},{7,388},{8,8},... | collective-permute-start | bytes 49160 | tf_op jit(solution)/shard_map/ppermute | solution.py:69
  33.6 30.6 %all-to-all-start.1 = ((bf16[8,8,48,256]{3,2,1,0:T(8,128)(2,1)}), bf16[8,8,48,256]{3,2,1,0:T(8,128)(2,1)S(1)}, u32[]{:S(2)}, u32[]{:S(2)}) async-start(bf16[8,8,48,256]{3,2,1,0:T(8,128)(2,1)} %shard_map.74), calls=%async_computation.1 | async-start | bytes 3145728 | tf_op jit(solution)/shard_map/all_to_all | solution.py:45
  41.7 56.8 %copy-start.3 = (bf16[256,512]{1,0:T(8,128)(2,1)S(1)}, bf16[256,512]{1,0:T(8,128)(2,1)}, u32[]{:S(2)}) copy-start(bf16[256,512]{1,0:T(8,128)(2,1)} %refs_4_.2) | copy-start | bytes 786436
  64.2 26.9 %all-to-all-start.2 = ((bf16[8,8,48,256]{3,2,1,0:T(8,128)(2,1)}), bf16[8,8,48,256]{3,2,1,0:T(8,128)(2,1)S(1)}, u32[]{:S(2)}, u32[]{:S(2)}) async-start(bf16[8,8,48,256]{3,2,1,0:T(8,128)(2,1)} %shard_map.79), calls=%async_computation.2 | async-start | bytes 3145728 | tf_op jit(solution)/shard_map/all_to_all | solution.py:45
  67.8 64.5 %collective-permute-start.5 = (bf16[8,8,48,256]{3,2,1,0:T(8,128)(2,1)S(1)}, bf16[8,8,48,256]{3,2,1,0:T(8,128)(2,1)}, u32[]{:S(2)}, u32[]{:S(2)}) collective-permute-start(bf16[8,8,48,256]{3,2,1,0:T(8,128)(2,1)S(1)} %all-to-all-done.1.refs_2_.mine), channel_id=1, source_target_pairs={{0,4},{4,0},{8,12},{12,8},{16,20},{20,16},{24,28},{28,24},{32,36},... | collective-permute-start | bytes 4718600 | tf_op jit(solution)/shard_map/ppermute | solution.py:57
  91.1 79.1 %collective-permute-start.12 = (bf16[8,8,48,256]{3,2,1,0:T(8,128)(2,1)S(1)}, bf16[8,8,48,256]{3,2,1,0:T(8,128)(2,1)}, u32[]{:S(2)}, u32[]{:S(2)}) collective-permute-start(bf16[8,8,48,256]{3,2,1,0:T(8,128)(2,1)S(1)} %all-to-all-done.2.refs_5_.mine), channel_id=1, source_target_pairs={{0,4},{4,0},{8,12},{12,8},{16,20},{20,16},{24,28},{28,24},{32,36},... | collective-permute-start | bytes 4718600 | tf_op jit(solution)/shard_map/ppermute | solution.py:57
  98.4 5.4 %collective-permute-start = (bf16[256,512]{1,0:T(8,128)(2,1)S(1)}, bf16[256,512]{1,0:T(8,128)(2,1)S(1)}, u32[]{:S(2)}, u32[]{:S(2)}) collective-permute-start(bf16[256,512]{1,0:T(8,128)(2,1)S(1)} %copy-done.3), channel_id=1, source_target_pairs={{0,4},{4,8},{8,12},{12,16},{16,20},{20,24},{24,28},{28,32},{32,36}... | collective-permute-start | bytes 786440 | tf_op jit(solution)/shard_map/ppermute | solution.py:504
  104.8 21.1 %collective-permute-start.2 = (bf16[384,512]{1,0:T(8,128)(2,1)S(1)}, bf16[384,512]{1,0:T(8,128)(2,1)}, u32[]{:S(2)}, u32[]{:S(2)}) collective-permute-start(bf16[384,512]{1,0:T(8,128)(2,1)S(1)} %pad_maximum_fusion.refs_0_), channel_id=1, source_target_pairs={{0,1},{1,2},{2,3},{3,0},{4,5},{5,6},{6,7},{7,4},{8,9},{9,10},{10,1... | collective-permute-start | bytes 1179656 | tf_op jit(solution)/shard_map/ppermute | solution.py:73
  108.0 18.0 %collective-permute-start.3 = (bf16[384,512]{1,0:T(8,128)(2,1)S(1)}, bf16[384,512]{1,0:T(8,128)(2,1)}, u32[]{:S(2)}, u32[]{:S(2)}) collective-permute-start(bf16[384,512]{1,0:T(8,128)(2,1)S(1)} %pad_maximum_fusion.refs_0_), channel_id=1, source_target_pairs={{0,2},{1,3},{2,0},{3,1},{4,6},{5,7},{6,4},{7,5},{8,10},{9,11},{10,... | collective-permute-start | bytes 1179656 | tf_op jit(solution)/shard_map/ppermute | solution.py:73
  109.9 18.8 %collective-permute-start.4 = (bf16[384,512]{1,0:T(8,128)(2,1)S(1)}, bf16[384,512]{1,0:T(8,128)(2,1)}, u32[]{:S(2)}, u32[]{:S(2)}) collective-permute-start(bf16[384,512]{1,0:T(8,128)(2,1)S(1)} %pad_maximum_fusion.refs_0_), channel_id=1, source_target_pairs={{0,3},{1,0},{2,1},{3,2},{4,7},{5,4},{6,5},{7,6},{8,11},{9,8},{10,9... | collective-permute-start | bytes 1179656 | tf_op jit(solution)/shard_map/ppermute | solution.py:73
  132.2 3.1 %copy-start = (f32[2,128,256]{2,1,0:T(8,128)S(1)}, f32[2,128,256]{2,1,0:T(8,128)}, u32[]{:S(2)}) copy-start(f32[2,128,256]{2,1,0:T(8,128)} %refs_3_.1) | copy-start | bytes 786436
  132.2 3.0 %copy-start.2 = (f32[2,256]{1,0:T(2,128)S(1)}, f32[2,256]{1,0:T(2,128)}, u32[]{:S(2)}) copy-start(f32[2,256]{1,0:T(2,128)} %refs_4_.3) | copy-start | bytes 6148
  138.6 11.9 %collective-permute-start.6 = (bf16[272,256]{1,0:T(8,128)(2,1)S(1)}, bf16[272,256]{1,0:T(8,128)(2,1)S(1)}, u32[]{:S(2)}, u32[]{:S(2)}) collective-permute-start(bf16[272,256]{1,0:T(8,128)(2,1)S(1)} %shard_map.76.refs_0_), channel_id=1, source_target_pairs={{0,1},{1,2},{2,3},{3,0},{4,5},{5,6},{6,7},{7,4},{8,9},{9,10},{10,1... | collective-permute-start | bytes 417800 | tf_op jit(solution)/shard_map/ppermute | solution.py:73
  141.4 9.2 %collective-permute-start.7 = (bf16[272,256]{1,0:T(8,128)(2,1)S(1)}, bf16[272,256]{1,0:T(8,128)(2,1)S(1)}, u32[]{:S(2)}, u32[]{:S(2)}) collective-permute-start(bf16[272,256]{1,0:T(8,128)(2,1)S(1)} %shard_map.76.refs_0_), channel_id=1, source_target_pairs={{0,2},{1,3},{2,0},{3,1},{4,6},{5,7},{6,4},{7,5},{8,10},{9,11},{10,... | collective-permute-start | bytes 417800 | tf_op jit(solution)/shard_map/ppermute | solution.py:73
  146.2 6.2 %collective-permute-start.8 = (bf16[272,256]{1,0:T(8,128)(2,1)S(1)}, bf16[272,256]{1,0:T(8,128)(2,1)S(1)}, u32[]{:S(2)}, u32[]{:S(2)}) collective-permute-start(bf16[272,256]{1,0:T(8,128)(2,1)S(1)} %shard_map.76.refs_0_), channel_id=1, source_target_pairs={{0,3},{1,0},{2,1},{3,2},{4,7},{5,4},{6,5},{7,6},{8,11},{9,8},{10,9... | collective-permute-start | bytes 417800 | tf_op jit(solution)/shard_map/ppermute | solution.py:73
  154.1 19.1 %copy-start.1 = (bf16[256,512]{1,0:T(8,128)(2,1)}, bf16[256,512]{1,0:T(8,128)(2,1)S(1)}, u32[]{:S(2)}) copy-start(bf16[256,512]{1,0:T(8,128)(2,1)S(1)} %shard_map.78.refs_0_.refs_1_) | copy-start | bytes 786436
  154.2 9.4 %collective-permute-start.10 = (bf16[256,512]{1,0:T(8,128)(2,1)S(1)}, bf16[256,512]{1,0:T(8,128)(2,1)S(1)}, u32[]{:S(2)}, u32[]{:S(2)}) collective-permute-start(bf16[256,512]{1,0:T(8,128)(2,1)S(1)} %shard_map.78.refs_0_.refs_1_), channel_id=1, source_target_pairs={{0,2},{1,3},{2,0},{3,1},{4,6},{5,7},{6,4},{7,5},{8,10},{9,11},{10,... | collective-permute-start | bytes 786440 | tf_op jit(solution)/shard_map/ppermute | solution.py:73
  156.8 13.2 %collective-permute-start.11 = (bf16[256,512]{1,0:T(8,128)(2,1)S(1)}, bf16[256,512]{1,0:T(8,128)(2,1)S(1)}, u32[]{:S(2)}, u32[]{:S(2)}) collective-permute-start(bf16[256,512]{1,0:T(8,128)(2,1)S(1)} %shard_map.78.refs_0_.refs_1_), channel_id=1, source_target_pairs={{0,3},{1,0},{2,1},{3,2},{4,7},{5,4},{6,5},{7,6},{8,11},{9,8},{10,9... | collective-permute-start | bytes 786440 | tf_op jit(solution)/shard_map/ppermute | solution.py:73
  160.9 9.3 %collective-permute-start.9 = (bf16[256,512]{1,0:T(8,128)(2,1)S(1)}, bf16[256,512]{1,0:T(8,128)(2,1)S(1)}, u32[]{:S(2)}, u32[]{:S(2)}) collective-permute-start(bf16[256,512]{1,0:T(8,128)(2,1)S(1)} %shard_map.78.refs_0_.refs_1_), channel_id=1, source_target_pairs={{0,1},{1,2},{2,3},{3,0},{4,5},{5,6},{6,7},{7,4},{8,9},{9,10},{10,1... | collective-permute-start | bytes 786440 | tf_op jit(solution)/shard_map/ppermute | solution.py:73
  173.2 6.8 %collective-permute-start.13 = (bf16[128,256]{1,0:T(8,128)(2,1)S(1)}, bf16[128,256]{1,0:T(8,128)(2,1)S(1)}, u32[]{:S(2)}, u32[]{:S(2)}) collective-permute-start(bf16[128,256]{1,0:T(8,128)(2,1)S(1)} %slice.9), channel_id=1, source_target_pairs={{0,4},{4,8},{8,12},{12,16},{16,20},{20,24},{24,28},{28,32},{32,36}... | collective-permute-start | bytes 196616 | tf_op jit(solution)/shard_map/ppermute | solution.py:525
  182.8 12.6 %all-to-all-start.3 = ((bf16[4,272,256]{2,1,0:T(8,128)(2,1)}), bf16[4,272,256]{2,1,0:T(8,128)(2,1)S(1)}, u32[]{:S(2)}, u32[]{:S(2)}) async-start(bf16[4,272,256]{2,1,0:T(8,128)(2,1)} %shard_map.82), calls=%async_computation.3 | async-start | bytes 1114112 | tf_op jit(solution)/shard_map/all_to_all | solution.py:82

commit v10 on v9

--- a/solution.py
+++ b/solution.py
@@ -203,7 +203,7 @@
                     acc += window * tap[b : b + 1]
                 return acc
 
-            acc = lax.fori_loop(0, TAPS // 8, step, jnp.zeros((HALF, 128), F32))
+            acc = lax.fori_loop(0, TAPS // 8, step, jnp.zeros((HALF, 128), F32), unroll=4)
             conv[base : base + HALF, lane : lane + 128] = acc
 
 
@@ -275,7 +275,7 @@
         scale[rows, :] = square
         return 0
 
-    lax.fori_loop(0, TOK // 16, squares, 0, unroll=2)
+    lax.fori_loop(0, TOK // 16, squares, 0, unroll=4)
     spread = jnp.sum(scale[...], axis=1, keepdims=True) / C
     scale[...] = jnp.broadcast_to(lax.rsqrt(spread + 1e-05), (TOK, 128))
     gains = []
@@ -292,7 +292,7 @@
             acts[owner, rows, :] = (u / (1.0 + jnp.exp(-u))).astype(BF)
         return 0
 
-    lax.fori_loop(0, TOK // 16, activate, 0, unroll=2)
+    lax.fori_loop(0, TOK // 16, activate, 0, unroll=4)
     weights.wait()
     branch = jnp.zeros((TOK, FEAT), F32)
     for k in range(NX):

time: 199 us -> 199 us (level)
  no operation moved by 1% of the time
where the time goes in v10:
time: 199 us; the launch traced here: 198 us
  waiting for transfers between devices  72.4 us (36%)
  starting transfers between devices  63.7 us (32%)
  blocking collectives  29.6 us (15%)
  Pallas kernels  28.4 us (14%)
  local copies, waits for them, and re-layouts  2.25 us (1%)
    all_to_all x2, waiting for transfers between devices, plane(): lax.all_to_all(copies, 'sp', split_axis=0, concat_axis=0, tiled=True, axi...  39.5 us
    all_to_all x1, blocking collectives, to_group(): lax.all_to_all(copies, 'sp', split_axis=0, concat_axis=0, tiled=True, axi...  29.6 us
    ppermute x9, starting transfers between devices, along_x(): return lax.ppermute(v, 'x', [(i, (i + step) % NX) for i in range(NX)])  27.5 us
    ppermute x9, waiting for transfers between devices, along_x(): return lax.ppermute(v, 'x', [(i, (i + step) % NX) for i in range(NX)])  22.9 us
    pallas_call x8, Pallas kernels, call(): pl.pallas_call(body, out_shape=out, in_specs=[pl.BlockSpec(memory_space=p...  18.1 us
    ppermute x2, starting transfers between devices, swap_cores(): return lax.ppermute(v, 'sp', [(i, i ^ 1) for i in range(count)])  13.6 us
    all_to_all x2, starting transfers between devices, plane(): lax.all_to_all(copies, 'sp', split_axis=0, concat_axis=0, tiled=True, axi...  10.4 us
    all_to_all x1, waiting for transfers between devices, exchange_x(): lax.all_to_all(copies, 'x', split_axis=0, concat_axis=0, tiled=True)  6.64 us
  transfers between devices with their start and end apart: 17, of which 10 were waited for; matrix products, arithmetic and copies ran while one was open for 2% of the time, Pallas kernels for 10%

profile of v10, /device:TPU:1, one launch (start us, length us, event | category | flops | bytes accessed | tf_op | source)
XLA Modules:
  0.0 197.5 jit_solution(5516017551378994499)
XLA Ops:
  2.8 29.6 %all_to_all.20.refs_0_ = bf16[8,2,48,256]{3,2,1,0:T(8,128)(2,1)S(1)} all-to-all(bf16[8,2,48,256]{3,2,1,0:T(8,128)(2,1)S(1)} %broadcast_in_dim.3), channel_id=1, replica_groups={{0,8,16,24,32,40,48,56},{64,72,80,88,96,104,112,120},{128,136,144,152,1..., dimensions={0} | all-to-all | bytes 786432 | tf_op jit(solution)/shard_map/all_to_all | solution.py:35
  33.6 6.8 %all-to-all-start.1 = ((bf16[8,8,48,256]{3,2,1,0:T(8,128)(2,1)}), bf16[8,8,48,256]{3,2,1,0:T(8,128)(2,1)S(1)}, u32[]{:S(2)}, u32[]{:S(2)}) async-start(bf16[8,8,48,256]{3,2,1,0:T(8,128)(2,1)} %shard_map.74), calls=%async_computation.1 | async-start | bytes 3145728 | tf_op jit(solution)/shard_map/all_to_all | solution.py:45
  41.7 22.5 %all-to-all-done.1.refs_2_.mine = bf16[8,8,48,256]{3,2,1,0:T(8,128)(2,1)S(1)} async-done(((bf16[8,8,48,256]{3,2,1,0:T(8,128)(2,1)}), bf16[8,8,48,256]{3,2,1,0:T(8,128)(2,1)S(1)}, u32[]{:S(2)}, u32[]{:S(2)}) %all-to-all-start.1) | async-done | bytes 1572896 | tf_op jit(solution)/shard_map/all_to_all | solution.py:45
  64.2 3.6 %all-to-all-start.2 = ((bf16[8,8,48,256]{3,2,1,0:T(8,128)(2,1)}), bf16[8,8,48,256]{3,2,1,0:T(8,128)(2,1)S(1)}, u32[]{:S(2)}, u32[]{:S(2)}) async-start(bf16[8,8,48,256]{3,2,1,0:T(8,128)(2,1)} %shard_map.79), calls=%async_computation.2 | async-start | bytes 3145728 | tf_op jit(solution)/shard_map/all_to_all | solution.py:45
  67.8 6.3 %collective-permute-start.5 = (bf16[8,8,48,256]{3,2,1,0:T(8,128)(2,1)S(1)}, bf16[8,8,48,256]{3,2,1,0:T(8,128)(2,1)}, u32[]{:S(2)}, u32[]{:S(2)}) collective-permute-start(bf16[8,8,48,256]{3,2,1,0:T(8,128)(2,1)S(1)} %all-to-all-done.1.refs_2_.mine), channel_id=1, source_target_pairs={{0,4},{4,0},{8,12},{12,8},{16,20},{20,16},{24,28},{28,24},{32,36},... | collective-permute-start | bytes 4718600 | tf_op jit(solution)/shard_map/ppermute | solution.py:57
  74.0 17.1 %all-to-all-done.2.refs_5_.mine = bf16[8,8,48,256]{3,2,1,0:T(8,128)(2,1)S(1)} async-done(((bf16[8,8,48,256]{3,2,1,0:T(8,128)(2,1)}), bf16[8,8,48,256]{3,2,1,0:T(8,128)(2,1)S(1)}, u32[]{:S(2)}, u32[]{:S(2)}) %all-to-all-start.2) | async-done | bytes 1572896 | tf_op jit(solution)/shard_map/all_to_all | solution.py:45
  91.1 7.3 %collective-permute-start.12 = (bf16[8,8,48,256]{3,2,1,0:T(8,128)(2,1)S(1)}, bf16[8,8,48,256]{3,2,1,0:T(8,128)(2,1)}, u32[]{:S(2)}, u32[]{:S(2)}) collective-permute-start(bf16[8,8,48,256]{3,2,1,0:T(8,128)(2,1)S(1)} %all-to-all-done.2.refs_5_.mine), channel_id=1, source_target_pairs={{0,4},{4,0},{8,12},{12,8},{16,20},{20,16},{24,28},{28,24},{32,36},... | collective-permute-start | bytes 4718600 | tf_op jit(solution)/shard_map/ppermute | solution.py:57
  100.5 3.3 %collective-permute-done = bf16[256,512]{1,0:T(8,128)(2,1)S(1)} collective-permute-done((bf16[256,512]{1,0:T(8,128)(2,1)S(1)}, bf16[256,512]{1,0:T(8,128)(2,1)S(1)}, u32[]{:S(2)}, u32[]{:S(2)}) %collective-permute-start) | collective-permute-done | bytes 262176 | tf_op jit(solution)/shard_map/ppermute | solution.py:504
  104.8 3.1 %collective-permute-start.2 = (bf16[384,512]{1,0:T(8,128)(2,1)S(1)}, bf16[384,512]{1,0:T(8,128)(2,1)}, u32[]{:S(2)}, u32[]{:S(2)}) collective-permute-start(bf16[384,512]{1,0:T(8,128)(2,1)S(1)} %pad_maximum_fusion.refs_0_), channel_id=1, source_target_pairs={{0,1},{1,2},{2,3},{3,0},{4,5},{5,6},{6,7},{7,4},{8,9},{9,10},{10,1... | collective-permute-start | bytes 1179656 | tf_op jit(solution)/shard_map/ppermute | solution.py:73
  109.9 4.3 %collective-permute-start.4 = (bf16[384,512]{1,0:T(8,128)(2,1)S(1)}, bf16[384,512]{1,0:T(8,128)(2,1)}, u32[]{:S(2)}, u32[]{:S(2)}) collective-permute-start(bf16[384,512]{1,0:T(8,128)(2,1)S(1)} %pad_maximum_fusion.refs_0_), channel_id=1, source_target_pairs={{0,3},{1,0},{2,1},{3,2},{4,7},{5,4},{6,5},{7,6},{8,11},{9,8},{10,9... | collective-permute-start | bytes 1179656 | tf_op jit(solution)/shard_map/ppermute | solution.py:73
  115.0 11.0 %collective-permute-done.2.refs_1_ = bf16[384,512]{1,0:T(8,128)(2,1)} collective-permute-done((bf16[384,512]{1,0:T(8,128)(2,1)S(1)}, bf16[384,512]{1,0:T(8,128)(2,1)}, u32[]{:S(2)}, u32[]{:S(2)}) %collective-permute-start.2) | collective-permute-done | bytes 393248 | tf_op jit(solution)/shard_map/ppermute | solution.py:73
  126.0 2.8 %collective-permute-done.4.refs_3_ = bf16[384,512]{1,0:T(8,128)(2,1)} collective-permute-done((bf16[384,512]{1,0:T(8,128)(2,1)S(1)}, bf16[384,512]{1,0:T(8,128)(2,1)}, u32[]{:S(2)}, u32[]{:S(2)}) %collective-permute-start.4) | collective-permute-done | bytes 393248 | tf_op jit(solution)/shard_map/ppermute | solution.py:73
  128.8 3.4 %shard_map.73.refs_0_ = bf16[4,384,512]{2,1,0:T(8,128)(2,1)} custom-call(bf16[384,512]{1,0:T(8,128)(2,1)S(1)} %pad_maximum_fusion.refs_0_, bf16[384,512]{1,0:T(8,128)(2,1)} %collective-permute-done.2.refs_1_, bf16[384,512]{1,0:T(8,128)(2,1)} %collective-permute-done.3.refs_2_, bf16[384,512]{1,0:T(8,128)(2,1)} %collective-permute-done.4.refs_3_, ...), custom_call_target="tpu_custom_call" | custom-call | flops 4194304 | bytes 1048576 | tf_op jit(solution)/shard_map/pallas_call | solution.py:318
  132.2 3.0 %shard_map.75.refs_0_ = bf16[384,256]{1,0:T(8,128)(2,1)S(1)} custom-call(bf16[4,384,512]{2,1,0:T(8,128)(2,1)} %shard_map.73.refs_0_, f32[8,1,512]{2,1,0:T(1,128)S(1)} %reshape.3.refs_4_.refs_1_, bf16[8,8,48,256]{3,2,1,0:T(8,128)(2,1)S(1)} %all-to-all-done.1.refs_2_.mine, bf16[8,8,48,256]{3,2,1,0:T(8,128)(2,1)} %collective-permute-done.5.refs_3_.other), custom_call_target="tpu_custom_call" | custom-call | flops 536870912 | bytes 1048576 | tf_op jit(solution)/shard_map/pallas_call | solution.py:358
  135.2 3.2 %shard_map.76.refs_0_ = bf16[272,256]{1,0:T(8,128)(2,1)S(1)} custom-call(bf16[384,256]{1,0:T(8,128)(2,1)S(1)} %shard_map.75.refs_0_, f32[2,128,256]{2,1,0:T(8,128)S(1)} %copy-done, f32[2,256]{1,0:T(2,128)S(1)} %copy-done.2), custom_call_target="tpu_custom_call" | custom-call | flops 16777216 | bytes 1048576 | tf_op jit(solution)/shard_map/pallas_call | solution.py:318
  138.4 2.8 %collective-permute-start.6 = (bf16[272,256]{1,0:T(8,128)(2,1)S(1)}, bf16[272,256]{1,0:T(8,128)(2,1)S(1)}, u32[]{:S(2)}, u32[]{:S(2)}) collective-permute-start(bf16[272,256]{1,0:T(8,128)(2,1)S(1)} %shard_map.76.refs_0_), channel_id=1, source_target_pairs={{0,1},{1,2},{2,3},{3,0},{4,5},{5,6},{6,7},{7,4},{8,9},{9,10},{10,1... | collective-permute-start | bytes 417800 | tf_op jit(solution)/shard_map/ppermute | solution.py:73
  141.2 4.8 %collective-permute-start.7 = (bf16[272,256]{1,0:T(8,128)(2,1)S(1)}, bf16[272,256]{1,0:T(8,128)(2,1)S(1)}, u32[]{:S(2)}, u32[]{:S(2)}) collective-permute-start(bf16[272,256]{1,0:T(8,128)(2,1)S(1)} %shard_map.76.refs_0_), channel_id=1, source_target_pairs={{0,2},{1,3},{2,0},{3,1},{4,6},{5,7},{6,4},{7,5},{8,10},{9,11},{10,... | collective-permute-start | bytes 417800 | tf_op jit(solution)/shard_map/ppermute | solution.py:73
  156.6 4.1 %collective-permute-start.11 = (bf16[256,512]{1,0:T(8,128)(2,1)S(1)}, bf16[256,512]{1,0:T(8,128)(2,1)S(1)}, u32[]{:S(2)}, u32[]{:S(2)}) collective-permute-start(bf16[256,512]{1,0:T(8,128)(2,1)S(1)} %shard_map.78.refs_0_.refs_1_), channel_id=1, source_target_pairs={{0,3},{1,0},{2,1},{3,2},{4,7},{5,4},{6,5},{7,6},{8,11},{9,8},{10,9... | collective-permute-start | bytes 786440 | tf_op jit(solution)/shard_map/ppermute | solution.py:73
  163.4 6.4 %collective-permute-done.11.refs_3_ = bf16[256,512]{1,0:T(8,128)(2,1)S(1)} collective-permute-done((bf16[256,512]{1,0:T(8,128)(2,1)S(1)}, bf16[256,512]{1,0:T(8,128)(2,1)S(1)}, u32[]{:S(2)}, u32[]{:S(2)}) %collective-permute-start.11) | collective-permute-done | bytes 262176 | tf_op jit(solution)/shard_map/ppermute | solution.py:73
  170.0 3.0 %shard_map.80.refs_0_.refs_1_ = bf16[256,256]{1,0:T(8,128)(2,1)S(1)} custom-call(bf16[256,512]{1,0:T(8,128)(2,1)S(1)} %shard_map.78.refs_0_.refs_1_, bf16[256,512]{1,0:T(8,128)(2,1)S(1)} %collective-permute-done.9.refs_1_, bf16[256,512]{1,0:T(8,128)(2,1)S(1)} %collective-permute-done.10.refs_2_, bf16[256,512]{1,0:T(8,128)(2,1)S(1)} %collective-permute-done.11.refs_3_, ...), custom_call_target="tpu_custom_call" | custom-call | flops 536870912 | bytes 1048576 | tf_op jit(solution)/shard_map/pallas_call | solution.py:358
  173.0 5.2 %collective-permute-start.13 = (bf16[128,256]{1,0:T(8,128)(2,1)S(1)}, bf16[128,256]{1,0:T(8,128)(2,1)S(1)}, u32[]{:S(2)}, u32[]{:S(2)}) collective-permute-start(bf16[128,256]{1,0:T(8,128)(2,1)S(1)} %slice.9), channel_id=1, source_target_pairs={{0,4},{4,8},{8,12},{12,16},{16,20},{20,24},{24,28},{28,32},{32,36}... | collective-permute-start | bytes 196616 | tf_op jit(solution)/shard_map/ppermute | solution.py:525
  179.8 2.7 %shard_map.82 = bf16[4,272,256]{2,1,0:T(8,128)(2,1)} custom-call(bf16[128,256]{1,0:T(8,128)(2,1)S(1)} %collective-permute-done.13.refs_0_, bf16[256,256]{1,0:T(8,128)(2,1)S(1)} %shard_map.80.refs_0_.refs_1_, f32[128,256]{1,0:T(8,128)S(1)} %shard_map.81.refs_2_, f32[2,128,256]{2,1,0:T(8,128)S(1)} %copy-done, f32[2,256]{1,0:T(2,128)S(1)} %copy-done.2), custom_call_target="tpu_custom_call" | custom-call | flops 8388608 | bytes 1048576 | tf_op jit(solution)/shard_map/pallas_call | solution.py:318
  182.5 3.5 %all-to-all-start.3 = ((bf16[4,272,256]{2,1,0:T(8,128)(2,1)}), bf16[4,272,256]{2,1,0:T(8,128)(2,1)S(1)}, u32[]{:S(2)}, u32[]{:S(2)}) async-start(bf16[4,272,256]{2,1,0:T(8,128)(2,1)} %shard_map.82), calls=%async_computation.3 | async-start | bytes 1114112 | tf_op jit(solution)/shard_map/all_to_all | solution.py:82
  188.4 6.6 %all-to-all-done.3.refs_0_ = bf16[4,272,256]{2,1,0:T(8,128)(2,1)S(1)} async-done(((bf16[4,272,256]{2,1,0:T(8,128)(2,1)}), bf16[4,272,256]{2,1,0:T(8,128)(2,1)S(1)}, u32[]{:S(2)}, u32[]{:S(2)}) %all-to-all-start.3) | async-done | bytes 557088 | tf_op jit(solution)/shard_map/all_to_all | solution.py:82
  (39 shorter events, 30.9 us)
Async XLA Ops:
  0.0 2.8 %collective-permute-start.1 = (bf16[2,16,256]{2,1,0:T(8,128)(2,1)}, bf16[2,16,256]{2,1,0:T(8,128)(2,1)S(1)}, u32[]{:S(2)}, u32[]{:S(2)}) collective-permute-start(bf16[2,16,256]{2,1,0:T(8,128)(2,1)} %bitcast.1), channel_id=1, source_target_pairs={{0,0},{1,128},{2,256},{3,384},{4,4},{5,132},{6,260},{7,388},{8,8},... | collective-permute-start | bytes 49160 | tf_op jit(solution)/shard_map/ppermute | solution.py:69
  33.6 30.6 %all-to-all-start.1 = ((bf16[8,8,48,256]{3,2,1,0:T(8,128)(2,1)}), bf16[8,8,48,256]{3,2,1,0:T(8,128)(2,1)S(1)}, u32[]{:S(2)}, u32[]{:S(2)}) async-start(bf16[8,8,48,256]{3,2,1,0:T(8,128)(2,1)} %shard_map.74), calls=%async_computation.1 | async-start | bytes 3145728 | tf_op jit(solution)/shard_map/all_to_all | solution.py:45
  41.7 56.8 %copy-start.3 = (bf16[256,512]{1,0:T(8,128)(2,1)S(1)}, bf16[256,512]{1,0:T(8,128)(2,1)}, u32[]{:S(2)}) copy-start(bf16[256,512]{1,0:T(8,128)(2,1)} %refs_4_.2) | copy-start | bytes 786436
  64.2 26.9 %all-to-all-start.2 = ((bf16[8,8,48,256]{3,2,1,0:T(8,128)(2,1)}), bf16[8,8,48,256]{3,2,1,0:T(8,128)(2,1)S(1)}, u32[]{:S(2)}, u32[]{:S(2)}) async-start(bf16[8,8,48,256]{3,2,1,0:T(8,128)(2,1)} %shard_map.79), calls=%async_computation.2 | async-start | bytes 3145728 | tf_op jit(solution)/shard_map/all_to_all | solution.py:45
  67.8 64.5 %collective-permute-start.5 = (bf16[8,8,48,256]{3,2,1,0:T(8,128)(2,1)S(1)}, bf16[8,8,48,256]{3,2,1,0:T(8,128)(2,1)}, u32[]{:S(2)}, u32[]{:S(2)}) collective-permute-start(bf16[8,8,48,256]{3,2,1,0:T(8,128)(2,1)S(1)} %all-to-all-done.1.refs_2_.mine), channel_id=1, source_target_pairs={{0,4},{4,0},{8,12},{12,8},{16,20},{20,16},{24,28},{28,24},{32,36},... | collective-permute-start | bytes 4718600 | tf_op jit(solution)/shard_map/ppermute | solution.py:57
  91.1 78.9 %collective-permute-start.12 = (bf16[8,8,48,256]{3,2,1,0:T(8,128)(2,1)S(1)}, bf16[8,8,48,256]{3,2,1,0:T(8,128)(2,1)}, u32[]{:S(2)}, u32[]{:S(2)}) collective-permute-start(bf16[8,8,48,256]{3,2,1,0:T(8,128)(2,1)S(1)} %all-to-all-done.2.refs_5_.mine), channel_id=1, source_target_pairs={{0,4},{4,0},{8,12},{12,8},{16,20},{20,16},{24,28},{28,24},{32,36},... | collective-permute-start | bytes 4718600 | tf_op jit(solution)/shard_map/ppermute | solution.py:57
  98.4 5.4 %collective-permute-start = (bf16[256,512]{1,0:T(8,128)(2,1)S(1)}, bf16[256,512]{1,0:T(8,128)(2,1)S(1)}, u32[]{:S(2)}, u32[]{:S(2)}) collective-permute-start(bf16[256,512]{1,0:T(8,128)(2,1)S(1)} %copy-done.3), channel_id=1, source_target_pairs={{0,4},{4,8},{8,12},{12,16},{16,20},{20,24},{24,28},{28,32},{32,36}... | collective-permute-start | bytes 786440 | tf_op jit(solution)/shard_map/ppermute | solution.py:504
  104.8 21.1 %collective-permute-start.2 = (bf16[384,512]{1,0:T(8,128)(2,1)S(1)}, bf16[384,512]{1,0:T(8,128)(2,1)}, u32[]{:S(2)}, u32[]{:S(2)}) collective-permute-start(bf16[384,512]{1,0:T(8,128)(2,1)S(1)} %pad_maximum_fusion.refs_0_), channel_id=1, source_target_pairs={{0,1},{1,2},{2,3},{3,0},{4,5},{5,6},{6,7},{7,4},{8,9},{9,10},{10,1... | collective-permute-start | bytes 1179656 | tf_op jit(solution)/shard_map/ppermute | solution.py:73
  108.0 18.0 %collective-permute-start.3 = (bf16[384,512]{1,0:T(8,128)(2,1)S(1)}, bf16[384,512]{1,0:T(8,128)(2,1)}, u32[]{:S(2)}, u32[]{:S(2)}) collective-permute-start(bf16[384,512]{1,0:T(8,128)(2,1)S(1)} %pad_maximum_fusion.refs_0_), channel_id=1, source_target_pairs={{0,2},{1,3},{2,0},{3,1},{4,6},{5,7},{6,4},{7,5},{8,10},{9,11},{10,... | collective-permute-start | bytes 1179656 | tf_op jit(solution)/shard_map/ppermute | solution.py:73
  109.9 18.8 %collective-permute-start.4 = (bf16[384,512]{1,0:T(8,128)(2,1)S(1)}, bf16[384,512]{1,0:T(8,128)(2,1)}, u32[]{:S(2)}, u32[]{:S(2)}) collective-permute-start(bf16[384,512]{1,0:T(8,128)(2,1)S(1)} %pad_maximum_fusion.refs_0_), channel_id=1, source_target_pairs={{0,3},{1,0},{2,1},{3,2},{4,7},{5,4},{6,5},{7,6},{8,11},{9,8},{10,9... | collective-permute-start | bytes 1179656 | tf_op jit(solution)/shard_map/ppermute | solution.py:73
  132.2 3.1 %copy-start = (f32[2,128,256]{2,1,0:T(8,128)S(1)}, f32[2,128,256]{2,1,0:T(8,128)}, u32[]{:S(2)}) copy-start(f32[2,128,256]{2,1,0:T(8,128)} %refs_3_.1) | copy-start | bytes 786436
  132.2 3.0 %copy-start.2 = (f32[2,256]{1,0:T(2,128)S(1)}, f32[2,256]{1,0:T(2,128)}, u32[]{:S(2)}) copy-start(f32[2,256]{1,0:T(2,128)} %refs_4_.3) | copy-start | bytes 6148
  138.4 11.9 %collective-permute-start.6 = (bf16[272,256]{1,0:T(8,128)(2,1)S(1)}, bf16[272,256]{1,0:T(8,128)(2,1)S(1)}, u32[]{:S(2)}, u32[]{:S(2)}) collective-permute-start(bf16[272,256]{1,0:T(8,128)(2,1)S(1)} %shard_map.76.refs_0_), channel_id=1, source_target_pairs={{0,1},{1,2},{2,3},{3,0},{4,5},{5,6},{6,7},{7,4},{8,9},{9,10},{10,1... | collective-permute-start | bytes 417800 | tf_op jit(solution)/shard_map/ppermute | solution.py:73
  141.2 9.2 %collective-permute-start.7 = (bf16[272,256]{1,0:T(8,128)(2,1)S(1)}, bf16[272,256]{1,0:T(8,128)(2,1)S(1)}, u32[]{:S(2)}, u32[]{:S(2)}) collective-permute-start(bf16[272,256]{1,0:T(8,128)(2,1)S(1)} %shard_map.76.refs_0_), channel_id=1, source_target_pairs={{0,2},{1,3},{2,0},{3,1},{4,6},{5,7},{6,4},{7,5},{8,10},{9,11},{10,... | collective-permute-start | bytes 417800 | tf_op jit(solution)/shard_map/ppermute | solution.py:73
  146.0 6.2 %collective-permute-start.8 = (bf16[272,256]{1,0:T(8,128)(2,1)S(1)}, bf16[272,256]{1,0:T(8,128)(2,1)S(1)}, u32[]{:S(2)}, u32[]{:S(2)}) collective-permute-start(bf16[272,256]{1,0:T(8,128)(2,1)S(1)} %shard_map.76.refs_0_), channel_id=1, source_target_pairs={{0,3},{1,0},{2,1},{3,2},{4,7},{5,4},{6,5},{7,6},{8,11},{9,8},{10,9... | collective-permute-start | bytes 417800 | tf_op jit(solution)/shard_map/ppermute | solution.py:73
  153.9 19.0 %copy-start.1 = (bf16[256,512]{1,0:T(8,128)(2,1)}, bf16[256,512]{1,0:T(8,128)(2,1)S(1)}, u32[]{:S(2)}) copy-start(bf16[256,512]{1,0:T(8,128)(2,1)S(1)} %shard_map.78.refs_0_.refs_1_) | copy-start | bytes 786436
  153.9 9.4 %collective-permute-start.10 = (bf16[256,512]{1,0:T(8,128)(2,1)S(1)}, bf16[256,512]{1,0:T(8,128)(2,1)S(1)}, u32[]{:S(2)}, u32[]{:S(2)}) collective-permute-start(bf16[256,512]{1,0:T(8,128)(2,1)S(1)} %shard_map.78.refs_0_.refs_1_), channel_id=1, source_target_pairs={{0,2},{1,3},{2,0},{3,1},{4,6},{5,7},{6,4},{7,5},{8,10},{9,11},{10,... | collective-permute-start | bytes 786440 | tf_op jit(solution)/shard_map/ppermute | solution.py:73
  156.6 13.2 %collective-permute-start.11 = (bf16[256,512]{1,0:T(8,128)(2,1)S(1)}, bf16[256,512]{1,0:T(8,128)(2,1)S(1)}, u32[]{:S(2)}, u32[]{:S(2)}) collective-permute-start(bf16[256,512]{1,0:T(8,128)(2,1)S(1)} %shard_map.78.refs_0_.refs_1_), channel_id=1, source_target_pairs={{0,3},{1,0},{2,1},{3,2},{4,7},{5,4},{6,5},{7,6},{8,11},{9,8},{10,9... | collective-permute-start | bytes 786440 | tf_op jit(solution)/shard_map/ppermute | solution.py:73
  160.7 9.3 %collective-permute-start.9 = (bf16[256,512]{1,0:T(8,128)(2,1)S(1)}, bf16[256,512]{1,0:T(8,128)(2,1)S(1)}, u32[]{:S(2)}, u32[]{:S(2)}) collective-permute-start(bf16[256,512]{1,0:T(8,128)(2,1)S(1)} %shard_map.78.refs_0_.refs_1_), channel_id=1, source_target_pairs={{0,1},{1,2},{2,3},{3,0},{4,5},{5,6},{6,7},{7,4},{8,9},{9,10},{10,1... | collective-permute-start | bytes 786440 | tf_op jit(solution)/shard_map/ppermute | solution.py:73
  173.0 6.8 %collective-permute-start.13 = (bf16[128,256]{1,0:T(8,128)(2,1)S(1)}, bf16[128,256]{1,0:T(8,128)(2,1)S(1)}, u32[]{:S(2)}, u32[]{:S(2)}) collective-permute-start(bf16[128,256]{1,0:T(8,128)(2,1)S(1)} %slice.9), channel_id=1, source_target_pairs={{0,4},{4,8},{8,12},{12,16},{16,20},{20,24},{24,28},{28,32},{32,36}... | collective-permute-start | bytes 196616 | tf_op jit(solution)/shard_map/ppermute | solution.py:525
  182.5 12.6 %all-to-all-start.3 = ((bf16[4,272,256]{2,1,0:T(8,128)(2,1)}), bf16[4,272,256]{2,1,0:T(8,128)(2,1)S(1)}, u32[]{:S(2)}, u32[]{:S(2)}) async-start(bf16[4,272,256]{2,1,0:T(8,128)(2,1)} %shard_map.82), calls=%async_computation.3 | async-start | bytes 1114112 | tf_op jit(solution)/shard_map/all_to_all | solution.py:82
